TPU v7x, 256 devices: a whole 4x4x8 slice. The times are simulated.
256 devices in a mesh: ep: 64 (over z, x, core), tp: 4 (over y).
Axes of the slice: x: 4, y: 4, z: 8, core: 2. Of those that a mesh axis runs over, the one named last changes fastest.
Arguments:
- residual: bfloat16 [2048, 2048], P('ep'), may hold values from -6 to 6
- routes: int32 [2048, 4], P('ep'), may hold values from 0 to 63, as said below
- lengths: int32 [2048], P('ep'), may hold values from 1 to 512, as said below
- key_cache: bfloat16 [2048, 512, 4, 128], P('ep', None, 'tp'), may hold values from -6 to 6
- value_cache: bfloat16 [2048, 512, 4, 128], P('ep', None, 'tp'), may hold values from -6 to 6
- mix_gain: float32 [2048], replicated, may hold values from 0.1 to 1.9
- w_query: bfloat16 [2048, 2048], P(None, 'tp'), may hold values from -0.125 to 0.125
- w_out: bfloat16 [2048, 2048], P('tp'), may hold values from -0.375 to 0.375
- head_bias: float32 [16], P('tp'), may hold values from -7 to -1
- moe_gain: float32 [2048], replicated, may hold values from 0.1 to 1.9
- w_group: bfloat16 [2048, 8], replicated, may hold values from -0.02734375 to 0.02734375
- w_expert: bfloat16 [2048, 64], replicated, may hold values from -0.02734375 to 0.02734375
- expert_gate: bfloat16 [64, 2048, 1024], P('ep', None, 'tp'), may hold values from -0.125 to 0.125
- expert_up: bfloat16 [64, 2048, 1024], P('ep', None, 'tp'), may hold values from -0.125 to 0.125
- expert_down: bfloat16 [64, 1024, 2048], P('ep', 'tp'), may hold values from -3 to 3
Outputs:
- layer_out: bfloat16 [2048, 2048], P('ep', 'tp')
Inputs may be any that keep to these rules, and one draw needn't show every extreme that they name: `routes`: each row names 4 different experts, all in one group of 8 consecutive experts. Within the rows of one device (aligned blocks of 32 rows) no expert is named more than 4 times, and some expert is named exactly 4 times in every block. `lengths`: some sequence has 512 cached positions in every draw.
All inputs are finite; a program needn't handle non-finite values.
Results may differ from a plain program's by a relative error of at most 0.02.
Values may be sent and summed in bfloat16 or wider, within the bound.
No kernel may reach another device: no remote copies, remote signals or barrier semaphores. Data moves between devices by JAX's collectives and lax.ppermute only.
A program may use at most 64 MiB of HBM per device.

v0:
```python
import functools

import jax
import jax.numpy as jnp
from jax import lax
from jax.experimental import pallas as pl
from jax.experimental.pallas import tpu as pltpu
from jax.sharding import PartitionSpec as P


GROUP_SIZE = 8
NZ = 8
NX = 4
NC = 2
EXTRA = 128
COPIES = 4


EPSILON = 1e-06


def rms_scale(tokens, gains):
    values = tokens.astype(jnp.float32)
    inverse = lax.rsqrt(jnp.mean(values * values, axis=-1, keepdims=True) + EPSILON)
    return (values * inverse * gains).astype(jnp.bfloat16)


def ep_index(z, x, c):
    return (z % NZ) * (NX * NC) + (x % NX) * NC + c % NC


def x_shift(value, step):
    perm = [
        (ep_index(z, x, c), ep_index(z, x + step, c))
        for z in range(NZ)
        for x in range(NX)
        for c in range(NC)
    ]
    return lax.ppermute(value, "ep", perm)


def core_swap(value):
    perm = [(i, i ^ 1) for i in range(NZ * NX * NC)]
    return lax.ppermute(value, "ep", perm)


def tp_shift(value, step):
    n = lax.axis_size("tp")
    return lax.ppermute(value, "tp", [(i, (i + step) % n) for i in range(n)])


def z_exchange(value):
    groups = [[z * NX * NC + r for z in range(NZ)] for r in range(NX * NC)]
    return lax.all_to_all(
        value, "ep", split_axis=0, concat_axis=0, axis_index_groups=groups, tiled=True
    )


def split_bf16(value, parts):
    out = []
    for _ in range(parts):
        part = lax.reduce_precision(value, 8, 7).astype(jnp.bfloat16)
        out.append(part)
        value = value - part.astype(jnp.float32)
    return out


def split_in_kernel(value, parts):
    out = []
    for _ in range(parts):
        part = value.astype(jnp.bfloat16)
        out.append(part)
        value = value - part.astype(jnp.float32)
    return out


def attn_kernel(lengths, bias, residual, gain, wq_hbm, k_hbm, v_hbm, wo_hbm, out,
                wq, k, v, wo, q_rows, s_rows, o_rows, wq_sem, wo_sem, k_sem, v_sem):
    seqs, _ = residual.shape
    cache = k.shape[1]
    heads = q_rows.shape[0] // seqs
    size = k.shape[2]
    rows = seqs * heads
    groups = k_sem.shape[0]
    each = seqs // groups
    wq_copy = pltpu.make_async_copy(wq_hbm, wq, wq_sem)
    wo_copy = pltpu.make_async_copy(wo_hbm, wo, wo_sem)

    def copy(src, dst, sem, n):
        part = pl.ds(n * each, each)
        return pltpu.make_async_copy(src.at[part], dst.at[part], sem.at[n])

    k_copies = [copy(k_hbm, k, k_sem, n) for n in range(groups)]
    v_copies = [copy(v_hbm, v, v_sem, n) for n in range(groups)]
    for piece in [wq_copy, *k_copies, *v_copies, wo_copy]:
        piece.start()
    x = residual[...].astype(jnp.float32)
    inverse = lax.rsqrt(jnp.mean(x * x, axis=-1, keepdims=True) + EPSILON)
    normed = (x * inverse * gain[...]).astype(jnp.bfloat16)
    r = lax.broadcasted_iota(jnp.int32, (rows, rows), 0)
    c = lax.broadcasted_iota(jnp.int32, (rows, rows), 1)
    perm = (c == (r % heads) * seqs + r // heads).astype(jnp.bfloat16)
    row = lax.broadcasted_iota(jnp.int32, (rows, 1), 0)
    b = jnp.zeros((rows, 1), jnp.float32)
    for n in range(heads):
        b = jnp.where(row % heads == n, bias[n], b)
    length = jnp.zeros((rows, 1), jnp.int32)
    for t in range(seqs):
        length = jnp.where(row // heads == t, lengths[t], length)
    inside = lax.broadcasted_iota(jnp.int32, (rows, cache), 1) < length
    wq_copy.wait()
    q = jnp.dot(normed, wq[...], preferred_element_type=jnp.float32).astype(jnp.bfloat16)
    q_head = jnp.concatenate([q[:, g * size:(g + 1) * size] for g in range(heads)], axis=0)
    q_rows[...] = jnp.dot(perm, q_head, preferred_element_type=jnp.float32)

    per = 8 // heads
    low = lax.broadcasted_iota(jnp.int32, (8, cache), 0) // heads
    low_o = lax.broadcasted_iota(jnp.int32, (8, size), 0) // heads
    for n in range(groups):
        k_copies[n].wait()
        for i in range(n * each // per, (n + 1) * each // per):
            q8 = q_rows[i * 8:(i + 1) * 8, :].astype(jnp.bfloat16)
            total = None
            for u in range(per):
                s = lax.dot_general(q8, k[i * per + u], (((1,), (1,)), ((), ())),
                                    preferred_element_type=jnp.float32)
                total = s if total is None else jnp.where(low == u, s, total)
            s_rows[i * 8:(i + 1) * 8, :] = total

    z = s_rows[...] * size ** (-0.5) + b
    remain = jnp.where(inside, -(jnp.maximum(z, 0.0) + jnp.log1p(jnp.exp(-jnp.abs(z)))), 0.0)
    first = lax.broadcasted_iota(jnp.int32, (cache, cache), 0)
    second = lax.broadcasted_iota(jnp.int32, (cache, cache), 1)
    later = (first >= second).astype(jnp.bfloat16)
    total = sum(
        jnp.dot(p, later, preferred_element_type=jnp.float32) for p in split_in_kernel(remain, 3)
    )
    s_rows[...] = jnp.where(inside, jnp.exp(z + total), 0.0)

    for n in range(groups):
        v_copies[n].wait()
        for i in range(n * each // per, (n + 1) * each // per):
            w8 = s_rows[i * 8:(i + 1) * 8, :].astype(jnp.bfloat16)
            total = None
            for u in range(per):
                o = jnp.dot(w8, v[i * per + u], preferred_element_type=jnp.float32)
                total = o if total is None else jnp.where(low_o == u, o, total)
            o_rows[i * 8:(i + 1) * 8, :] = total

    o_head = lax.dot_general(perm, o_rows[...].astype(jnp.bfloat16), (((0,), (0,)), ((), ())),
                             preferred_element_type=jnp.float32).astype(jnp.bfloat16)
    att = jnp.concatenate([o_head[n * seqs:(n + 1) * seqs] for n in range(heads)], axis=1)
    wo_copy.wait()
    out[...] = jnp.dot(att, wo[...], preferred_element_type=jnp.float32).astype(out.dtype)


def attention(residual, gain, w_query, w_out, bias, lengths, keys, values):
    seqs, width = residual.shape
    heads = bias.shape[0]
    cache, size = keys.shape[1:]
    hbm = pl.BlockSpec(memory_space=pltpu.HBM)
    vmem = pl.BlockSpec(memory_space=pltpu.VMEM)
    smem = pl.BlockSpec(memory_space=pltpu.SMEM)
    return pl.pallas_call(
        attn_kernel,
        out_shape=pltpu.VMEM((seqs, w_out.shape[1]), jnp.bfloat16),
        in_specs=[smem, smem, vmem, vmem, hbm, hbm, hbm, hbm],
        out_specs=vmem,
        scratch_shapes=[
            pltpu.VMEM(w_query.shape, jnp.bfloat16),
            pltpu.VMEM(keys.shape, jnp.bfloat16),
            pltpu.VMEM(values.shape, jnp.bfloat16),
            pltpu.VMEM(w_out.shape, jnp.bfloat16),
            pltpu.VMEM((seqs * heads, size), jnp.float32),
            pltpu.VMEM((seqs * heads, cache), jnp.float32),
            pltpu.VMEM((seqs * heads, size), jnp.float32),
            pltpu.SemaphoreType.DMA(()),
            pltpu.SemaphoreType.DMA(()),
            pltpu.SemaphoreType.DMA((COPIES,)),
            pltpu.SemaphoreType.DMA((COPIES,)),
        ],
        name="attend",
    )(lengths, bias, residual, gain.reshape(1, width), w_query, keys, values, w_out)


def expert_kernel(count, steps, place, *refs):
    pieces = refs[:count]
    gate_w, up_w, down_w = refs[count : count + 3]
    blocks = refs[count + 3 : count + 3 + steps]
    sent = refs[count + 3 + steps]
    width = gate_w.shape[0]
    rows = jnp.concatenate([piece[:, :width] for piece in pieces], axis=0)
    extra = jnp.concatenate([piece[:, width:] for piece in pieces], axis=0).astype(jnp.float32)
    lane = lax.broadcasted_iota(jnp.int32, extra.shape, 1) % (EXTRA // 2)
    weight = jnp.sum(jnp.where(lane == place[1], extra, 0.0), axis=1, keepdims=True)
    gate = jnp.dot(rows, gate_w[...], preferred_element_type=jnp.float32)
    upward = jnp.dot(rows, up_w[...], preferred_element_type=jnp.float32)
    active = (gate / (1.0 + jnp.exp(-gate)) * upward).astype(jnp.bfloat16)
    own = blocks[0].shape[0]
    block = blocks[0].shape[1]
    for step in range(steps):
        start = pl.multiple_of(lax.rem(place[0] + step, steps) * block, block)
        down = down_w[:, pl.ds(start, block)]
        part = jnp.dot(active, down, preferred_element_type=jnp.float32) * weight
        part = part.astype(jnp.bfloat16)
        blocks[step][...] = part[:own]
        sent[step] = part[own:]


def experts(place, ours, theirs, weights, steps):
    width = weights[2].shape[1]
    rows = sum(piece.shape[0] for piece in ours)
    block = width // steps
    vmem = pl.BlockSpec(memory_space=pltpu.VMEM)
    out = pl.pallas_call(
        functools.partial(expert_kernel, len(ours) + len(theirs), steps),
        out_shape=[pltpu.VMEM((rows, block), jnp.bfloat16)] * steps
        + [pltpu.VMEM((steps, rows, block), jnp.bfloat16)],
        in_specs=[pl.BlockSpec(memory_space=pltpu.SMEM)]
        + [vmem] * (len(ours) + len(theirs) + 3),
        out_specs=[vmem] * (steps + 1),
        compiler_params=pltpu.CompilerParams(vmem_limit_bytes=16 << 20),
        cost_estimate=pl.CostEstimate(
            flops=2 * 2 * rows * 3 * width * weights[0].shape[1],
            transcendentals=2 * rows * weights[0].shape[1],
            bytes_accessed=0,
        ),
        name="experts",
    )(place, *ours, *theirs, *weights)
    return out[:steps], out[steps]


def add_kernel(steps, *refs):
    blocks, arrived, outs = refs[:steps], refs[steps], refs[steps + 1 :]
    for step in range(steps):
        total = blocks[step][...].astype(jnp.float32) + arrived[step].astype(jnp.float32)
        outs[step][...] = total.astype(jnp.bfloat16)


def add_blocks(blocks, arrived):
    steps = len(blocks)
    vmem = pl.BlockSpec(memory_space=pltpu.VMEM)
    return pl.pallas_call(
        functools.partial(add_kernel, steps),
        out_shape=[pltpu.VMEM(blocks[0].shape, jnp.bfloat16)] * steps,
        in_specs=[vmem] * (steps + 1),
        out_specs=[vmem] * steps,
        compiler_params=pltpu.CompilerParams(vmem_limit_bytes=4 << 20),
        name="add_blocks",
    )(*blocks, arrived)


def f32(value):
    return value.astype(jnp.float32)


def per_device(
    residual,
    routes,
    lengths,
    key_cache,
    value_cache,
    mix_gain,
    w_query,
    w_out,
    head_bias,
    moe_gain,
    w_group,
    w_expert,
    expert_gate,
    expert_up,
    expert_down,
):
    bf16 = jnp.bfloat16
    seq_count, width = residual.shape
    n_tp = lax.axis_size("tp")
    tp = lax.axis_index("tp")
    me = lax.axis_index("ep")
    own_width = width // n_tp
    expert_count = w_expert.shape[1]
    group_count = w_group.shape[1]

    head_part = attention(
        residual,
        mix_gain,
        w_query,
        w_out,
        head_bias,
        lengths,
        key_cache.reshape(key_cache.shape[0], key_cache.shape[1], key_cache.shape[3]),
        value_cache.reshape(value_cache.shape[0], value_cache.shape[1], value_cache.shape[3]),
    )
    head_sum = f32(head_part)
    for part in [tp_shift(head_part, step) for step in range(1, n_tp)]:
        head_sum = head_sum + f32(part)
    mid = (f32(residual) + f32(head_sum.astype(bf16))).astype(bf16)
    mid_own = lax.dynamic_slice_in_dim(mid, tp * own_width, own_width, 1)
    hidden_in = rms_scale(mid, moe_gain)

    group_prob = jax.nn.softmax(
        jnp.dot(hidden_in, w_group, preferred_element_type=jnp.float32), axis=-1
    )
    expert_logit = jnp.dot(hidden_in, w_expert, preferred_element_type=jnp.float32)
    expert_ids = jnp.arange(expert_count, dtype=jnp.int32)
    chosen = routes[:, :, None] == expert_ids[None, None, :]
    picked = jnp.sum(jnp.where(chosen, expert_logit[:, None, :], 0.0), axis=2)
    group = routes[:, :1] // GROUP_SIZE
    group_hot = group == jnp.arange(group_count, dtype=jnp.int32)[None, :]
    top_prob = jnp.sum(jnp.where(group_hot, group_prob, 0.0), axis=1, keepdims=True)
    share = jax.nn.softmax(picked, axis=1) * top_prob
    member = routes % GROUP_SIZE
    lanes = jnp.arange(EXTRA // 2, dtype=jnp.int32)
    spread = jnp.sum(
        jnp.where(member[:, :, None] == lanes[None, None, :], share[:, :, None], 0.0), axis=1
    )
    high, low = split_bf16(spread, 2)

    group_row = group[:, 0]
    order = jnp.arange(seq_count, dtype=jnp.int32)
    same = (group_row[:, None] == group_row[None, :]) & (order[None, :] < order[:, None])
    slot = group_row * GROUP_SIZE + jnp.sum(same.astype(jnp.int32), axis=1)
    slots = group_count * GROUP_SIZE
    placing = (jnp.arange(slots, dtype=jnp.int32)[:, None] == slot[None, :]).astype(bf16)
    extended = jnp.concatenate([hidden_in, high, low], axis=1)
    outgoing = jnp.dot(placing, extended, preferred_element_type=jnp.float32).astype(bf16)
    arrived = z_exchange(outgoing.reshape(NZ, GROUP_SIZE, width + EXTRA))
    arrived = arrived.reshape(slots, width + EXTRA)

    half = slots // 2
    place = jnp.stack([tp, me % GROUP_SIZE]).astype(jnp.int32)
    weights = (expert_gate[0], expert_up[0], expert_down[0])

    def chunk(pieces):
        theirs = []
        for piece in pieces:
            theirs.append(core_swap(piece))
        blocks, sent = experts(place, pieces, theirs, weights, n_tp)
        sent = core_swap(sent)
        blocks = add_blocks(blocks, sent)
        total = f32(blocks[0])
        for step in range(1, n_tp):
            part = tp_shift(blocks[step], step)
            total = total + f32(part)
        return total.astype(bf16)

    left = x_shift(arrived, 1)
    right = x_shift(arrived, -1)
    near = chunk([arrived])
    relay0 = x_shift(left[:half], 1)
    relay1 = x_shift(right[half:], -1)
    sides = chunk([left, right])
    far = chunk([relay0, relay1])
    back0 = x_shift(sides[:slots], -1)
    back1 = x_shift(sides[slots:], 1)
    back2 = x_shift(far, 2)
    back = f32(near) + f32(back0) + f32(back1) + f32(back2)
    returned = z_exchange(back.astype(bf16).reshape(NZ, GROUP_SIZE, own_width))
    returned = returned.reshape(slots, own_width)
    moe = lax.dot_general(
        placing, returned, (((0,), (0,)), ((), ())), preferred_element_type=jnp.float32
    )
    return (f32(mid_own) + moe).astype(bf16)


def solution(mesh):
    in_specs = (
        P("ep", None),
        P("ep", None),
        P("ep"),
        P("ep", None, "tp", None),
        P("ep", None, "tp", None),
        P(),
        P(None, "tp"),
        P("tp", None),
        P("tp"),
        P(),
        P(),
        P(),
        P("ep", None, "tp"),
        P("ep", None, "tp"),
        P("ep", "tp", None),
    )
    out_specs = P("ep", "tp")
    return jax.shard_map(
        per_device, mesh=mesh, in_specs=in_specs, out_specs=out_specs, check_vma=False
    )
```

profile of v0, /device:TPU:8, one launch (start us, length us, event | category | flops | bytes accessed | tf_op | source)
XLA Modules:
  0.0 108.3 jit_solution(11918488084654917350)
XLA Ops:
  0.0 8.1 %attend.1 = bf16[32,2048]{1,0:T(8,128)(2,1)S(1)} custom-call(s32[32]{0:T(128)} %lengths.1, f32[4]{0:T(128)} %bias.1, bf16[32,2048]{1,0:T(8,128)(2,1)} %residual.1, f32[1,2048]{1,0:T(1,128)} %bitcast.40, bf16[2048,512]{1,0:T(8,128)(2,1)} %wq_hbm.1, bf16[32,512,128]{2,1,0:T(8,128)(2,1)} %bitcast.38, bf16[32,512,128]{2,1,0:T(8,128)(2,1)} %bitcast.39, ...), custom_call_target="tpu_custom_call" | custom-call | tf_op jit(solution)/shard_map/attend/pallas_call | solution.py:164
  8.1 1.7 %collective-permute-start = (bf16[32,2048]{1,0:T(8,128)(2,1)S(1)}, bf16[32,2048]{1,0:T(8,128)(2,1)S(1)}, u32[]{:S(2)}, u32[]{:S(2)}) collective-permute-start(bf16[32,2048]{1,0:T(8,128)(2,1)S(1)} %attend.1), channel_id=1, source_target_pairs={{0,1},{1,2},{2,3},{3,0},{4,5},{5,6},{6,7},{7,4},{8,9},{9,10},{10,1... | collective-permute-start | bytes 393224 | tf_op jit(solution)/shard_map/ppermute | solution.py:49
  9.8 2.6 %collective-permute-start.1 = (bf16[32,2048]{1,0:T(8,128)(2,1)S(1)}, bf16[32,2048]{1,0:T(8,128)(2,1)S(1)}, u32[]{:S(2)}, u32[]{:S(2)}) collective-permute-start(bf16[32,2048]{1,0:T(8,128)(2,1)S(1)} %attend.1), channel_id=1, source_target_pairs={{0,2},{1,3},{2,0},{3,1},{4,6},{5,7},{6,4},{7,5},{8,10},{9,11},{10,... | collective-permute-start | bytes 393224 | tf_op jit(solution)/shard_map/ppermute | solution.py:49
  14.0 3.7 %collective-permute-done.1 = bf16[32,2048]{1,0:T(8,128)(2,1)S(1)} collective-permute-done((bf16[32,2048]{1,0:T(8,128)(2,1)S(1)}, bf16[32,2048]{1,0:T(8,128)(2,1)S(1)}, u32[]{:S(2)}, u32[]{:S(2)}) %collective-permute-start.1) | collective-permute-done | bytes 131104 | tf_op jit(solution)/shard_map/ppermute | solution.py:49
  18.4 1.1 %fusion.2 = (f32[32]{0:T(128)S(1)}, bf16[32,2048]{1,0:T(8,128)(2,1)S(1)}) fusion(bf16[32,2048]{1,0:T(8,128)(2,1)S(1)} %collective-permute-done.2, bf16[32,2048]{1,0:T(8,128)(2,1)S(1)} %collective-permute-done.1, bf16[32,2048]{1,0:T(8,128)(2,1)S(1)} %collective-permute-done, bf16[32,2048]{1,0:T(8,128)(2,1)S(1)} %attend.1, bf16[32,2048]{1,0:T(8,128)(2,1)} %residual.1), kind=kLoop, calls=%fused_computation.6 | loop fusion | flops 983008 | bytes 786560 | tf_op jit(solution)/shard_map/reduce_sum | solution.py:24
  23.7 1.1 %fusion = bf16[8,8,2176]{2,1,0:T(8,128)(2,1)S(1)} fusion(bf16[32,2176]{1,0:T(8,128)(2,1)} %concatenate.3, s32[32]{0:T(128)} %multiply_add_fusion), kind=kOutput, calls=%fused_computation.1 | convolution fusion | flops 9054208 | bytes 417920 | tf_op jit(solution)/shard_map/dot_general | solution.py:325
  24.8 19.9 %all_to_all.10 = bf16[8,8,2176]{2,1,0:T(8,128)(2,1)S(1)} all-to-all(bf16[8,8,2176]{2,1,0:T(8,128)(2,1)S(1)} %fusion), channel_id=1, replica_groups={{0,32,64,96,128,160,192,224},{4,36,68,100,132,164,196,228},{8,40,72,104..., dimensions={0} | all-to-all | bytes 557056 | tf_op jit(solution)/shard_map/all_to_all | solution.py:54
  44.8 1.5 %collective-permute-start.8 = (bf16[64,2176]{1,0:T(8,128)(2,1)S(1)}, bf16[64,2176]{1,0:T(8,128)(2,1)}, u32[]{:S(2)}, u32[]{:S(2)}) collective-permute-start(bf16[64,2176]{1,0:T(8,128)(2,1)S(1)} %bitcast.34), channel_id=1, source_target_pairs={{0,8},{4,12},{8,16},{12,20},{16,24},{20,28},{24,0},{28,4},{32,40},... | collective-permute-start | bytes 835592 | tf_op jit(solution)/shard_map/ppermute | solution.py:39
  46.2 2.0 %collective-permute-start.9 = (bf16[64,2176]{1,0:T(8,128)(2,1)S(1)}, bf16[64,2176]{1,0:T(8,128)(2,1)}, u32[]{:S(2)}, u32[]{:S(2)}) collective-permute-start(bf16[64,2176]{1,0:T(8,128)(2,1)S(1)} %bitcast.35), channel_id=1, source_target_pairs={{0,24},{4,28},{8,0},{12,4},{16,8},{20,12},{24,16},{28,20},{32,56},... | collective-permute-start | bytes 835592 | tf_op jit(solution)/shard_map/ppermute | solution.py:39
  48.2 4.4 %collective-permute-done.8.refs_0_ = bf16[64,2176]{1,0:T(8,128)(2,1)} collective-permute-done((bf16[64,2176]{1,0:T(8,128)(2,1)S(1)}, bf16[64,2176]{1,0:T(8,128)(2,1)}, u32[]{:S(2)}, u32[]{:S(2)}) %collective-permute-start.8) | collective-permute-done | bytes 278560 | tf_op jit(solution)/shard_map/ppermute | solution.py:39
  53.1 0.9 slice.22
  54.1 1.3 %collective-permute-start.18 = (bf16[32,2176]{1,0:T(8,128)(2,1)S(1)}, bf16[32,2176]{1,0:T(8,128)(2,1)S(1)}, u32[]{:S(2)}, u32[]{:S(2)}) collective-permute-start(bf16[32,2176]{1,0:T(8,128)(2,1)S(1)} %slice.22), channel_id=1, source_target_pairs={{0,8},{4,12},{8,16},{12,20},{16,24},{20,28},{24,0},{28,4},{32,40},... | collective-permute-start | bytes 417800 | tf_op jit(solution)/shard_map/ppermute | solution.py:39
  56.3 2.0 %collective-permute-start.19 = (bf16[32,2176]{1,0:T(8,128)(2,1)S(1)}, bf16[32,2176]{1,0:T(8,128)(2,1)S(1)}, u32[]{:S(2)}, u32[]{:S(2)}) collective-permute-start(bf16[32,2176]{1,0:T(8,128)(2,1)S(1)} %slice.23), channel_id=1, source_target_pairs={{0,24},{4,28},{8,0},{12,4},{16,8},{20,12},{24,16},{28,20},{32,56},... | collective-permute-start | bytes 417800 | tf_op jit(solution)/shard_map/ppermute | solution.py:39
  58.5 2.3 %experts.4 = (bf16[128,512]{1,0:T(8,128)(2,1)S(1)}, bf16[128,512]{1,0:T(8,128)(2,1)S(1)}, bf16[128,512]{1,0:T(8,128)(2,1)S(1)}, bf16[128,512]{1,0:T(8,128)(2,1)S(1)}, bf16[4,128,512]{2,1,0:T(8,128)(2,1)S(1)}) custom-call(s32[2]{0:T(128)S(1)} %pad_add_fusion.place, bf16[64,2176]{1,0:T(8,128)(2,1)} %collective-permute-done.8.refs_0_, ...), custom_call_target="tpu_custom_call" | custom-call | flops 805306368 | tf_op jit(solution)/shard_map/experts/pallas_call | solution.py:215
  62.2 0.9 collective-permute-done.20.refs_2_
  63.6 1.3 %experts.5 = (bf16[64,512]{1,0:T(8,128)(2,1)S(1)}, bf16[64,512]{1,0:T(8,128)(2,1)S(1)}, bf16[64,512]{1,0:T(8,128)(2,1)S(1)}, bf16[64,512]{1,0:T(8,128)(2,1)S(1)}, bf16[4,64,512]{2,1,0:T(8,128)(2,1)S(1)}) custom-call(s32[2]{0:T(128)S(1)} %pad_add_fusion.place, bf16[32,2176]{1,0:T(8,128)(2,1)S(1)} %collective-permute-done.18.refs_0_, ...), custom_call_target="tpu_custom_call" | custom-call | flops 402653184 | tf_op jit(solution)/shard_map/experts/pallas_call | solution.py:215
  65.1 1.3 %experts.3 = (bf16[64,512]{1,0:T(8,128)(2,1)S(1)}, bf16[64,512]{1,0:T(8,128)(2,1)S(1)}, bf16[64,512]{1,0:T(8,128)(2,1)S(1)}, bf16[64,512]{1,0:T(8,128)(2,1)S(1)}, bf16[4,64,512]{2,1,0:T(8,128)(2,1)S(1)}) custom-call(s32[2]{0:T(128)S(1)} %pad_add_fusion.place, bf16[64,2176]{1,0:T(8,128)(2,1)S(1)} %bitcast.37, ...), custom_call_target="tpu_custom_call" | custom-call | flops 402653184 | tf_op jit(solution)/shard_map/experts/pallas_call | solution.py:215
  67.7 1.8 %collective-permute-start.24 = (bf16[64,512]{1,0:T(8,128)(2,1)S(1)}, bf16[64,512]{1,0:T(8,128)(2,1)S(1)}, u32[]{:S(2)}, u32[]{:S(2)}) collective-permute-start(bf16[64,512]{1,0:T(8,128)(2,1)S(1)} %get-tuple-element.57), channel_id=1, source_target_pairs={{0,2},{1,3},{2,0},{3,1},{4,6},{5,7},{6,4},{7,5},{8,10},{9,11},{10,... | collective-permute-start | bytes 196616 | tf_op jit(solution)/shard_map/ppermute | solution.py:49
  69.5 1.9 %collective-permute-start.25 = (bf16[64,512]{1,0:T(8,128)(2,1)S(1)}, bf16[64,512]{1,0:T(8,128)(2,1)S(1)}, u32[]{:S(2)}, u32[]{:S(2)}) collective-permute-start(bf16[64,512]{1,0:T(8,128)(2,1)S(1)} %get-tuple-element.58), channel_id=1, source_target_pairs={{0,3},{1,0},{2,1},{3,2},{4,7},{5,4},{6,5},{7,6},{8,11},{9,8},{10,9... | collective-permute-start | bytes 196616 | tf_op jit(solution)/shard_map/ppermute | solution.py:49
  71.7 2.9 %collective-permute-start.6 = (bf16[64,512]{1,0:T(8,128)(2,1)S(1)}, bf16[64,512]{1,0:T(8,128)(2,1)S(1)}, u32[]{:S(2)}, u32[]{:S(2)}) collective-permute-start(bf16[64,512]{1,0:T(8,128)(2,1)S(1)} %get-tuple-element.39), channel_id=1, source_target_pairs={{0,2},{1,3},{2,0},{3,1},{4,6},{5,7},{6,4},{7,5},{8,10},{9,11},{10,... | collective-permute-start | bytes 196616 | tf_op jit(solution)/shard_map/ppermute | solution.py:49
  75.3 1.7 %collective-permute-start.14 = (bf16[128,512]{1,0:T(8,128)(2,1)S(1)}, bf16[128,512]{1,0:T(8,128)(2,1)S(1)}, u32[]{:S(2)}, u32[]{:S(2)}) collective-permute-start(bf16[128,512]{1,0:T(8,128)(2,1)S(1)} %get-tuple-element.48), channel_id=1, source_target_pairs={{0,2},{1,3},{2,0},{3,1},{4,6},{5,7},{6,4},{7,5},{8,10},{9,11},{10,... | collective-permute-start | bytes 393224 | tf_op jit(solution)/shard_map/ppermute | solution.py:49
  77.0 1.1 %collective-permute-start.15 = (bf16[128,512]{1,0:T(8,128)(2,1)S(1)}, bf16[128,512]{1,0:T(8,128)(2,1)S(1)}, u32[]{:S(2)}, u32[]{:S(2)}) collective-permute-start(bf16[128,512]{1,0:T(8,128)(2,1)S(1)} %get-tuple-element.49), channel_id=1, source_target_pairs={{0,3},{1,0},{2,1},{3,2},{4,7},{5,4},{6,5},{7,6},{8,11},{9,8},{10,9... | collective-permute-start | bytes 393224 | tf_op jit(solution)/shard_map/ppermute | solution.py:49
  78.1 3.0 %collective-permute-done.13 = bf16[128,512]{1,0:T(8,128)(2,1)S(1)} collective-permute-done((bf16[128,512]{1,0:T(8,128)(2,1)S(1)}, bf16[128,512]{1,0:T(8,128)(2,1)S(1)}, u32[]{:S(2)}, u32[]{:S(2)}) %collective-permute-start.13) | collective-permute-done | bytes 131104 | tf_op jit(solution)/shard_map/ppermute | solution.py:49
  81.1 3.5 %collective-permute-start.7 = (bf16[64,512]{1,0:T(8,128)(2,1)S(1)}, bf16[64,512]{1,0:T(8,128)(2,1)S(1)}, u32[]{:S(2)}, u32[]{:S(2)}) collective-permute-start(bf16[64,512]{1,0:T(8,128)(2,1)S(1)} %get-tuple-element.40), channel_id=1, source_target_pairs={{0,3},{1,0},{2,1},{3,2},{4,7},{5,4},{6,5},{7,6},{8,11},{9,8},{10,9... | collective-permute-start | bytes 196616 | tf_op jit(solution)/shard_map/ppermute | solution.py:49
  84.7 3.2 %collective-permute-start.26 = (bf16[64,512]{1,0:T(8,128)(2,1)S(1)}, bf16[64,512]{1,0:T(8,128)(2,1)S(1)}, u32[]{:S(2)}, u32[]{:S(2)}) collective-permute-start(bf16[64,512]{1,0:T(8,128)(2,1)S(1)} %add_convert_fusion.4), channel_id=1, source_target_pairs={{0,16},{4,20},{8,24},{12,28},{16,0},{20,4},{24,8},{28,12},{32,48},... | collective-permute-start | bytes 196616 | tf_op jit(solution)/shard_map/ppermute | solution.py:39
  87.9 1.0 collective-permute-start.16
  88.9 1.1 %collective-permute-start.17 = (bf16[64,512]{1,0:T(8,128)(2,1)S(1)}, bf16[64,512]{1,0:T(8,128)(2,1)S(1)}, u32[]{:S(2)}, u32[]{:S(2)}) collective-permute-start(bf16[64,512]{1,0:T(8,128)(2,1)S(1)} %get-tuple-element.62), channel_id=1, source_target_pairs={{0,8},{4,12},{8,16},{12,20},{16,24},{20,28},{24,0},{28,4},{32,40},... | collective-permute-start | bytes 196616 | tf_op jit(solution)/shard_map/ppermute | solution.py:39
  90.5 1.8 %collective-permute-done.16 = bf16[64,512]{1,0:T(8,128)(2,1)S(1)} collective-permute-done((bf16[64,512]{1,0:T(8,128)(2,1)S(1)}, bf16[64,512]{1,0:T(8,128)(2,1)S(1)}, u32[]{:S(2)}, u32[]{:S(2)}) %collective-permute-start.16) | collective-permute-done | bytes 65568 | tf_op jit(solution)/shard_map/ppermute | solution.py:39
  92.2 2.1 %collective-permute-done.17 = bf16[64,512]{1,0:T(8,128)(2,1)S(1)} collective-permute-done((bf16[64,512]{1,0:T(8,128)(2,1)S(1)}, bf16[64,512]{1,0:T(8,128)(2,1)S(1)}, u32[]{:S(2)}, u32[]{:S(2)}) %collective-permute-start.17) | collective-permute-done | bytes 65568 | tf_op jit(solution)/shard_map/ppermute | solution.py:39
  95.0 3.3 %all-to-all-start.1 = ((bf16[8,8,512]{2,1,0:T(8,128)(2,1)}), bf16[8,8,512]{2,1,0:T(8,128)(2,1)S(1)}, u32[]{:S(2)}, u32[]{:S(2)}) async-start(bf16[8,8,512]{2,1,0:T(8,128)(2,1)} %fusion.5), calls=%async_computation.1 | async-start | bytes 131072 | tf_op jit(solution)/shard_map/all_to_all | solution.py:54
  98.4 8.3 %all-to-all-done.1 = bf16[8,8,512]{2,1,0:T(8,128)(2,1)S(1)} async-done(((bf16[8,8,512]{2,1,0:T(8,128)(2,1)}), bf16[8,8,512]{2,1,0:T(8,128)(2,1)S(1)}, u32[]{:S(2)}, u32[]{:S(2)}) %all-to-all-start.1) | async-done | bytes 65568 | tf_op jit(solution)/shard_map/all_to_all | solution.py:54
  106.7 1.6 %fusion.1 = bf16[32,512]{1,0:T(8,128)(2,1)} fusion(bf16[8,8,512]{2,1,0:T(8,128)(2,1)S(1)} %all-to-all-done.1, bf16[32,2048]{1,0:T(8,128)(2,1)} %copy-done.6, s32[]{:T(128)S(6)} %select_n.33, s32[32]{0:T(128)S(1)} %copy-done.9), kind=kOutput, calls=%fused_computation.3 | convolution fusion | flops 2148352 | bytes 131204 | tf_op jit(solution)/shard_map/dot_general | solution.py:359
  (79 shorter events, 13.5 us)
Async XLA Ops:
  8.1 50.4 %copy-start.1 = (bf16[1,2048,256]{2,1,0:T(8,128)(2,1)S(1)}, bf16[1,2048,256]{2,1,0:T(8,128)(2,1)}, u32[]{:S(2)}) copy-start(bf16[1,2048,256]{2,1,0:T(8,128)(2,1)} %param.27) | copy-start | bytes 3145732
  8.1 50.4 %copy-start.2 = (bf16[1,2048,256]{2,1,0:T(8,128)(2,1)S(1)}, bf16[1,2048,256]{2,1,0:T(8,128)(2,1)}, u32[]{:S(2)}) copy-start(bf16[1,2048,256]{2,1,0:T(8,128)(2,1)} %param.28) | copy-start | bytes 3145732
  8.1 50.4 %copy-start.3 = (bf16[1,256,2048]{2,1,0:T(8,128)(2,1)S(1)}, bf16[1,256,2048]{2,1,0:T(8,128)(2,1)}, u32[]{:S(2)}) copy-start(bf16[1,256,2048]{2,1,0:T(8,128)(2,1)} %param.29) | copy-start | bytes 3145732
  8.1 5.8 %collective-permute-start = (bf16[32,2048]{1,0:T(8,128)(2,1)S(1)}, bf16[32,2048]{1,0:T(8,128)(2,1)S(1)}, u32[]{:S(2)}, u32[]{:S(2)}) collective-permute-start(bf16[32,2048]{1,0:T(8,128)(2,1)S(1)} %attend.1), channel_id=1, source_target_pairs={{0,1},{1,2},{2,3},{3,0},{4,5},{5,6},{6,7},{7,4},{8,9},{9,10},{10,1... | collective-permute-start | bytes 393224 | tf_op jit(solution)/shard_map/ppermute | solution.py:49
  9.8 7.9 %collective-permute-start.1 = (bf16[32,2048]{1,0:T(8,128)(2,1)S(1)}, bf16[32,2048]{1,0:T(8,128)(2,1)S(1)}, u32[]{:S(2)}, u32[]{:S(2)}) collective-permute-start(bf16[32,2048]{1,0:T(8,128)(2,1)S(1)} %attend.1), channel_id=1, source_target_pairs={{0,2},{1,3},{2,0},{3,1},{4,6},{5,7},{6,4},{7,5},{8,10},{9,11},{10,... | collective-permute-start | bytes 393224 | tf_op jit(solution)/shard_map/ppermute | solution.py:49
  12.4 5.9 %collective-permute-start.2 = (bf16[32,2048]{1,0:T(8,128)(2,1)S(1)}, bf16[32,2048]{1,0:T(8,128)(2,1)S(1)}, u32[]{:S(2)}, u32[]{:S(2)}) collective-permute-start(bf16[32,2048]{1,0:T(8,128)(2,1)S(1)} %attend.1), channel_id=1, source_target_pairs={{0,3},{1,0},{2,1},{3,2},{4,7},{5,4},{6,5},{7,6},{8,11},{9,8},{10,9... | collective-permute-start | bytes 393224 | tf_op jit(solution)/shard_map/ppermute | solution.py:49
  44.8 7.9 %collective-permute-start.8 = (bf16[64,2176]{1,0:T(8,128)(2,1)S(1)}, bf16[64,2176]{1,0:T(8,128)(2,1)}, u32[]{:S(2)}, u32[]{:S(2)}) collective-permute-start(bf16[64,2176]{1,0:T(8,128)(2,1)S(1)} %bitcast.34), channel_id=1, source_target_pairs={{0,8},{4,12},{8,16},{12,20},{16,24},{20,28},{24,0},{28,4},{32,40},... | collective-permute-start | bytes 835592 | tf_op jit(solution)/shard_map/ppermute | solution.py:39
  46.2 6.7 %collective-permute-start.9 = (bf16[64,2176]{1,0:T(8,128)(2,1)S(1)}, bf16[64,2176]{1,0:T(8,128)(2,1)}, u32[]{:S(2)}, u32[]{:S(2)}) collective-permute-start(bf16[64,2176]{1,0:T(8,128)(2,1)S(1)} %bitcast.35), channel_id=1, source_target_pairs={{0,24},{4,28},{8,0},{12,4},{16,8},{20,12},{24,16},{28,20},{32,56},... | collective-permute-start | bytes 835592 | tf_op jit(solution)/shard_map/ppermute | solution.py:39
  52.6 5.9 %collective-permute-start.10 = (bf16[64,2176]{1,0:T(8,128)(2,1)}, bf16[64,2176]{1,0:T(8,128)(2,1)}, u32[]{:S(2)}, u32[]{:S(2)}) collective-permute-start(bf16[64,2176]{1,0:T(8,128)(2,1)} %collective-permute-done.8.refs_0_), channel_id=1, source_target_pairs={{0,4},{4,0},{8,12},{12,8},{16,20},{20,16},{24,28},{28,24},{32,36},... | collective-permute-start | bytes 835592 | tf_op jit(solution)/shard_map/ppermute | solution.py:44
  52.9 5.6 %collective-permute-start.11 = (bf16[64,2176]{1,0:T(8,128)(2,1)}, bf16[64,2176]{1,0:T(8,128)(2,1)}, u32[]{:S(2)}, u32[]{:S(2)}) collective-permute-start(bf16[64,2176]{1,0:T(8,128)(2,1)} %collective-permute-done.9.refs_1_), channel_id=1, source_target_pairs={{0,4},{4,0},{8,12},{12,8},{16,20},{20,16},{24,28},{28,24},{32,36},... | collective-permute-start | bytes 835592 | tf_op jit(solution)/shard_map/ppermute | solution.py:44
  54.1 7.4 %collective-permute-start.18 = (bf16[32,2176]{1,0:T(8,128)(2,1)S(1)}, bf16[32,2176]{1,0:T(8,128)(2,1)S(1)}, u32[]{:S(2)}, u32[]{:S(2)}) collective-permute-start(bf16[32,2176]{1,0:T(8,128)(2,1)S(1)} %slice.22), channel_id=1, source_target_pairs={{0,8},{4,12},{8,16},{12,20},{16,24},{20,28},{24,0},{28,4},{32,40},... | collective-permute-start | bytes 417800 | tf_op jit(solution)/shard_map/ppermute | solution.py:39
  56.3 5.9 %collective-permute-start.19 = (bf16[32,2176]{1,0:T(8,128)(2,1)S(1)}, bf16[32,2176]{1,0:T(8,128)(2,1)S(1)}, u32[]{:S(2)}, u32[]{:S(2)}) collective-permute-start(bf16[32,2176]{1,0:T(8,128)(2,1)S(1)} %slice.23), channel_id=1, source_target_pairs={{0,24},{4,28},{8,0},{12,4},{16,8},{20,12},{24,16},{28,20},{32,56},... | collective-permute-start | bytes 417800 | tf_op jit(solution)/shard_map/ppermute | solution.py:39
  58.5 6.6 %collective-permute-start.3 = (bf16[64,2176]{1,0:T(8,128)(2,1)}, bf16[64,2176]{1,0:T(8,128)(2,1)S(1)}, u32[]{:S(2)}, u32[]{:S(2)}) collective-permute-start(bf16[64,2176]{1,0:T(8,128)(2,1)} %bitcast.36), channel_id=1, source_target_pairs={{0,4},{4,0},{8,12},{12,8},{16,20},{20,16},{24,28},{28,24},{32,36},... | collective-permute-start | bytes 835592 | tf_op jit(solution)/shard_map/ppermute | solution.py:44
  60.9 10.9 %collective-permute-start.12 = (bf16[4,128,512]{2,1,0:T(8,128)(2,1)S(1)}, bf16[4,128,512]{2,1,0:T(8,128)(2,1)S(1)}, u32[]{:S(2)}, u32[]{:S(2)}) collective-permute-start(bf16[4,128,512]{2,1,0:T(8,128)(2,1)S(1)} %get-tuple-element.45), channel_id=1, source_target_pairs={{0,4},{4,0},{8,12},{12,8},{16,20},{20,16},{24,28},{28,24},{32,36},... | collective-permute-start | bytes 1572872 | tf_op jit(solution)/shard_map/ppermute | solution.py:44
  61.4 1.7 %collective-permute-start.20 = (bf16[32,2176]{1,0:T(8,128)(2,1)S(1)}, bf16[32,2176]{1,0:T(8,128)(2,1)S(1)}, u32[]{:S(2)}, u32[]{:S(2)}) collective-permute-start(bf16[32,2176]{1,0:T(8,128)(2,1)S(1)} %collective-permute-done.18.refs_0_), channel_id=1, source_target_pairs={{0,4},{4,0},{8,12},{12,8},{16,20},{20,16},{24,28},{28,24},{32,36},... | collective-permute-start | bytes 417800 | tf_op jit(solution)/shard_map/ppermute | solution.py:44
  62.2 1.4 %collective-permute-start.21 = (bf16[32,2176]{1,0:T(8,128)(2,1)S(1)}, bf16[32,2176]{1,0:T(8,128)(2,1)S(1)}, u32[]{:S(2)}, u32[]{:S(2)}) collective-permute-start(bf16[32,2176]{1,0:T(8,128)(2,1)S(1)} %collective-permute-done.19.refs_1_), channel_id=1, source_target_pairs={{0,4},{4,0},{8,12},{12,8},{16,20},{20,16},{24,28},{28,24},{32,36},... | collective-permute-start | bytes 417800 | tf_op jit(solution)/shard_map/ppermute | solution.py:44
  64.8 41.9 %copy-start.9 = (s32[32]{0:T(128)S(1)}, s32[32]{0:T(128)}, u32[]{:S(2)}) copy-start(s32[32]{0:T(128)} %multiply_add_fusion) | copy-start | bytes 388
  64.9 2.0 %collective-permute-start.22 = (bf16[4,64,512]{2,1,0:T(8,128)(2,1)S(1)}, bf16[4,64,512]{2,1,0:T(8,128)(2,1)S(1)}, u32[]{:S(2)}, u32[]{:S(2)}) collective-permute-start(bf16[4,64,512]{2,1,0:T(8,128)(2,1)S(1)} %get-tuple-element.54), channel_id=1, source_target_pairs={{0,4},{4,0},{8,12},{12,8},{16,20},{20,16},{24,28},{28,24},{32,36},... | collective-permute-start | bytes 786440 | tf_op jit(solution)/shard_map/ppermute | solution.py:44
  66.4 5.1 %collective-permute-start.4 = (bf16[4,64,512]{2,1,0:T(8,128)(2,1)S(1)}, bf16[4,64,512]{2,1,0:T(8,128)(2,1)S(1)}, u32[]{:S(2)}, u32[]{:S(2)}) collective-permute-start(bf16[4,64,512]{2,1,0:T(8,128)(2,1)S(1)} %get-tuple-element.36), channel_id=1, source_target_pairs={{0,4},{4,0},{8,12},{12,8},{16,20},{20,16},{24,28},{28,24},{32,36},... | collective-permute-start | bytes 786440 | tf_op jit(solution)/shard_map/ppermute | solution.py:44
  66.9 7.9 %collective-permute-start.23 = (bf16[64,512]{1,0:T(8,128)(2,1)S(1)}, bf16[64,512]{1,0:T(8,128)(2,1)S(1)}, u32[]{:S(2)}, u32[]{:S(2)}) collective-permute-start(bf16[64,512]{1,0:T(8,128)(2,1)S(1)} %get-tuple-element.56), channel_id=1, source_target_pairs={{0,1},{1,2},{2,3},{3,0},{4,5},{5,6},{6,7},{7,4},{8,9},{9,10},{10,1... | collective-permute-start | bytes 196616 | tf_op jit(solution)/shard_map/ppermute | solution.py:49
  67.7 7.6 %collective-permute-start.24 = (bf16[64,512]{1,0:T(8,128)(2,1)S(1)}, bf16[64,512]{1,0:T(8,128)(2,1)S(1)}, u32[]{:S(2)}, u32[]{:S(2)}) collective-permute-start(bf16[64,512]{1,0:T(8,128)(2,1)S(1)} %get-tuple-element.57), channel_id=1, source_target_pairs={{0,2},{1,3},{2,0},{3,1},{4,6},{5,7},{6,4},{7,5},{8,10},{9,11},{10,... | collective-permute-start | bytes 196616 | tf_op jit(solution)/shard_map/ppermute | solution.py:49
  69.5 7.4 %collective-permute-start.25 = (bf16[64,512]{1,0:T(8,128)(2,1)S(1)}, bf16[64,512]{1,0:T(8,128)(2,1)S(1)}, u32[]{:S(2)}, u32[]{:S(2)}) collective-permute-start(bf16[64,512]{1,0:T(8,128)(2,1)S(1)} %get-tuple-element.58), channel_id=1, source_target_pairs={{0,3},{1,0},{2,1},{3,2},{4,7},{5,4},{6,5},{7,6},{8,11},{9,8},{10,9... | collective-permute-start | bytes 196616 | tf_op jit(solution)/shard_map/ppermute | solution.py:49
  71.5 17.4 %collective-permute-start.5 = (bf16[64,512]{1,0:T(8,128)(2,1)S(1)}, bf16[64,512]{1,0:T(8,128)(2,1)S(1)}, u32[]{:S(2)}, u32[]{:S(2)}) collective-permute-start(bf16[64,512]{1,0:T(8,128)(2,1)S(1)} %get-tuple-element.38), channel_id=1, source_target_pairs={{0,1},{1,2},{2,3},{3,0},{4,5},{5,6},{6,7},{7,4},{8,9},{9,10},{10,1... | collective-permute-start | bytes 196616 | tf_op jit(solution)/shard_map/ppermute | solution.py:49
  71.7 18.3 %collective-permute-start.6 = (bf16[64,512]{1,0:T(8,128)(2,1)S(1)}, bf16[64,512]{1,0:T(8,128)(2,1)S(1)}, u32[]{:S(2)}, u32[]{:S(2)}) collective-permute-start(bf16[64,512]{1,0:T(8,128)(2,1)S(1)} %get-tuple-element.39), channel_id=1, source_target_pairs={{0,2},{1,3},{2,0},{3,1},{4,6},{5,7},{6,4},{7,5},{8,10},{9,11},{10,... | collective-permute-start | bytes 196616 | tf_op jit(solution)/shard_map/ppermute | solution.py:49
  74.8 6.3 %collective-permute-start.13 = (bf16[128,512]{1,0:T(8,128)(2,1)S(1)}, bf16[128,512]{1,0:T(8,128)(2,1)S(1)}, u32[]{:S(2)}, u32[]{:S(2)}) collective-permute-start(bf16[128,512]{1,0:T(8,128)(2,1)S(1)} %get-tuple-element.47), channel_id=1, source_target_pairs={{0,1},{1,2},{2,3},{3,0},{4,5},{5,6},{6,7},{7,4},{8,9},{9,10},{10,1... | collective-permute-start | bytes 393224 | tf_op jit(solution)/shard_map/ppermute | solution.py:49
  75.3 9.4 %collective-permute-start.14 = (bf16[128,512]{1,0:T(8,128)(2,1)S(1)}, bf16[128,512]{1,0:T(8,128)(2,1)S(1)}, u32[]{:S(2)}, u32[]{:S(2)}) collective-permute-start(bf16[128,512]{1,0:T(8,128)(2,1)S(1)} %get-tuple-element.48), channel_id=1, source_target_pairs={{0,2},{1,3},{2,0},{3,1},{4,6},{5,7},{6,4},{7,5},{8,10},{9,11},{10,... | collective-permute-start | bytes 393224 | tf_op jit(solution)/shard_map/ppermute | solution.py:49
  77.0 10.8 %collective-permute-start.15 = (bf16[128,512]{1,0:T(8,128)(2,1)S(1)}, bf16[128,512]{1,0:T(8,128)(2,1)S(1)}, u32[]{:S(2)}, u32[]{:S(2)}) collective-permute-start(bf16[128,512]{1,0:T(8,128)(2,1)S(1)} %get-tuple-element.49), channel_id=1, source_target_pairs={{0,3},{1,0},{2,1},{3,2},{4,7},{5,4},{6,5},{7,6},{8,11},{9,8},{10,9... | collective-permute-start | bytes 393224 | tf_op jit(solution)/shard_map/ppermute | solution.py:49
  81.1 8.9 %collective-permute-start.7 = (bf16[64,512]{1,0:T(8,128)(2,1)S(1)}, bf16[64,512]{1,0:T(8,128)(2,1)S(1)}, u32[]{:S(2)}, u32[]{:S(2)}) collective-permute-start(bf16[64,512]{1,0:T(8,128)(2,1)S(1)} %get-tuple-element.40), channel_id=1, source_target_pairs={{0,3},{1,0},{2,1},{3,2},{4,7},{5,4},{6,5},{7,6},{8,11},{9,8},{10,9... | collective-permute-start | bytes 196616 | tf_op jit(solution)/shard_map/ppermute | solution.py:49
  84.7 5.8 %collective-permute-start.26 = (bf16[64,512]{1,0:T(8,128)(2,1)S(1)}, bf16[64,512]{1,0:T(8,128)(2,1)S(1)}, u32[]{:S(2)}, u32[]{:S(2)}) collective-permute-start(bf16[64,512]{1,0:T(8,128)(2,1)S(1)} %add_convert_fusion.4), channel_id=1, source_target_pairs={{0,16},{4,20},{8,24},{12,28},{16,0},{20,4},{24,8},{28,12},{32,48},... | collective-permute-start | bytes 196616 | tf_op jit(solution)/shard_map/ppermute | solution.py:39
  87.9 4.3 %collective-permute-start.16 = (bf16[64,512]{1,0:T(8,128)(2,1)S(1)}, bf16[64,512]{1,0:T(8,128)(2,1)S(1)}, u32[]{:S(2)}, u32[]{:S(2)}) collective-permute-start(bf16[64,512]{1,0:T(8,128)(2,1)S(1)} %get-tuple-element.61), channel_id=1, source_target_pairs={{0,24},{4,28},{8,0},{12,4},{16,8},{20,12},{24,16},{28,20},{32,56},... | collective-permute-start | bytes 196616 | tf_op jit(solution)/shard_map/ppermute | solution.py:39
  88.9 5.5 %collective-permute-start.17 = (bf16[64,512]{1,0:T(8,128)(2,1)S(1)}, bf16[64,512]{1,0:T(8,128)(2,1)S(1)}, u32[]{:S(2)}, u32[]{:S(2)}) collective-permute-start(bf16[64,512]{1,0:T(8,128)(2,1)S(1)} %get-tuple-element.62), channel_id=1, source_target_pairs={{0,8},{4,12},{8,16},{12,20},{16,24},{20,28},{24,0},{28,4},{32,40},... | collective-permute-start | bytes 196616 | tf_op jit(solution)/shard_map/ppermute | solution.py:39
  95.0 11.7 %all-to-all-start.1 = ((bf16[8,8,512]{2,1,0:T(8,128)(2,1)}), bf16[8,8,512]{2,1,0:T(8,128)(2,1)S(1)}, u32[]{:S(2)}, u32[]{:S(2)}) async-start(bf16[8,8,512]{2,1,0:T(8,128)(2,1)} %fusion.5), calls=%async_computation.1 | async-start | bytes 131072 | tf_op jit(solution)/shard_map/all_to_all | solution.py:54
  (6 other events, 68.3 us)
where the time goes:
time: 109 us; the launch traced here: 108 us
  starting transfers between devices  36.6 us (34%)
  waiting for transfers between devices  26.8 us (25%)
  blocking collectives  19.9 us (18%)
  Pallas kernels  13.2 us (12%)
  other arithmetic  4.47 us (4%)
  matrix products  3.78 us (3%)
  local copies, waits for them, and re-layouts  3.27 us (3%)
    all_to_all x1, blocking collectives, z_exchange(): lax.all_to_all(value, 'ep', split_axis=0, concat_axis=0, axis_index_group...  19.9 us
    ppermute x12, starting transfers between devices, tp_shift(): return lax.ppermute(value, 'tp', [(i, (i + step) % n) for i in range(n)])  19.5 us
    ppermute x7, starting transfers between devices, x_shift(): return lax.ppermute(value, 'ep', perm)  12.1 us
    ppermute x7, waiting for transfers between devices, x_shift(): return lax.ppermute(value, 'ep', perm)  9.72 us
    all_to_all x1, waiting for transfers between devices, z_exchange(): lax.all_to_all(value, 'ep', split_axis=0, concat_axis=0, axis_index_group...  8.29 us
    pallas_call x1, Pallas kernels, attention(): pl.pallas_call(attn_kernel, out_shape=pltpu.VMEM((seqs, w_out.shape[1]),...  8.09 us
    ppermute x12, waiting for transfers between devices, tp_shift(): return lax.ppermute(value, 'tp', [(i, (i + step) % n) for i in range(n)])  7.44 us
    pallas_call x3, Pallas kernels, experts(): pl.pallas_call(functools.partial(expert_kernel, len(ours) + len(theirs),...  4.84 us
  transfers between devices with their start and end apart: 28, of which 12 were waited for; matrix products, arithmetic and copies ran while one was open for 3% of the time, Pallas kernels for 5%

commit v1 on v0

--- a/solution.py
+++ b/solution.py
@@ -9,6 +9,7 @@
 
 
 GROUP_SIZE = 8
+TOPK = 4
 NZ = 8
 NX = 4
 NC = 2
@@ -17,12 +18,6 @@
 
 
 EPSILON = 1e-06
-
-
-def rms_scale(tokens, gains):
-    values = tokens.astype(jnp.float32)
-    inverse = lax.rsqrt(jnp.mean(values * values, axis=-1, keepdims=True) + EPSILON)
-    return (values * inverse * gains).astype(jnp.bfloat16)
 
 
 def ep_index(z, x, c):
@@ -54,15 +49,6 @@
     return lax.all_to_all(
         value, "ep", split_axis=0, concat_axis=0, axis_index_groups=groups, tiled=True
     )
-
-
-def split_bf16(value, parts):
-    out = []
-    for _ in range(parts):
-        part = lax.reduce_precision(value, 8, 7).astype(jnp.bfloat16)
-        out.append(part)
-        value = value - part.astype(jnp.float32)
-    return out
 
 
 def split_in_kernel(value, parts):
@@ -183,75 +169,141 @@
     )(lengths, bias, residual, gain.reshape(1, width), w_query, keys, values, w_out)
 
 
-def expert_kernel(count, steps, place, *refs):
+def call(kernel, outs, args, flops=0, vmem=16):
+    in_vmem = pl.BlockSpec(memory_space=pltpu.VMEM)
+    in_smem = pl.BlockSpec(memory_space=pltpu.SMEM)
+    return pl.pallas_call(
+        kernel,
+        out_shape=[pltpu.VMEM(shape, dtype) for shape, dtype in outs],
+        in_specs=[in_smem if arg.ndim == 1 else in_vmem for arg in args],
+        out_specs=[in_vmem] * len(outs),
+        compiler_params=pltpu.CompilerParams(vmem_limit_bytes=vmem << 20),
+        cost_estimate=pl.CostEstimate(flops=flops, transcendentals=0, bytes_accessed=0),
+    )(*args)
+
+
+def route_kernel(count, place, *refs):
+    parts = refs[:count]
+    residual, gain, group_w, expert_w, routes, outgoing, mid_own, placing = refs[count:]
+    total = sum(part[...].astype(jnp.float32) for part in parts)
+    mid = residual[...].astype(jnp.float32) + total.astype(jnp.bfloat16).astype(jnp.float32)
+    mid = mid.astype(jnp.bfloat16)
+    values = mid.astype(jnp.float32)
+    seqs, width = values.shape
+    inverse = lax.rsqrt(jnp.mean(values * values, axis=-1, keepdims=True) + EPSILON)
+    hidden = (values * inverse * gain[...]).astype(jnp.bfloat16)
+
+    def logits(weight):
+        return lax.dot_general(
+            hidden, weight[...], (((1,), (1,)), ((), ())), preferred_element_type=jnp.float32
+        )
+
+    group_logit = logits(group_w)
+    expert_logit = logits(expert_w)
+    named = [routes[:, k : k + 1] for k in range(TOPK)]
+    group = jnp.right_shift(named[0], 3)
+    member = [jnp.bitwise_and(one, GROUP_SIZE - 1) for one in named]
+    lane_e = lax.broadcasted_iota(jnp.int32, expert_logit.shape, 1)
+    lane_g = lax.broadcasted_iota(jnp.int32, group_logit.shape, 1)
+    picked = [
+        jnp.sum(jnp.where(lane_e == one, expert_logit, 0.0), axis=1, keepdims=True)
+        for one in named
+    ]
+    most = functools.reduce(jnp.maximum, picked)
+    powers = [jnp.exp(one - most) for one in picked]
+    group_power = jnp.exp(group_logit - jnp.max(group_logit, axis=1, keepdims=True))
+    in_group = lane_g == group
+    top = jnp.sum(jnp.where(in_group, group_power, 0.0), axis=1, keepdims=True)
+    top = top / jnp.sum(group_power, axis=1, keepdims=True)
+    scale = top / sum(powers)
+    lane = lax.broadcasted_iota(jnp.int32, (seqs, EXTRA), 1)
+    half = EXTRA // 2
+    spread = jnp.zeros((seqs, EXTRA), jnp.float32)
+    for one, power in zip(member, powers):
+        spread = jnp.where(jnp.bitwise_and(lane, half - 1) == one, power * scale, spread)
+    high = spread.astype(jnp.bfloat16).astype(jnp.float32)
+    extra = jnp.where(lane < half, high, spread - high).astype(jnp.bfloat16)
+    before = lax.broadcasted_iota(jnp.int32, (seqs, seqs), 0)
+    before = before > lax.broadcasted_iota(jnp.int32, (seqs, seqs), 1)
+    hot = in_group.astype(jnp.float32)
+    earlier = jnp.dot(
+        before.astype(jnp.bfloat16), hot.astype(jnp.bfloat16), preferred_element_type=jnp.float32
+    )
+    rank = jnp.sum(earlier * hot, axis=1, keepdims=True).astype(jnp.int32)
+    slot = group * GROUP_SIZE + rank
+    slots = outgoing.shape[0]
+    puts = (lax.broadcasted_iota(jnp.int32, (seqs, slots), 1) == slot).astype(jnp.bfloat16)
+    placing[...] = puts
+
+    def placed(value):
+        out = lax.dot_general(
+            puts, value, (((0,), (0,)), ((), ())), preferred_element_type=jnp.float32
+        )
+        return out.astype(jnp.bfloat16)
+
+    outgoing[:, :width] = placed(hidden)
+    outgoing[:, width:] = placed(extra)
+    own = mid_own.shape[1]
+    low = lax.broadcasted_iota(jnp.int32, (1, 1), 0) + place[0]
+    kept = jnp.zeros(mid_own.shape, jnp.float32)
+    for n in range(width // own):
+        kept = jnp.where(low == n, values[:, n * own : (n + 1) * own], kept)
+    mid_own[...] = kept.astype(jnp.bfloat16)
+
+
+def expert_kernel(count, place, *refs):
     pieces = refs[:count]
-    gate_w, up_w, down_w = refs[count : count + 3]
-    blocks = refs[count + 3 : count + 3 + steps]
-    sent = refs[count + 3 + steps]
+    gate_w, up_w, down_w, kept, sent = refs[count:]
     width = gate_w.shape[0]
     rows = jnp.concatenate([piece[:, :width] for piece in pieces], axis=0)
     extra = jnp.concatenate([piece[:, width:] for piece in pieces], axis=0).astype(jnp.float32)
-    lane = lax.broadcasted_iota(jnp.int32, extra.shape, 1) % (EXTRA // 2)
-    weight = jnp.sum(jnp.where(lane == place[1], extra, 0.0), axis=1, keepdims=True)
+    lane = lax.broadcasted_iota(jnp.int32, extra.shape, 1)
+    mine = jnp.bitwise_and(lane, EXTRA // 2 - 1) == place[1]
+    weight = jnp.sum(jnp.where(mine, extra, 0.0), axis=1, keepdims=True)
     gate = jnp.dot(rows, gate_w[...], preferred_element_type=jnp.float32)
     upward = jnp.dot(rows, up_w[...], preferred_element_type=jnp.float32)
     active = (gate / (1.0 + jnp.exp(-gate)) * upward).astype(jnp.bfloat16)
-    own = blocks[0].shape[0]
-    block = blocks[0].shape[1]
+    part = jnp.dot(active, down_w[...], preferred_element_type=jnp.float32) * weight
+    own = kept.shape[0]
+    kept[...] = part[:own].astype(jnp.bfloat16)
+    sent[...] = part[own:].astype(jnp.bfloat16)
+
+
+def experts(place, ours, theirs, weights):
+    width = weights[2].shape[1]
+    rows = sum(piece.shape[0] for piece in ours)
+    out = ((rows, width), jnp.bfloat16)
+    count = len(ours) + len(theirs)
+    flops = 2 * 2 * rows * 3 * width * weights[0].shape[1]
+    kernel = functools.partial(expert_kernel, count)
+    return call(kernel, [out, out], [place, *ours, *theirs, *weights], flops)
+
+
+def add_kernel(kept, arrived, *outs):
+    rows = outs[0].shape[0]
+    for n, out in enumerate(outs):
+        part = slice(n * rows, (n + 1) * rows)
+        total = kept[part].astype(jnp.float32) + arrived[part].astype(jnp.float32)
+        out[...] = total.astype(jnp.bfloat16)
+
+
+def block_kernel(count, place, *refs):
+    parts, outs = refs[:count], refs[count:]
+    steps, block = len(outs), outs[0].shape[1]
     for step in range(steps):
         start = pl.multiple_of(lax.rem(place[0] + step, steps) * block, block)
-        down = down_w[:, pl.ds(start, block)]
-        part = jnp.dot(active, down, preferred_element_type=jnp.float32) * weight
-        part = part.astype(jnp.bfloat16)
-        blocks[step][...] = part[:own]
-        sent[step] = part[own:]
-
-
-def experts(place, ours, theirs, weights, steps):
-    width = weights[2].shape[1]
-    rows = sum(piece.shape[0] for piece in ours)
-    block = width // steps
-    vmem = pl.BlockSpec(memory_space=pltpu.VMEM)
-    out = pl.pallas_call(
-        functools.partial(expert_kernel, len(ours) + len(theirs), steps),
-        out_shape=[pltpu.VMEM((rows, block), jnp.bfloat16)] * steps
-        + [pltpu.VMEM((steps, rows, block), jnp.bfloat16)],
-        in_specs=[pl.BlockSpec(memory_space=pltpu.SMEM)]
-        + [vmem] * (len(ours) + len(theirs) + 3),
-        out_specs=[vmem] * (steps + 1),
-        compiler_params=pltpu.CompilerParams(vmem_limit_bytes=16 << 20),
-        cost_estimate=pl.CostEstimate(
-            flops=2 * 2 * rows * 3 * width * weights[0].shape[1],
-            transcendentals=2 * rows * weights[0].shape[1],
-            bytes_accessed=0,
-        ),
-        name="experts",
-    )(place, *ours, *theirs, *weights)
-    return out[:steps], out[steps]
-
-
-def add_kernel(steps, *refs):
-    blocks, arrived, outs = refs[:steps], refs[steps], refs[steps + 1 :]
-    for step in range(steps):
-        total = blocks[step][...].astype(jnp.float32) + arrived[step].astype(jnp.float32)
+        part = pl.ds(start, block)
+        total = sum(one[:, part].astype(jnp.float32) for one in parts)
         outs[step][...] = total.astype(jnp.bfloat16)
 
 
-def add_blocks(blocks, arrived):
-    steps = len(blocks)
-    vmem = pl.BlockSpec(memory_space=pltpu.VMEM)
-    return pl.pallas_call(
-        functools.partial(add_kernel, steps),
-        out_shape=[pltpu.VMEM(blocks[0].shape, jnp.bfloat16)] * steps,
-        in_specs=[vmem] * (steps + 1),
-        out_specs=[vmem] * steps,
-        compiler_params=pltpu.CompilerParams(vmem_limit_bytes=4 << 20),
-        name="add_blocks",
-    )(*blocks, arrived)
-
-
-def f32(value):
-    return value.astype(jnp.float32)
+def sum_kernel(*refs):
+    refs[-1][...] = sum(one[...].astype(jnp.float32) for one in refs[:-1]).astype(jnp.bfloat16)
+
+
+def last_kernel(mid_own, placing, returned, out):
+    moe = jnp.dot(placing[...], returned[...], preferred_element_type=jnp.float32)
+    out[...] = (mid_own[...].astype(jnp.float32) + moe).astype(jnp.bfloat16)
 
 
 def per_device(
@@ -277,8 +329,9 @@
     tp = lax.axis_index("tp")
     me = lax.axis_index("ep")
     own_width = width // n_tp
-    expert_count = w_expert.shape[1]
-    group_count = w_group.shape[1]
+    slots = w_group.shape[1] * GROUP_SIZE
+    place = jnp.stack([tp, me % GROUP_SIZE]).astype(jnp.int32)
+    weights = (expert_gate[0], expert_up[0], expert_down[0])
 
     head_part = attention(
         residual,
@@ -290,76 +343,72 @@
         key_cache.reshape(key_cache.shape[0], key_cache.shape[1], key_cache.shape[3]),
         value_cache.reshape(value_cache.shape[0], value_cache.shape[1], value_cache.shape[3]),
     )
-    head_sum = f32(head_part)
-    for part in [tp_shift(head_part, step) for step in range(1, n_tp)]:
-        head_sum = head_sum + f32(part)
-    mid = (f32(residual) + f32(head_sum.astype(bf16))).astype(bf16)
-    mid_own = lax.dynamic_slice_in_dim(mid, tp * own_width, own_width, 1)
-    hidden_in = rms_scale(mid, moe_gain)
-
-    group_prob = jax.nn.softmax(
-        jnp.dot(hidden_in, w_group, preferred_element_type=jnp.float32), axis=-1
-    )
-    expert_logit = jnp.dot(hidden_in, w_expert, preferred_element_type=jnp.float32)
-    expert_ids = jnp.arange(expert_count, dtype=jnp.int32)
-    chosen = routes[:, :, None] == expert_ids[None, None, :]
-    picked = jnp.sum(jnp.where(chosen, expert_logit[:, None, :], 0.0), axis=2)
-    group = routes[:, :1] // GROUP_SIZE
-    group_hot = group == jnp.arange(group_count, dtype=jnp.int32)[None, :]
-    top_prob = jnp.sum(jnp.where(group_hot, group_prob, 0.0), axis=1, keepdims=True)
-    share = jax.nn.softmax(picked, axis=1) * top_prob
-    member = routes % GROUP_SIZE
-    lanes = jnp.arange(EXTRA // 2, dtype=jnp.int32)
-    spread = jnp.sum(
-        jnp.where(member[:, :, None] == lanes[None, None, :], share[:, :, None], 0.0), axis=1
-    )
-    high, low = split_bf16(spread, 2)
-
-    group_row = group[:, 0]
-    order = jnp.arange(seq_count, dtype=jnp.int32)
-    same = (group_row[:, None] == group_row[None, :]) & (order[None, :] < order[:, None])
-    slot = group_row * GROUP_SIZE + jnp.sum(same.astype(jnp.int32), axis=1)
-    slots = group_count * GROUP_SIZE
-    placing = (jnp.arange(slots, dtype=jnp.int32)[:, None] == slot[None, :]).astype(bf16)
-    extended = jnp.concatenate([hidden_in, high, low], axis=1)
-    outgoing = jnp.dot(placing, extended, preferred_element_type=jnp.float32).astype(bf16)
+    head_parts = [head_part]
+    for step in (1, 3, 2):
+        head_parts.append(tp_shift(head_part, step))
+    outgoing, mid_own, placing = call(
+        functools.partial(route_kernel, n_tp),
+        [
+            ((slots, width + EXTRA), bf16),
+            ((seq_count, own_width), bf16),
+            ((seq_count, slots), bf16),
+        ],
+        [
+            place,
+            *head_parts,
+            residual,
+            moe_gain.reshape(1, width),
+            w_group.T,
+            w_expert.T,
+            routes,
+        ],
+    )
     arrived = z_exchange(outgoing.reshape(NZ, GROUP_SIZE, width + EXTRA))
     arrived = arrived.reshape(slots, width + EXTRA)
-
-    half = slots // 2
-    place = jnp.stack([tp, me % GROUP_SIZE]).astype(jnp.int32)
-    weights = (expert_gate[0], expert_up[0], expert_down[0])
 
     def chunk(pieces):
         theirs = []
         for piece in pieces:
             theirs.append(core_swap(piece))
-        blocks, sent = experts(place, pieces, theirs, weights, n_tp)
-        sent = core_swap(sent)
-        blocks = add_blocks(blocks, sent)
-        total = f32(blocks[0])
-        for step in range(1, n_tp):
-            part = tp_shift(blocks[step], step)
-            total = total + f32(part)
-        return total.astype(bf16)
-
+        kept, sent = experts(place, pieces, theirs, weights)
+        return kept, core_swap(sent)
+
+    def added(pair, count):
+        rows = pair[0].shape[0] // count
+        return call(add_kernel, [((rows, width), bf16)] * count, list(pair), vmem=8)
+
+    half = slots // 2
     left = x_shift(arrived, 1)
     right = x_shift(arrived, -1)
     near = chunk([arrived])
     relay0 = x_shift(left[:half], 1)
     relay1 = x_shift(right[half:], -1)
-    sides = chunk([left, right])
-    far = chunk([relay0, relay1])
-    back0 = x_shift(sides[:slots], -1)
-    back1 = x_shift(sides[slots:], 1)
-    back2 = x_shift(far, 2)
-    back = f32(near) + f32(back0) + f32(back1) + f32(back2)
-    returned = z_exchange(back.astype(bf16).reshape(NZ, GROUP_SIZE, own_width))
-    returned = returned.reshape(slots, own_width)
-    moe = lax.dot_general(
-        placing, returned, (((0,), (0,)), ((), ())), preferred_element_type=jnp.float32
-    )
-    return (f32(mid_own) + moe).astype(bf16)
+    to_left, to_right = added(chunk([left, right]), 2)
+    back0 = x_shift(to_left, -1)
+    back1 = x_shift(to_right, 1)
+    (to_far,) = added(chunk([relay0, relay1]), 1)
+    back2 = x_shift(to_far, 2)
+    parts = [*near, back0, back1, back2]
+    blocks = call(
+        functools.partial(block_kernel, len(parts)),
+        [((slots, own_width), bf16)] * n_tp,
+        [place, *parts],
+        vmem=8,
+    )
+    summed = [blocks[0]]
+    for step in (1, 3, 2):
+        summed.append(tp_shift(blocks[step], step))
+    (total,) = call(sum_kernel, [((slots, own_width), bf16)], summed, vmem=4)
+    returned = z_exchange(total.reshape(NZ, GROUP_SIZE, own_width)).reshape(slots, own_width)
+    vmem = pl.BlockSpec(memory_space=pltpu.VMEM)
+    return pl.pallas_call(
+        last_kernel,
+        out_shape=jax.ShapeDtypeStruct((seq_count, own_width), bf16),
+        in_specs=[vmem] * 3,
+        out_specs=vmem,
+        compiler_params=pltpu.CompilerParams(vmem_limit_bytes=4 << 20),
+        name="last",
+    )(mid_own, placing, returned)
 
 
 def solution(mesh):

time: 109 us -> 101 us (0.927)
  the two profiles are of different devices: /device:TPU:8 before, /device:TPU:6 now
where the time goes in v1:
time: 101 us; the launch traced here: 100 us
  waiting for transfers between devices  32 us (32%)
  blocking collectives  30.8 us (30%)
  starting transfers between devices  18.4 us (18%)
  Pallas kernels  15.9 us (16%)
  local copies, waits for them, and re-layouts  3.2 us (3%)
    all_to_all x2, blocking collectives, z_exchange(): lax.all_to_all(value, 'ep', split_axis=0, concat_axis=0, axis_index_group...  30.8 us
    ppermute x7, waiting for transfers between devices, x_shift(): return lax.ppermute(value, 'ep', perm)  20.9 us
    ppermute x6, waiting for transfers between devices, tp_shift(): return lax.ppermute(value, 'tp', [(i, (i + step) % n) for i in range(n)])  10.3 us
    ppermute x6, starting transfers between devices, tp_shift(): return lax.ppermute(value, 'tp', [(i, (i + step) % n) for i in range(n)])  8.61 us
    ppermute x7, starting transfers between devices, x_shift(): return lax.ppermute(value, 'ep', perm)  8.5 us
    pallas_call x1, Pallas kernels, attention(): pl.pallas_call(attn_kernel, out_shape=pltpu.VMEM((seqs, w_out.shape[1]),...  8.19 us
    pallas_call x8, Pallas kernels, call(): pl.pallas_call(kernel, out_shape=[pltpu.VMEM(shape, dtype) for shape, dty...  6.94 us
    unnamed x15, local copies, waits for them, and re-layouts  3.18 us
  transfers between devices with their start and end apart: 21, of which 12 were waited for; matrix products, arithmetic and copies ran while one was open for 1% of the time, Pallas kernels for 4%

profile of v1, /device:TPU:6, one launch (start us, length us, event | category | flops | bytes accessed | tf_op | source)
XLA Modules:
  0.0 100.5 jit_solution(15901269918477102810)
XLA Ops:
  0.0 8.2 %attend.1.refs_0_ = bf16[32,2048]{1,0:T(8,128)(2,1)S(1)} custom-call(s32[32]{0:T(128)} %lengths.1, f32[4]{0:T(128)} %bias.1, bf16[32,2048]{1,0:T(8,128)(2,1)} %refs_4_.1, f32[1,2048]{1,0:T(1,128)} %bitcast.36, bf16[2048,512]{1,0:T(8,128)(2,1)} %wq_hbm.1, bf16[32,512,128]{2,1,0:T(8,128)(2,1)} %bitcast.34, bf16[32,512,128]{2,1,0:T(8,128)(2,1)} %bitcast.35, ...), custom_call_target="tpu_custom_call" | custom-call | tf_op jit(solution)/shard_map/attend/pallas_call | solution.py:150
  8.2 1.7 %collective-permute-start = (bf16[32,2048]{1,0:T(8,128)(2,1)S(1)}, bf16[32,2048]{1,0:T(8,128)(2,1)S(1)}, u32[]{:S(2)}, u32[]{:S(2)}) collective-permute-start(bf16[32,2048]{1,0:T(8,128)(2,1)S(1)} %attend.1.refs_0_), channel_id=1, source_target_pairs={{0,1},{1,2},{2,3},{3,0},{4,5},{5,6},{6,7},{7,4},{8,9},{9,10},{10,1... | collective-permute-start | bytes 393224 | tf_op jit(solution)/shard_map/ppermute | solution.py:44
  9.9 1.7 %collective-permute-start.1 = (bf16[32,2048]{1,0:T(8,128)(2,1)S(1)}, bf16[32,2048]{1,0:T(8,128)(2,1)}, u32[]{:S(2)}, u32[]{:S(2)}) collective-permute-start(bf16[32,2048]{1,0:T(8,128)(2,1)S(1)} %attend.1.refs_0_), channel_id=1, source_target_pairs={{0,3},{1,0},{2,1},{3,2},{4,7},{5,4},{6,5},{7,6},{8,11},{9,8},{10,9... | collective-permute-start | bytes 393224 | tf_op jit(solution)/shard_map/ppermute | solution.py:44
  11.5 2.0 %collective-permute-start.2 = (bf16[32,2048]{1,0:T(8,128)(2,1)S(1)}, bf16[32,2048]{1,0:T(8,128)(2,1)}, u32[]{:S(2)}, u32[]{:S(2)}) collective-permute-start(bf16[32,2048]{1,0:T(8,128)(2,1)S(1)} %attend.1.refs_0_), channel_id=1, source_target_pairs={{0,2},{1,3},{2,0},{3,1},{4,6},{5,7},{6,4},{7,5},{8,10},{9,11},{10,... | collective-permute-start | bytes 393224 | tf_op jit(solution)/shard_map/ppermute | solution.py:44
  13.5 0.8 copy.16.refs_8_
  14.8 2.2 %collective-permute-done.1.refs_2_ = bf16[32,2048]{1,0:T(8,128)(2,1)} collective-permute-done((bf16[32,2048]{1,0:T(8,128)(2,1)S(1)}, bf16[32,2048]{1,0:T(8,128)(2,1)}, u32[]{:S(2)}, u32[]{:S(2)}) %collective-permute-start.1) | collective-permute-done | bytes 131104 | tf_op jit(solution)/shard_map/ppermute | solution.py:44
  17.0 1.9 %collective-permute-done.2.refs_3_ = bf16[32,2048]{1,0:T(8,128)(2,1)} collective-permute-done((bf16[32,2048]{1,0:T(8,128)(2,1)S(1)}, bf16[32,2048]{1,0:T(8,128)(2,1)}, u32[]{:S(2)}, u32[]{:S(2)}) %collective-permute-start.2) | collective-permute-done | bytes 131104 | tf_op jit(solution)/shard_map/ppermute | solution.py:44
  18.9 0.9 copy-done.4
  19.9 0.8 copy-done.5
  20.6 0.7 copy-done.6
  21.3 1.8 %shard_map.145 = (bf16[64,2176]{1,0:T(8,128)(2,1)S(1)}, bf16[32,512]{1,0:T(8,128)(2,1)S(1)}, bf16[32,64]{1,0:T(8,128)(2,1)S(1)}) custom-call(s32[2]{0:T(128)S(1)} %pad_add_fusion.place, bf16[32,2048]{1,0:T(8,128)(2,1)S(1)} %attend.1.refs_0_, bf16[32,2048]{1,0:T(8,128)(2,1)S(1)} %collective-permute-done.refs_1_, ...), custom_call_target="tpu_custom_call" | custom-call | tf_op jit(solution)/shard_map/pallas_call | solution.py:175
  23.1 19.8 %all_to_all.10 = bf16[8,8,2176]{2,1,0:T(8,128)(2,1)S(1)} all-to-all(bf16[8,8,2176]{2,1,0:T(8,128)(2,1)S(1)} %bitcast.28), channel_id=1, replica_groups={{0,32,64,96,128,160,192,224},{4,36,68,100,132,164,196,228},{8,40,72,104..., dimensions={0} | all-to-all | bytes 557056 | tf_op jit(solution)/shard_map/all_to_all | solution.py:49
  43.5 1.5 %collective-permute-start.6 = (bf16[64,2176]{1,0:T(8,128)(2,1)S(1)}, bf16[64,2176]{1,0:T(8,128)(2,1)S(1)}, u32[]{:S(2)}, u32[]{:S(2)}) collective-permute-start(bf16[64,2176]{1,0:T(8,128)(2,1)S(1)} %bitcast.25), channel_id=1, source_target_pairs={{0,24},{4,28},{8,0},{12,4},{16,8},{20,12},{24,16},{28,20},{32,56},... | collective-permute-start | bytes 835592 | tf_op jit(solution)/shard_map/ppermute | solution.py:34
  45.0 4.5 %collective-permute-done.5.refs_0_ = bf16[64,2176]{1,0:T(8,128)(2,1)S(1)} collective-permute-done((bf16[64,2176]{1,0:T(8,128)(2,1)S(1)}, bf16[64,2176]{1,0:T(8,128)(2,1)S(1)}, u32[]{:S(2)}, u32[]{:S(2)}) %collective-permute-start.5) | collective-permute-done | bytes 278560 | tf_op jit(solution)/shard_map/ppermute | solution.py:34
  49.5 1.7 %collective-permute-done.6.refs_1_ = bf16[64,2176]{1,0:T(8,128)(2,1)S(1)} collective-permute-done((bf16[64,2176]{1,0:T(8,128)(2,1)S(1)}, bf16[64,2176]{1,0:T(8,128)(2,1)S(1)}, u32[]{:S(2)}, u32[]{:S(2)}) %collective-permute-start.6) | collective-permute-done | bytes 278560 | tf_op jit(solution)/shard_map/ppermute | solution.py:34
  51.8 1.6 %collective-permute-start.13 = (bf16[32,2176]{1,0:T(8,128)(2,1)S(1)}, bf16[32,2176]{1,0:T(8,128)(2,1)S(1)}, u32[]{:S(2)}, u32[]{:S(2)}) collective-permute-start(bf16[32,2176]{1,0:T(8,128)(2,1)S(1)} %slice.9), channel_id=1, source_target_pairs={{0,24},{4,28},{8,0},{12,4},{16,8},{20,12},{24,16},{28,20},{32,56},... | collective-permute-start | bytes 417800 | tf_op jit(solution)/shard_map/ppermute | solution.py:34
  53.5 1.6 %shard_map.147 = (bf16[128,2048]{1,0:T(8,128)(2,1)S(1)}, bf16[128,2048]{1,0:T(8,128)(2,1)S(1)}) custom-call(s32[2]{0:T(128)S(1)} %pad_add_fusion.place, bf16[64,2176]{1,0:T(8,128)(2,1)S(1)} %collective-permute-done.5.refs_0_, bf16[64,2176]{1,0:T(8,128)(2,1)S(1)} %collective-permute-done.6.refs_1_, bf16[64,2176]{1,0:T(8,128)(2,1)S(1)} %collective-permute-done.7.refs_2_, ...), custom_call_target="tpu_custom_call" | custom-call | flops 805306368 | tf_op jit(solution)/shard_map/pallas_call | solution.py:175
  55.2 2.2 %collective-permute-done.12.refs_0_ = bf16[32,2176]{1,0:T(8,128)(2,1)S(1)} collective-permute-done((bf16[32,2176]{1,0:T(8,128)(2,1)S(1)}, bf16[32,2176]{1,0:T(8,128)(2,1)S(1)}, u32[]{:S(2)}, u32[]{:S(2)}) %collective-permute-start.12) | collective-permute-done | bytes 139296 | tf_op jit(solution)/shard_map/ppermute | solution.py:34
  57.4 1.3 %collective-permute-done.13.refs_1_ = bf16[32,2176]{1,0:T(8,128)(2,1)S(1)} collective-permute-done((bf16[32,2176]{1,0:T(8,128)(2,1)S(1)}, bf16[32,2176]{1,0:T(8,128)(2,1)S(1)}, u32[]{:S(2)}, u32[]{:S(2)}) %collective-permute-start.13) | collective-permute-done | bytes 139296 | tf_op jit(solution)/shard_map/ppermute | solution.py:34
  59.2 0.8 collective-permute-done.15.refs_3_
  60.1 1.3 %shard_map.149 = (bf16[64,2048]{1,0:T(8,128)(2,1)S(1)}, bf16[64,2048]{1,0:T(8,128)(2,1)S(1)}) custom-call(s32[2]{0:T(128)S(1)} %pad_add_fusion.place, bf16[32,2176]{1,0:T(8,128)(2,1)S(1)} %collective-permute-done.12.refs_0_, bf16[32,2176]{1,0:T(8,128)(2,1)S(1)} %collective-permute-done.13.refs_1_, bf16[32,2176]{1,0:T(8,128)(2,1)S(1)} %collective-permute-done.14.refs_2_, ...), custom_call_target="tpu_custom_call" | custom-call | flops 402653184 | tf_op jit(solution)/shard_map/pallas_call | solution.py:175
  61.6 1.3 %shard_map.146 = (bf16[64,2048]{1,0:T(8,128)(2,1)S(1)}, bf16[64,2048]{1,0:T(8,128)(2,1)S(1)}) custom-call(s32[2]{0:T(128)S(1)} %pad_add_fusion.place, bf16[64,2176]{1,0:T(8,128)(2,1)S(1)} %bitcast.27, bf16[64,2176]{1,0:T(8,128)(2,1)S(1)} %collective-permute-done.3.refs_1_, bf16[2048,256]{1,0:T(8,128)(2,1)S(1)} %bitcast.17, bf16[2048,256]{1,0:T(8,128)(2,1)S(1)} %bitcast.20, ...), custom_call_target="tpu_custom_call" | custom-call | flops 402653184 | tf_op jit(solution)/shard_map/pallas_call | solution.py:175
  63.4 1.0 collective-permute-start.17
  64.9 2.9 %collective-permute-start.11 = (bf16[64,2048]{1,0:T(8,128)(2,1)S(1)}, bf16[64,2048]{1,0:T(8,128)(2,1)S(1)}, u32[]{:S(2)}, u32[]{:S(2)}) collective-permute-start(bf16[64,2048]{1,0:T(8,128)(2,1)S(1)} %get-tuple-element.28), channel_id=1, source_target_pairs={{0,8},{4,12},{8,16},{12,20},{16,24},{20,28},{24,0},{28,4},{32,40},... | collective-permute-start | bytes 786440 | tf_op jit(solution)/shard_map/ppermute | solution.py:34
  67.8 6.4 %collective-permute-done.17.refs_4_ = bf16[64,2048]{1,0:T(8,128)(2,1)S(1)} collective-permute-done((bf16[64,2048]{1,0:T(8,128)(2,1)S(1)}, bf16[64,2048]{1,0:T(8,128)(2,1)S(1)}, u32[]{:S(2)}, u32[]{:S(2)}) %collective-permute-start.17) | collective-permute-done | bytes 262176 | tf_op jit(solution)/shard_map/ppermute | solution.py:34
  74.2 4.8 %collective-permute-done.10.refs_2_ = bf16[64,2048]{1,0:T(8,128)(2,1)S(1)} collective-permute-done((bf16[64,2048]{1,0:T(8,128)(2,1)S(1)}, bf16[64,2048]{1,0:T(8,128)(2,1)S(1)}, u32[]{:S(2)}, u32[]{:S(2)}) %collective-permute-start.10) | collective-permute-done | bytes 262176 | tf_op jit(solution)/shard_map/ppermute | solution.py:34
  79.0 0.7 shard_map.151
  80.1 2.9 %collective-permute-start.19 = (bf16[64,512]{1,0:T(8,128)(2,1)S(1)}, bf16[64,512]{1,0:T(8,128)(2,1)S(1)}, u32[]{:S(2)}, u32[]{:S(2)}) collective-permute-start(bf16[64,512]{1,0:T(8,128)(2,1)S(1)} %get-tuple-element.33), channel_id=1, source_target_pairs={{0,3},{1,0},{2,1},{3,2},{4,7},{5,4},{6,5},{7,6},{8,11},{9,8},{10,9... | collective-permute-start | bytes 196616 | tf_op jit(solution)/shard_map/ppermute | solution.py:44
  83.0 2.2 %collective-permute-done.18.refs_1_ = bf16[64,512]{1,0:T(8,128)(2,1)S(1)} collective-permute-done((bf16[64,512]{1,0:T(8,128)(2,1)S(1)}, bf16[64,512]{1,0:T(8,128)(2,1)S(1)}, u32[]{:S(2)}, u32[]{:S(2)}) %collective-permute-start.18) | collective-permute-done | bytes 65568 | tf_op jit(solution)/shard_map/ppermute | solution.py:44
  85.2 3.5 %collective-permute-done.20.refs_3_ = bf16[64,512]{1,0:T(8,128)(2,1)S(1)} collective-permute-done((bf16[64,512]{1,0:T(8,128)(2,1)S(1)}, bf16[64,512]{1,0:T(8,128)(2,1)S(1)}, u32[]{:S(2)}, u32[]{:S(2)}) %collective-permute-start.20) | collective-permute-done | bytes 65568 | tf_op jit(solution)/shard_map/ppermute | solution.py:44
  88.8 10.9 %all_to_all.11 = bf16[8,8,512]{2,1,0:T(8,128)(2,1)S(1)} all-to-all(bf16[8,8,512]{2,1,0:T(8,128)(2,1)S(1)} %bitcast.30), channel_id=1, replica_groups={{0,32,64,96,128,160,192,224},{4,36,68,100,132,164,196,228},{8,40,72,104..., dimensions={0} | all-to-all | bytes 131072 | tf_op jit(solution)/shard_map/all_to_all | solution.py:49
  99.7 0.7 last.1
  (40 shorter events, 4.0 us)
Async XLA Ops:
  0.0 18.9 %copy-start.3 = (bf16[32,2048]{1,0:T(8,128)(2,1)S(1)}, bf16[32,2048]{1,0:T(8,128)(2,1)}, u32[]{:S(2)}) copy-start(bf16[32,2048]{1,0:T(8,128)(2,1)} %refs_4_.1) | copy-start | bytes 393220
  0.0 53.4 %copy-start = (bf16[1,2048,256]{2,1,0:T(8,128)(2,1)S(1)}, bf16[1,2048,256]{2,1,0:T(8,128)(2,1)}, u32[]{:S(2)}) copy-start(bf16[1,2048,256]{2,1,0:T(8,128)(2,1)} %param.27) | copy-start | bytes 3145732
  0.0 53.4 %copy-start.1 = (bf16[1,2048,256]{2,1,0:T(8,128)(2,1)S(1)}, bf16[1,2048,256]{2,1,0:T(8,128)(2,1)}, u32[]{:S(2)}) copy-start(bf16[1,2048,256]{2,1,0:T(8,128)(2,1)} %param.28) | copy-start | bytes 3145732
  0.0 53.4 %copy-start.2 = (bf16[1,256,2048]{2,1,0:T(8,128)(2,1)S(1)}, bf16[1,256,2048]{2,1,0:T(8,128)(2,1)}, u32[]{:S(2)}) copy-start(bf16[1,256,2048]{2,1,0:T(8,128)(2,1)} %param.29) | copy-start | bytes 3145732
  8.2 6.6 %collective-permute-start = (bf16[32,2048]{1,0:T(8,128)(2,1)S(1)}, bf16[32,2048]{1,0:T(8,128)(2,1)S(1)}, u32[]{:S(2)}, u32[]{:S(2)}) collective-permute-start(bf16[32,2048]{1,0:T(8,128)(2,1)S(1)} %attend.1.refs_0_), channel_id=1, source_target_pairs={{0,1},{1,2},{2,3},{3,0},{4,5},{5,6},{6,7},{7,4},{8,9},{9,10},{10,1... | collective-permute-start | bytes 393224 | tf_op jit(solution)/shard_map/ppermute | solution.py:44
  9.9 7.1 %collective-permute-start.1 = (bf16[32,2048]{1,0:T(8,128)(2,1)S(1)}, bf16[32,2048]{1,0:T(8,128)(2,1)}, u32[]{:S(2)}, u32[]{:S(2)}) collective-permute-start(bf16[32,2048]{1,0:T(8,128)(2,1)S(1)} %attend.1.refs_0_), channel_id=1, source_target_pairs={{0,3},{1,0},{2,1},{3,2},{4,7},{5,4},{6,5},{7,6},{8,11},{9,8},{10,9... | collective-permute-start | bytes 393224 | tf_op jit(solution)/shard_map/ppermute | solution.py:44
  11.5 7.4 %collective-permute-start.2 = (bf16[32,2048]{1,0:T(8,128)(2,1)S(1)}, bf16[32,2048]{1,0:T(8,128)(2,1)}, u32[]{:S(2)}, u32[]{:S(2)}) collective-permute-start(bf16[32,2048]{1,0:T(8,128)(2,1)S(1)} %attend.1.refs_0_), channel_id=1, source_target_pairs={{0,2},{1,3},{2,0},{3,1},{4,6},{5,7},{6,4},{7,5},{8,10},{9,11},{10,... | collective-permute-start | bytes 393224 | tf_op jit(solution)/shard_map/ppermute | solution.py:44
  18.9 1.0 copy-start.4
  19.9 0.8 copy-start.5
  20.6 0.7 copy-start.6
  43.0 6.5 %collective-permute-start.5 = (bf16[64,2176]{1,0:T(8,128)(2,1)S(1)}, bf16[64,2176]{1,0:T(8,128)(2,1)S(1)}, u32[]{:S(2)}, u32[]{:S(2)}) collective-permute-start(bf16[64,2176]{1,0:T(8,128)(2,1)S(1)} %bitcast.24), channel_id=1, source_target_pairs={{0,8},{4,12},{8,16},{12,20},{16,24},{20,28},{24,0},{28,4},{32,40},... | collective-permute-start | bytes 835592 | tf_op jit(solution)/shard_map/ppermute | solution.py:34
  43.5 7.8 %collective-permute-start.6 = (bf16[64,2176]{1,0:T(8,128)(2,1)S(1)}, bf16[64,2176]{1,0:T(8,128)(2,1)S(1)}, u32[]{:S(2)}, u32[]{:S(2)}) collective-permute-start(bf16[64,2176]{1,0:T(8,128)(2,1)S(1)} %bitcast.25), channel_id=1, source_target_pairs={{0,24},{4,28},{8,0},{12,4},{16,8},{20,12},{24,16},{28,20},{32,56},... | collective-permute-start | bytes 835592 | tf_op jit(solution)/shard_map/ppermute | solution.py:34
  49.5 3.9 %collective-permute-start.7 = (bf16[64,2176]{1,0:T(8,128)(2,1)S(1)}, bf16[64,2176]{1,0:T(8,128)(2,1)S(1)}, u32[]{:S(2)}, u32[]{:S(2)}) collective-permute-start(bf16[64,2176]{1,0:T(8,128)(2,1)S(1)} %collective-permute-done.5.refs_0_), channel_id=1, source_target_pairs={{0,4},{4,0},{8,12},{12,8},{16,20},{20,16},{24,28},{28,24},{32,36},... | collective-permute-start | bytes 835592 | tf_op jit(solution)/shard_map/ppermute | solution.py:39
  51.2 2.2 %collective-permute-start.8 = (bf16[64,2176]{1,0:T(8,128)(2,1)S(1)}, bf16[64,2176]{1,0:T(8,128)(2,1)S(1)}, u32[]{:S(2)}, u32[]{:S(2)}) collective-permute-start(bf16[64,2176]{1,0:T(8,128)(2,1)S(1)} %collective-permute-done.6.refs_1_), channel_id=1, source_target_pairs={{0,4},{4,0},{8,12},{12,8},{16,20},{20,16},{24,28},{28,24},{32,36},... | collective-permute-start | bytes 835592 | tf_op jit(solution)/shard_map/ppermute | solution.py:39
  51.2 6.2 %collective-permute-start.12 = (bf16[32,2176]{1,0:T(8,128)(2,1)S(1)}, bf16[32,2176]{1,0:T(8,128)(2,1)S(1)}, u32[]{:S(2)}, u32[]{:S(2)}) collective-permute-start(bf16[32,2176]{1,0:T(8,128)(2,1)S(1)} %slice.8), channel_id=1, source_target_pairs={{0,8},{4,12},{8,16},{12,20},{16,24},{20,28},{24,0},{28,4},{32,40},... | collective-permute-start | bytes 417800 | tf_op jit(solution)/shard_map/ppermute | solution.py:34
  51.8 6.9 %collective-permute-start.13 = (bf16[32,2176]{1,0:T(8,128)(2,1)S(1)}, bf16[32,2176]{1,0:T(8,128)(2,1)S(1)}, u32[]{:S(2)}, u32[]{:S(2)}) collective-permute-start(bf16[32,2176]{1,0:T(8,128)(2,1)S(1)} %slice.9), channel_id=1, source_target_pairs={{0,24},{4,28},{8,0},{12,4},{16,8},{20,12},{24,16},{28,20},{32,56},... | collective-permute-start | bytes 417800 | tf_op jit(solution)/shard_map/ppermute | solution.py:34
  55.1 9.3 %collective-permute-start.9 = (bf16[128,2048]{1,0:T(8,128)(2,1)S(1)}, bf16[128,2048]{1,0:T(8,128)(2,1)S(1)}, u32[]{:S(2)}, u32[]{:S(2)}) collective-permute-start(bf16[128,2048]{1,0:T(8,128)(2,1)S(1)} %get-tuple-element.26), channel_id=1, source_target_pairs={{0,4},{4,0},{8,12},{12,8},{16,20},{20,16},{24,28},{28,24},{32,36},... | collective-permute-start | bytes 1572872 | tf_op jit(solution)/shard_map/ppermute | solution.py:39
  57.4 1.8 %collective-permute-start.14 = (bf16[32,2176]{1,0:T(8,128)(2,1)S(1)}, bf16[32,2176]{1,0:T(8,128)(2,1)S(1)}, u32[]{:S(2)}, u32[]{:S(2)}) collective-permute-start(bf16[32,2176]{1,0:T(8,128)(2,1)S(1)} %collective-permute-done.12.refs_0_), channel_id=1, source_target_pairs={{0,4},{4,0},{8,12},{12,8},{16,20},{20,16},{24,28},{28,24},{32,36},... | collective-permute-start | bytes 417800 | tf_op jit(solution)/shard_map/ppermute | solution.py:39
  58.7 1.4 %collective-permute-start.15 = (bf16[32,2176]{1,0:T(8,128)(2,1)S(1)}, bf16[32,2176]{1,0:T(8,128)(2,1)S(1)}, u32[]{:S(2)}, u32[]{:S(2)}) collective-permute-start(bf16[32,2176]{1,0:T(8,128)(2,1)S(1)} %collective-permute-done.13.refs_1_), channel_id=1, source_target_pairs={{0,4},{4,0},{8,12},{12,8},{16,20},{20,16},{24,28},{28,24},{32,36},... | collective-permute-start | bytes 417800 | tf_op jit(solution)/shard_map/ppermute | solution.py:39
  58.7 2.9 %collective-permute-start.3 = (bf16[64,2176]{1,0:T(8,128)(2,1)S(1)}, bf16[64,2176]{1,0:T(8,128)(2,1)S(1)}, u32[]{:S(2)}, u32[]{:S(2)}) collective-permute-start(bf16[64,2176]{1,0:T(8,128)(2,1)S(1)} %bitcast.26), channel_id=1, source_target_pairs={{0,4},{4,0},{8,12},{12,8},{16,20},{20,16},{24,28},{28,24},{32,36},... | collective-permute-start | bytes 835592 | tf_op jit(solution)/shard_map/ppermute | solution.py:39
  61.4 2.0 %collective-permute-start.16 = (bf16[64,2048]{1,0:T(8,128)(2,1)S(1)}, bf16[64,2048]{1,0:T(8,128)(2,1)S(1)}, u32[]{:S(2)}, u32[]{:S(2)}) collective-permute-start(bf16[64,2048]{1,0:T(8,128)(2,1)S(1)} %get-tuple-element.30), channel_id=1, source_target_pairs={{0,4},{4,0},{8,12},{12,8},{16,20},{20,16},{24,28},{28,24},{32,36},... | collective-permute-start | bytes 786440 | tf_op jit(solution)/shard_map/ppermute | solution.py:39
  62.9 4.9 %collective-permute-start.4 = (bf16[64,2048]{1,0:T(8,128)(2,1)S(1)}, bf16[64,2048]{1,0:T(8,128)(2,1)S(1)}, u32[]{:S(2)}, u32[]{:S(2)}) collective-permute-start(bf16[64,2048]{1,0:T(8,128)(2,1)S(1)} %get-tuple-element.24), channel_id=1, source_target_pairs={{0,4},{4,0},{8,12},{12,8},{16,20},{20,16},{24,28},{28,24},{32,36},... | collective-permute-start | bytes 786440 | tf_op jit(solution)/shard_map/ppermute | solution.py:39
  63.4 10.8 %collective-permute-start.17 = (bf16[64,2048]{1,0:T(8,128)(2,1)S(1)}, bf16[64,2048]{1,0:T(8,128)(2,1)S(1)}, u32[]{:S(2)}, u32[]{:S(2)}) collective-permute-start(bf16[64,2048]{1,0:T(8,128)(2,1)S(1)} %shard_map.150), channel_id=1, source_target_pairs={{0,16},{4,20},{8,24},{12,28},{16,0},{20,4},{24,8},{28,12},{32,48},... | collective-permute-start | bytes 786440 | tf_op jit(solution)/shard_map/ppermute | solution.py:34
  64.5 14.5 %collective-permute-start.10 = (bf16[64,2048]{1,0:T(8,128)(2,1)S(1)}, bf16[64,2048]{1,0:T(8,128)(2,1)S(1)}, u32[]{:S(2)}, u32[]{:S(2)}) collective-permute-start(bf16[64,2048]{1,0:T(8,128)(2,1)S(1)} %get-tuple-element.27), channel_id=1, source_target_pairs={{0,24},{4,28},{8,0},{12,4},{16,8},{20,12},{24,16},{28,20},{32,56},... | collective-permute-start | bytes 786440 | tf_op jit(solution)/shard_map/ppermute | solution.py:34
  64.9 14.0 %collective-permute-start.11 = (bf16[64,2048]{1,0:T(8,128)(2,1)S(1)}, bf16[64,2048]{1,0:T(8,128)(2,1)S(1)}, u32[]{:S(2)}, u32[]{:S(2)}) collective-permute-start(bf16[64,2048]{1,0:T(8,128)(2,1)S(1)} %get-tuple-element.28), channel_id=1, source_target_pairs={{0,8},{4,12},{8,16},{12,20},{16,24},{20,28},{24,0},{28,4},{32,40},... | collective-permute-start | bytes 786440 | tf_op jit(solution)/shard_map/ppermute | solution.py:34
  79.7 5.6 %collective-permute-start.18 = (bf16[64,512]{1,0:T(8,128)(2,1)S(1)}, bf16[64,512]{1,0:T(8,128)(2,1)S(1)}, u32[]{:S(2)}, u32[]{:S(2)}) collective-permute-start(bf16[64,512]{1,0:T(8,128)(2,1)S(1)} %get-tuple-element.32), channel_id=1, source_target_pairs={{0,1},{1,2},{2,3},{3,0},{4,5},{5,6},{6,7},{7,4},{8,9},{9,10},{10,1... | collective-permute-start | bytes 196616 | tf_op jit(solution)/shard_map/ppermute | solution.py:44
  80.1 5.1 %collective-permute-start.19 = (bf16[64,512]{1,0:T(8,128)(2,1)S(1)}, bf16[64,512]{1,0:T(8,128)(2,1)S(1)}, u32[]{:S(2)}, u32[]{:S(2)}) collective-permute-start(bf16[64,512]{1,0:T(8,128)(2,1)S(1)} %get-tuple-element.33), channel_id=1, source_target_pairs={{0,3},{1,0},{2,1},{3,2},{4,7},{5,4},{6,5},{7,6},{8,11},{9,8},{10,9... | collective-permute-start | bytes 196616 | tf_op jit(solution)/shard_map/ppermute | solution.py:44
  83.0 5.8 %collective-permute-start.20 = (bf16[64,512]{1,0:T(8,128)(2,1)S(1)}, bf16[64,512]{1,0:T(8,128)(2,1)S(1)}, u32[]{:S(2)}, u32[]{:S(2)}) collective-permute-start(bf16[64,512]{1,0:T(8,128)(2,1)S(1)} %get-tuple-element.34), channel_id=1, source_target_pairs={{0,2},{1,3},{2,0},{3,1},{4,6},{5,7},{6,4},{7,5},{8,10},{9,11},{10,... | collective-permute-start | bytes 196616 | tf_op jit(solution)/shard_map/ppermute | solution.py:44

commit v2 on v1

--- a/solution.py
+++ b/solution.py
@@ -60,8 +60,12 @@
     return out
 
 
-def attn_kernel(lengths, bias, residual, gain, wq_hbm, k_hbm, v_hbm, wo_hbm, out,
-                wq, k, v, wo, q_rows, s_rows, o_rows, wq_sem, wo_sem, k_sem, v_sem):
+def attn_kernel(lengths, bias, gain_hbm, wq_hbm, k_hbm, v_hbm, wo_hbm, *refs):
+    small = refs[:4]
+    out, smalls = refs[4], refs[5:9]
+    residual = smalls[0]
+    (gain, wq, k, v, wo, q_rows, s_rows, o_rows, wq_sem, wo_sem, k_sem, v_sem, small_sem,
+     gain_sem) = refs[9:]
     seqs, _ = residual.shape
     cache = k.shape[1]
     heads = q_rows.shape[0] // seqs
@@ -78,8 +82,16 @@
 
     k_copies = [copy(k_hbm, k, k_sem, n) for n in range(groups)]
     v_copies = [copy(v_hbm, v, v_sem, n) for n in range(groups)]
-    for piece in [wq_copy, *k_copies, *v_copies, wo_copy]:
+    small_copies = [
+        pltpu.make_async_copy(src, dst, small_sem.at[n])
+        for n, (src, dst) in enumerate(zip(small, smalls))
+    ]
+    gain_copy = pltpu.make_async_copy(gain_hbm, gain, gain_sem)
+    first = [gain_copy, small_copies[0], wq_copy, *k_copies, *v_copies[:-1]]
+    for piece in [*first, wo_copy, v_copies[-1], *small_copies[1:]]:
         piece.start()
+    gain_copy.wait()
+    small_copies[0].wait()
     x = residual[...].astype(jnp.float32)
     inverse = lax.rsqrt(jnp.mean(x * x, axis=-1, keepdims=True) + EPSILON)
     normed = (x * inverse * gain[...]).astype(jnp.bfloat16)
@@ -136,23 +148,29 @@
     o_head = lax.dot_general(perm, o_rows[...].astype(jnp.bfloat16), (((0,), (0,)), ((), ())),
                              preferred_element_type=jnp.float32).astype(jnp.bfloat16)
     att = jnp.concatenate([o_head[n * seqs:(n + 1) * seqs] for n in range(heads)], axis=1)
+    for piece in small_copies[1:]:
+        piece.wait()
     wo_copy.wait()
     out[...] = jnp.dot(att, wo[...], preferred_element_type=jnp.float32).astype(out.dtype)
 
 
-def attention(residual, gain, w_query, w_out, bias, lengths, keys, values):
+def attention(residual, gain, w_query, w_out, bias, lengths, keys, values, small):
     seqs, width = residual.shape
     heads = bias.shape[0]
     cache, size = keys.shape[1:]
     hbm = pl.BlockSpec(memory_space=pltpu.HBM)
     vmem = pl.BlockSpec(memory_space=pltpu.VMEM)
     smem = pl.BlockSpec(memory_space=pltpu.SMEM)
+    outs = [((seqs, w_out.shape[1]), jnp.bfloat16)] + [(one.shape, one.dtype) for one in small]
+    small = [pltpu.with_memory_space_constraint(one, pltpu.HBM) for one in small]
+    gain = pltpu.with_memory_space_constraint(gain.reshape(1, width), pltpu.HBM)
     return pl.pallas_call(
         attn_kernel,
-        out_shape=pltpu.VMEM((seqs, w_out.shape[1]), jnp.bfloat16),
-        in_specs=[smem, smem, vmem, vmem, hbm, hbm, hbm, hbm],
-        out_specs=vmem,
+        out_shape=[pltpu.VMEM(shape, dtype) for shape, dtype in outs],
+        in_specs=[smem, smem] + [hbm] * (5 + len(small)),
+        out_specs=[vmem] * len(outs),
         scratch_shapes=[
+            pltpu.VMEM((1, width), jnp.float32),
             pltpu.VMEM(w_query.shape, jnp.bfloat16),
             pltpu.VMEM(keys.shape, jnp.bfloat16),
             pltpu.VMEM(values.shape, jnp.bfloat16),
@@ -164,9 +182,11 @@
             pltpu.SemaphoreType.DMA(()),
             pltpu.SemaphoreType.DMA((COPIES,)),
             pltpu.SemaphoreType.DMA((COPIES,)),
+            pltpu.SemaphoreType.DMA((len(small),)),
+            pltpu.SemaphoreType.DMA(()),
         ],
         name="attend",
-    )(lengths, bias, residual, gain.reshape(1, width), w_query, keys, values, w_out)
+    )(lengths, bias, gain, w_query, keys, values, w_out, *small)
 
 
 def call(kernel, outs, args, flops=0, vmem=16):
@@ -182,7 +202,7 @@
     )(*args)
 
 
-def route_kernel(count, place, *refs):
+def route_kernel(count, *refs):
     parts = refs[:count]
     residual, gain, group_w, expert_w, routes, outgoing, mid_own, placing = refs[count:]
     total = sum(part[...].astype(jnp.float32) for part in parts)
@@ -200,7 +220,15 @@
 
     group_logit = logits(group_w)
     expert_logit = logits(expert_w)
-    named = [routes[:, k : k + 1] for k in range(TOPK)]
+    eye = lax.broadcasted_iota(jnp.int32, (TOPK, TOPK), 0)
+    eye = (eye == lax.broadcasted_iota(jnp.int32, (TOPK, TOPK), 1)).astype(jnp.bfloat16)
+    turned = lax.dot_general(
+        routes[...].astype(jnp.float32).astype(jnp.bfloat16),
+        eye,
+        (((0,), (0,)), ((), ())),
+        preferred_element_type=jnp.float32,
+    ).astype(jnp.int32)
+    named = [turned[:, k : k + 1] for k in range(TOPK)]
     group = jnp.right_shift(named[0], 3)
     member = [jnp.bitwise_and(one, GROUP_SIZE - 1) for one in named]
     lane_e = lax.broadcasted_iota(jnp.int32, expert_logit.shape, 1)
@@ -244,21 +272,50 @@
     outgoing[:, :width] = placed(hidden)
     outgoing[:, width:] = placed(extra)
     own = mid_own.shape[1]
-    low = lax.broadcasted_iota(jnp.int32, (1, 1), 0) + place[0]
+    low = lax.broadcasted_iota(jnp.int32, (1, 1), 0) + lax.axis_index("tp")
     kept = jnp.zeros(mid_own.shape, jnp.float32)
     for n in range(width // own):
         kept = jnp.where(low == n, values[:, n * own : (n + 1) * own], kept)
     mid_own[...] = kept.astype(jnp.bfloat16)
 
 
-def expert_kernel(count, place, *refs):
+def fetch_kernel(after, *refs):
+    count = (len(refs) - 1) // 2
+    sem = refs[-1]
+    copies = [
+        pltpu.make_async_copy(src, dst, sem.at[n])
+        for n, (src, dst) in enumerate(zip(refs[:count], refs[count : 2 * count]))
+    ]
+    for piece in copies:
+        piece.start()
+    for piece in copies:
+        piece.wait()
+
+
+def fetched(arrays, after):
+    hbm = pl.BlockSpec(memory_space=pltpu.HBM)
+    vmem = pl.BlockSpec(memory_space=pltpu.VMEM)
+    arrays = [pltpu.with_memory_space_constraint(one, pltpu.HBM) for one in arrays]
+    return pl.pallas_call(
+        fetch_kernel,
+        out_shape=[pltpu.VMEM(one.shape, one.dtype) for one in arrays],
+        in_specs=[vmem] + [hbm] * len(arrays),
+        out_specs=[vmem] * len(arrays),
+        scratch_shapes=[pltpu.SemaphoreType.DMA((len(arrays),))],
+        compiler_params=pltpu.CompilerParams(vmem_limit_bytes=4 << 20),
+        cost_estimate=pl.CostEstimate(flops=1 << 30, transcendentals=0, bytes_accessed=0),
+        name="fetch",
+    )(after, *arrays)
+
+
+def expert_kernel(count, *refs):
     pieces = refs[:count]
     gate_w, up_w, down_w, kept, sent = refs[count:]
     width = gate_w.shape[0]
     rows = jnp.concatenate([piece[:, :width] for piece in pieces], axis=0)
     extra = jnp.concatenate([piece[:, width:] for piece in pieces], axis=0).astype(jnp.float32)
     lane = lax.broadcasted_iota(jnp.int32, extra.shape, 1)
-    mine = jnp.bitwise_and(lane, EXTRA // 2 - 1) == place[1]
+    mine = jnp.bitwise_and(lane, EXTRA // 2 - 1) == lax.rem(lax.axis_index("ep"), GROUP_SIZE)
     weight = jnp.sum(jnp.where(mine, extra, 0.0), axis=1, keepdims=True)
     gate = jnp.dot(rows, gate_w[...], preferred_element_type=jnp.float32)
     upward = jnp.dot(rows, up_w[...], preferred_element_type=jnp.float32)
@@ -269,14 +326,14 @@
     sent[...] = part[own:].astype(jnp.bfloat16)
 
 
-def experts(place, ours, theirs, weights):
+def experts(ours, theirs, weights):
     width = weights[2].shape[1]
     rows = sum(piece.shape[0] for piece in ours)
     out = ((rows, width), jnp.bfloat16)
     count = len(ours) + len(theirs)
     flops = 2 * 2 * rows * 3 * width * weights[0].shape[1]
     kernel = functools.partial(expert_kernel, count)
-    return call(kernel, [out, out], [place, *ours, *theirs, *weights], flops)
+    return call(kernel, [out, out], [*ours, *theirs, *weights], flops)
 
 
 def add_kernel(kept, arrived, *outs):
@@ -287,11 +344,11 @@
         out[...] = total.astype(jnp.bfloat16)
 
 
-def block_kernel(count, place, *refs):
+def block_kernel(count, *refs):
     parts, outs = refs[:count], refs[count:]
     steps, block = len(outs), outs[0].shape[1]
     for step in range(steps):
-        start = pl.multiple_of(lax.rem(place[0] + step, steps) * block, block)
+        start = pl.multiple_of(lax.rem(lax.axis_index("tp") + step, steps) * block, block)
         part = pl.ds(start, block)
         total = sum(one[:, part].astype(jnp.float32) for one in parts)
         outs[step][...] = total.astype(jnp.bfloat16)
@@ -326,14 +383,10 @@
     bf16 = jnp.bfloat16
     seq_count, width = residual.shape
     n_tp = lax.axis_size("tp")
-    tp = lax.axis_index("tp")
-    me = lax.axis_index("ep")
     own_width = width // n_tp
     slots = w_group.shape[1] * GROUP_SIZE
-    place = jnp.stack([tp, me % GROUP_SIZE]).astype(jnp.int32)
-    weights = (expert_gate[0], expert_up[0], expert_down[0])
-
-    head_part = attention(
+
+    head_part, *small = attention(
         residual,
         mix_gain,
         w_query,
@@ -342,10 +395,13 @@
         lengths,
         key_cache.reshape(key_cache.shape[0], key_cache.shape[1], key_cache.shape[3]),
         value_cache.reshape(value_cache.shape[0], value_cache.shape[1], value_cache.shape[3]),
-    )
+        [residual, moe_gain.reshape(1, width), w_group.T, w_expert.T],
+    )
+    weights = fetched((expert_gate[0], expert_up[0], expert_down[0]), head_part)
     head_parts = [head_part]
     for step in (1, 3, 2):
-        head_parts.append(tp_shift(head_part, step))
+        part = tp_shift(head_part, step)
+        head_parts.append(pltpu.with_memory_space_constraint(part, pltpu.VMEM))
     outgoing, mid_own, placing = call(
         functools.partial(route_kernel, n_tp),
         [
@@ -354,13 +410,9 @@
             ((seq_count, slots), bf16),
         ],
         [
-            place,
             *head_parts,
-            residual,
-            moe_gain.reshape(1, width),
-            w_group.T,
-            w_expert.T,
-            routes,
+            *small,
+            routes.T,
         ],
     )
     arrived = z_exchange(outgoing.reshape(NZ, GROUP_SIZE, width + EXTRA))
@@ -370,7 +422,7 @@
         theirs = []
         for piece in pieces:
             theirs.append(core_swap(piece))
-        kept, sent = experts(place, pieces, theirs, weights)
+        kept, sent = experts(pieces, theirs, weights)
         return kept, core_swap(sent)
 
     def added(pair, count):
@@ -386,19 +438,27 @@
     to_left, to_right = added(chunk([left, right]), 2)
     back0 = x_shift(to_left, -1)
     back1 = x_shift(to_right, 1)
-    (to_far,) = added(chunk([relay0, relay1]), 1)
+    far = chunk([relay0, relay1])
+
+    def y_sum(parts):
+        blocks = call(
+            functools.partial(block_kernel, len(parts)),
+            [((slots, own_width), bf16)] * n_tp,
+            list(parts),
+            vmem=8,
+        )
+        summed = [blocks[0]]
+        for step in (1, 3, 2):
+            summed.append(tp_shift(blocks[step], step))
+        return summed
+
+    def total(parts):
+        return call(sum_kernel, [((slots, own_width), bf16)], parts, vmem=4)[0]
+
+    to_far = total(y_sum(far))
+    own = y_sum([*near, back0, back1])
     back2 = x_shift(to_far, 2)
-    parts = [*near, back0, back1, back2]
-    blocks = call(
-        functools.partial(block_kernel, len(parts)),
-        [((slots, own_width), bf16)] * n_tp,
-        [place, *parts],
-        vmem=8,
-    )
-    summed = [blocks[0]]
-    for step in (1, 3, 2):
-        summed.append(tp_shift(blocks[step], step))
-    (total,) = call(sum_kernel, [((slots, own_width), bf16)], summed, vmem=4)
+    total = total([*own, back2])
     returned = z_exchange(total.reshape(NZ, GROUP_SIZE, own_width)).reshape(slots, own_width)
     vmem = pl.BlockSpec(memory_space=pltpu.VMEM)
     return pl.pallas_call(

time: 101 us -> 101 us (level)
  the two profiles are of different devices: /device:TPU:6 before, /device:TPU:2 now
where the time goes in v2:
time: 101 us
  blocking collectives  31.1 us (31%)
  waiting for transfers between devices  30.9 us (31%)
  starting transfers between devices  23.6 us (23%)
  Pallas kernels  15.4 us (15%)
    all_to_all x2, blocking collectives, z_exchange(): lax.all_to_all(value, 'ep', split_axis=0, concat_axis=0, axis_index_group...  31.1 us
    ppermute x9, waiting for transfers between devices, tp_shift(): return lax.ppermute(value, 'tp', [(i, (i + step) % n) for i in range(n)])  19 us
    ppermute x9, starting transfers between devices, tp_shift(): return lax.ppermute(value, 'tp', [(i, (i + step) % n) for i in range(n)])  11.9 us
    ppermute x7, waiting for transfers between devices, x_shift(): return lax.ppermute(value, 'ep', perm)  10.5 us
    ppermute x7, starting transfers between devices, x_shift(): return lax.ppermute(value, 'ep', perm)  10.4 us
    pallas_call x1, Pallas kernels, attention(): pl.pallas_call(attn_kernel, out_shape=[pltpu.VMEM(shape, dtype) for shape...  8.67 us
    pallas_call x9, Pallas kernels, call(): pl.pallas_call(kernel, out_shape=[pltpu.VMEM(shape, dtype) for shape, dty...  4.11 us
  transfers between devices with their start and end apart: 24, of which 14 were waited for; matrix products, arithmetic and copies ran while one was open for 0% of the time, Pallas kernels for 4%

profile of v2, /device:TPU:2, one launch (start us, length us, event | category | flops | bytes accessed | tf_op | source)
XLA Modules:
  0.0 101.2 jit_solution(17966038210367673902)
XLA Ops:
  0.0 8.7 %attend.1 = (bf16[32,2048]{1,0:T(8,128)(2,1)S(1)}, bf16[32,2048]{1,0:T(8,128)(2,1)S(1)}, f32[1,2048]{1,0:T(1,128)S(1)}, bf16[8,2048]{1,0:T(8,128)(2,1)S(1)}, bf16[64,2048]{1,0:T(8,128)(2,1)S(1)}) custom-call(s32[32]{0:T(128)} %lengths.1, f32[4]{0:T(128)} %bias.1, f32[1,2048]{1,0:T(1,128)} %bitcast.26, bf16[2048,512]{1,0:T(8,128)(2,1)} %wq_hbm.1, ...), custom_call_target="tpu_custom_call" | custom-call | tf_op jit(solution)/shard_map/attend/pallas_call | solution.py:167
  8.7 1.7 %collective-permute-start = (bf16[32,2048]{1,0:T(8,128)(2,1)S(1)}, bf16[32,2048]{1,0:T(8,128)(2,1)S(1)}, u32[]{:S(2)}, u32[]{:S(2)}) collective-permute-start(bf16[32,2048]{1,0:T(8,128)(2,1)S(1)} %get-tuple-element.32.refs_0_.after), channel_id=1, source_target_pairs={{0,1},{1,2},{2,3},{3,0},{4,5},{5,6},{6,7},{7,4},{8,9},{9,10},{10,1... | collective-permute-start | bytes 393224 | tf_op jit(solution)/shard_map/ppermute | solution.py:44
  10.3 1.7 %collective-permute-start.1 = (bf16[32,2048]{1,0:T(8,128)(2,1)S(1)}, bf16[32,2048]{1,0:T(8,128)(2,1)S(1)}, u32[]{:S(2)}, u32[]{:S(2)}) collective-permute-start(bf16[32,2048]{1,0:T(8,128)(2,1)S(1)} %get-tuple-element.32.refs_0_.after), channel_id=1, source_target_pairs={{0,3},{1,0},{2,1},{3,2},{4,7},{5,4},{6,5},{7,6},{8,11},{9,8},{10,9... | collective-permute-start | bytes 393224 | tf_op jit(solution)/shard_map/ppermute | solution.py:44
  12.0 2.0 %collective-permute-start.2 = (bf16[32,2048]{1,0:T(8,128)(2,1)S(1)}, bf16[32,2048]{1,0:T(8,128)(2,1)S(1)}, u32[]{:S(2)}, u32[]{:S(2)}) collective-permute-start(bf16[32,2048]{1,0:T(8,128)(2,1)S(1)} %get-tuple-element.32.refs_0_.after), channel_id=1, source_target_pairs={{0,2},{1,3},{2,0},{3,1},{4,6},{5,7},{6,4},{7,5},{8,10},{9,11},{10,... | collective-permute-start | bytes 393224 | tf_op jit(solution)/shard_map/ppermute | solution.py:44
  14.0 1.3 %collective-permute-done.refs_1_ = bf16[32,2048]{1,0:T(8,128)(2,1)S(1)} collective-permute-done((bf16[32,2048]{1,0:T(8,128)(2,1)S(1)}, bf16[32,2048]{1,0:T(8,128)(2,1)S(1)}, u32[]{:S(2)}, u32[]{:S(2)}) %collective-permute-start) | collective-permute-done | bytes 131104 | tf_op jit(solution)/shard_map/ppermute | solution.py:44
  15.3 2.2 %collective-permute-done.1.refs_2_ = bf16[32,2048]{1,0:T(8,128)(2,1)S(1)} collective-permute-done((bf16[32,2048]{1,0:T(8,128)(2,1)S(1)}, bf16[32,2048]{1,0:T(8,128)(2,1)S(1)}, u32[]{:S(2)}, u32[]{:S(2)}) %collective-permute-start.1) | collective-permute-done | bytes 131104 | tf_op jit(solution)/shard_map/ppermute | solution.py:44
  17.5 1.8 %collective-permute-done.2.refs_3_ = bf16[32,2048]{1,0:T(8,128)(2,1)S(1)} collective-permute-done((bf16[32,2048]{1,0:T(8,128)(2,1)S(1)}, bf16[32,2048]{1,0:T(8,128)(2,1)S(1)}, u32[]{:S(2)}, u32[]{:S(2)}) %collective-permute-start.2) | collective-permute-done | bytes 131104 | tf_op jit(solution)/shard_map/ppermute | solution.py:44
  19.3 1.2 %shard_map.145 = (bf16[64,2176]{1,0:T(8,128)(2,1)S(1)}, bf16[32,512]{1,0:T(8,128)(2,1)S(1)}, bf16[32,64]{1,0:T(8,128)(2,1)S(1)}) custom-call(bf16[32,2048]{1,0:T(8,128)(2,1)S(1)} %get-tuple-element.32.refs_0_.after, bf16[32,2048]{1,0:T(8,128)(2,1)S(1)} %collective-permute-done.refs_1_, bf16[32,2048]{1,0:T(8,128)(2,1)S(1)} %collective-permute-done.1.refs_2_, ...), custom_call_target="tpu_custom_call" | custom-call | tf_op jit(solution)/shard_map/pallas_call | solution.py:195
  20.4 19.8 %all_to_all.10 = bf16[8,8,2176]{2,1,0:T(8,128)(2,1)S(1)} all-to-all(bf16[8,8,2176]{2,1,0:T(8,128)(2,1)S(1)} %bitcast.18), channel_id=1, replica_groups={{0,32,64,96,128,160,192,224},{4,36,68,100,132,164,196,228},{8,40,72,104..., dimensions={0} | all-to-all | bytes 557056 | tf_op jit(solution)/shard_map/all_to_all | solution.py:49
  40.3 1.5 %collective-permute-start.5 = (bf16[64,2176]{1,0:T(8,128)(2,1)S(1)}, bf16[64,2176]{1,0:T(8,128)(2,1)S(1)}, u32[]{:S(2)}, u32[]{:S(2)}) collective-permute-start(bf16[64,2176]{1,0:T(8,128)(2,1)S(1)} %bitcast.14), channel_id=1, source_target_pairs={{0,8},{4,12},{8,16},{12,20},{16,24},{20,28},{24,0},{28,4},{32,40},... | collective-permute-start | bytes 835592 | tf_op jit(solution)/shard_map/ppermute | solution.py:34
  42.3 4.5 %collective-permute-done.5.refs_0_ = bf16[64,2176]{1,0:T(8,128)(2,1)S(1)} collective-permute-done((bf16[64,2176]{1,0:T(8,128)(2,1)S(1)}, bf16[64,2176]{1,0:T(8,128)(2,1)S(1)}, u32[]{:S(2)}, u32[]{:S(2)}) %collective-permute-start.5) | collective-permute-done | bytes 278560 | tf_op jit(solution)/shard_map/ppermute | solution.py:34
  46.8 1.5 %collective-permute-done.6.refs_1_ = bf16[64,2176]{1,0:T(8,128)(2,1)S(1)} collective-permute-done((bf16[64,2176]{1,0:T(8,128)(2,1)S(1)}, bf16[64,2176]{1,0:T(8,128)(2,1)S(1)}, u32[]{:S(2)}, u32[]{:S(2)}) %collective-permute-start.6) | collective-permute-done | bytes 278560 | tf_op jit(solution)/shard_map/ppermute | solution.py:34
  48.3 1.9 %fetch.1 = (bf16[2048,256]{1,0:T(8,128)(2,1)S(1)}, bf16[2048,256]{1,0:T(8,128)(2,1)S(1)}, bf16[256,2048]{1,0:T(8,128)(2,1)S(1)}) custom-call(bf16[32,2048]{1,0:T(8,128)(2,1)S(1)} %get-tuple-element.32.refs_0_.after, bf16[2048,256]{1,0:T(8,128)(2,1)} %bitcast.28, bf16[2048,256]{1,0:T(8,128)(2,1)} %bitcast.29, bf16[256,2048]{1,0:T(8,128)(2,1)} %bitcast.30), custom_call_target="tpu_custom_call" | custom-call | flops 1073741824 | tf_op jit(solution)/shard_map/fetch/pallas_call | solution.py:299
  50.2 1.1 %shard_map.147 = (bf16[128,2048]{1,0:T(8,128)(2,1)S(1)}, bf16[128,2048]{1,0:T(8,128)(2,1)S(1)}) custom-call(bf16[64,2176]{1,0:T(8,128)(2,1)S(1)} %collective-permute-done.5.refs_0_, bf16[64,2176]{1,0:T(8,128)(2,1)S(1)} %collective-permute-done.6.refs_1_, bf16[64,2176]{1,0:T(8,128)(2,1)S(1)} %collective-permute-done.7.refs_2_, ...), custom_call_target="tpu_custom_call" | custom-call | flops 805306368 | tf_op jit(solution)/shard_map/pallas_call | solution.py:195
  51.9 1.3 %collective-permute-start.15 = (bf16[32,2176]{1,0:T(8,128)(2,1)S(1)}, bf16[32,2176]{1,0:T(8,128)(2,1)S(1)}, u32[]{:S(2)}, u32[]{:S(2)}) collective-permute-start(bf16[32,2176]{1,0:T(8,128)(2,1)S(1)} %slice.8), channel_id=1, source_target_pairs={{0,8},{4,12},{8,16},{12,20},{16,24},{20,28},{24,0},{28,4},{32,40},... | collective-permute-start | bytes 417800 | tf_op jit(solution)/shard_map/ppermute | solution.py:34
  53.2 0.9 collective-permute-start.16
  54.1 3.5 %collective-permute-done.15.refs_0_ = bf16[32,2176]{1,0:T(8,128)(2,1)S(1)} collective-permute-done((bf16[32,2176]{1,0:T(8,128)(2,1)S(1)}, bf16[32,2176]{1,0:T(8,128)(2,1)S(1)}, u32[]{:S(2)}, u32[]{:S(2)}) %collective-permute-start.15) | collective-permute-done | bytes 139296 | tf_op jit(solution)/shard_map/ppermute | solution.py:34
  57.6 1.0 collective-permute-done.16.refs_1_
  59.0 1.0 %collective-permute-done.18.refs_3_ = bf16[32,2176]{1,0:T(8,128)(2,1)S(1)} collective-permute-done((bf16[32,2176]{1,0:T(8,128)(2,1)S(1)}, bf16[32,2176]{1,0:T(8,128)(2,1)S(1)}, u32[]{:S(2)}, u32[]{:S(2)}) %collective-permute-start.18) | collective-permute-done | bytes 139296 | tf_op jit(solution)/shard_map/ppermute | solution.py:39
  60.0 0.7 shard_map.150
  60.9 0.7 shard_map.146
  62.3 1.2 %collective-permute-start.10 = (bf16[64,2048]{1,0:T(8,128)(2,1)S(1)}, bf16[64,2048]{1,0:T(8,128)(2,1)S(1)}, u32[]{:S(2)}, u32[]{:S(2)}) collective-permute-start(bf16[64,2048]{1,0:T(8,128)(2,1)S(1)} %get-tuple-element.47), channel_id=1, source_target_pairs={{0,24},{4,28},{8,0},{12,4},{16,8},{20,12},{24,16},{28,20},{32,56},... | collective-permute-start | bytes 786440 | tf_op jit(solution)/shard_map/ppermute | solution.py:34
  63.5 0.9 collective-permute-start.11
  64.9 2.9 %collective-permute-start.21 = (bf16[64,512]{1,0:T(8,128)(2,1)S(1)}, bf16[64,512]{1,0:T(8,128)(2,1)S(1)}, u32[]{:S(2)}, u32[]{:S(2)}) collective-permute-start(bf16[64,512]{1,0:T(8,128)(2,1)S(1)} %get-tuple-element.57), channel_id=1, source_target_pairs={{0,3},{1,0},{2,1},{3,2},{4,7},{5,4},{6,5},{7,6},{8,11},{9,8},{10,9... | collective-permute-start | bytes 196616 | tf_op jit(solution)/shard_map/ppermute | solution.py:44
  67.8 2.2 %collective-permute-done.20.refs_1_ = bf16[64,512]{1,0:T(8,128)(2,1)S(1)} collective-permute-done((bf16[64,512]{1,0:T(8,128)(2,1)S(1)}, bf16[64,512]{1,0:T(8,128)(2,1)S(1)}, u32[]{:S(2)}, u32[]{:S(2)}) %collective-permute-start.20) | collective-permute-done | bytes 65568 | tf_op jit(solution)/shard_map/ppermute | solution.py:44
  70.0 5.8 %collective-permute-done.22.refs_3_ = bf16[64,512]{1,0:T(8,128)(2,1)S(1)} collective-permute-done((bf16[64,512]{1,0:T(8,128)(2,1)S(1)}, bf16[64,512]{1,0:T(8,128)(2,1)S(1)}, u32[]{:S(2)}, u32[]{:S(2)}) %collective-permute-start.22) | collective-permute-done | bytes 65568 | tf_op jit(solution)/shard_map/ppermute | solution.py:44
  75.8 4.1 %collective-permute-start.23 = (bf16[64,512]{1,0:T(8,128)(2,1)S(1)}, bf16[64,512]{1,0:T(8,128)(2,1)S(1)}, u32[]{:S(2)}, u32[]{:S(2)}) collective-permute-start(bf16[64,512]{1,0:T(8,128)(2,1)S(1)} %shard_map.152), channel_id=1, source_target_pairs={{0,16},{4,20},{8,24},{12,28},{16,0},{20,4},{24,8},{28,12},{32,48},... | collective-permute-start | bytes 196616 | tf_op jit(solution)/shard_map/ppermute | solution.py:34
  80.2 3.2 %collective-permute-start.13 = (bf16[64,512]{1,0:T(8,128)(2,1)S(1)}, bf16[64,512]{1,0:T(8,128)(2,1)S(1)}, u32[]{:S(2)}, u32[]{:S(2)}) collective-permute-start(bf16[64,512]{1,0:T(8,128)(2,1)S(1)} %get-tuple-element.51), channel_id=1, source_target_pairs={{0,3},{1,0},{2,1},{3,2},{4,7},{5,4},{6,5},{7,6},{8,11},{9,8},{10,9... | collective-permute-start | bytes 196616 | tf_op jit(solution)/shard_map/ppermute | solution.py:44
  83.4 2.3 %collective-permute-done.12.refs_1_ = bf16[64,512]{1,0:T(8,128)(2,1)S(1)} collective-permute-done((bf16[64,512]{1,0:T(8,128)(2,1)S(1)}, bf16[64,512]{1,0:T(8,128)(2,1)S(1)}, u32[]{:S(2)}, u32[]{:S(2)}) %collective-permute-start.12) | collective-permute-done | bytes 65568 | tf_op jit(solution)/shard_map/ppermute | solution.py:44
  85.9 3.3 %collective-permute-done.14.refs_3_ = bf16[64,512]{1,0:T(8,128)(2,1)S(1)} collective-permute-done((bf16[64,512]{1,0:T(8,128)(2,1)S(1)}, bf16[64,512]{1,0:T(8,128)(2,1)S(1)}, u32[]{:S(2)}, u32[]{:S(2)}) %collective-permute-start.14) | collective-permute-done | bytes 65568 | tf_op jit(solution)/shard_map/ppermute | solution.py:44
  89.2 11.2 %all_to_all.11 = bf16[8,8,512]{2,1,0:T(8,128)(2,1)S(1)} all-to-all(bf16[8,8,512]{2,1,0:T(8,128)(2,1)S(1)} %bitcast.20), channel_id=1, replica_groups={{0,32,64,96,128,160,192,224},{4,36,68,100,132,164,196,228},{8,40,72,104..., dimensions={0} | all-to-all | bytes 131072 | tf_op jit(solution)/shard_map/all_to_all | solution.py:49
  100.4 0.7 last.1
  (34 shorter events, 3.4 us)
Async XLA Ops:
  0.0 19.3 %copy-start = (s32[32,4]{0,1:T(4,128)S(1)}, s32[32,4]{0,1:T(4,128)}, u32[]{:S(2)}) copy-start(s32[32,4]{0,1:T(4,128)} %param.16) | copy-start | bytes 1540
  8.7 6.6 %collective-permute-start = (bf16[32,2048]{1,0:T(8,128)(2,1)S(1)}, bf16[32,2048]{1,0:T(8,128)(2,1)S(1)}, u32[]{:S(2)}, u32[]{:S(2)}) collective-permute-start(bf16[32,2048]{1,0:T(8,128)(2,1)S(1)} %get-tuple-element.32.refs_0_.after), channel_id=1, source_target_pairs={{0,1},{1,2},{2,3},{3,0},{4,5},{5,6},{6,7},{7,4},{8,9},{9,10},{10,1... | collective-permute-start | bytes 393224 | tf_op jit(solution)/shard_map/ppermute | solution.py:44
  10.3 7.1 %collective-permute-start.1 = (bf16[32,2048]{1,0:T(8,128)(2,1)S(1)}, bf16[32,2048]{1,0:T(8,128)(2,1)S(1)}, u32[]{:S(2)}, u32[]{:S(2)}) collective-permute-start(bf16[32,2048]{1,0:T(8,128)(2,1)S(1)} %get-tuple-element.32.refs_0_.after), channel_id=1, source_target_pairs={{0,3},{1,0},{2,1},{3,2},{4,7},{5,4},{6,5},{7,6},{8,11},{9,8},{10,9... | collective-permute-start | bytes 393224 | tf_op jit(solution)/shard_map/ppermute | solution.py:44
  12.0 7.3 %collective-permute-start.2 = (bf16[32,2048]{1,0:T(8,128)(2,1)S(1)}, bf16[32,2048]{1,0:T(8,128)(2,1)S(1)}, u32[]{:S(2)}, u32[]{:S(2)}) collective-permute-start(bf16[32,2048]{1,0:T(8,128)(2,1)S(1)} %get-tuple-element.32.refs_0_.after), channel_id=1, source_target_pairs={{0,2},{1,3},{2,0},{3,1},{4,6},{5,7},{6,4},{7,5},{8,10},{9,11},{10,... | collective-permute-start | bytes 393224 | tf_op jit(solution)/shard_map/ppermute | solution.py:44
  40.3 6.5 %collective-permute-start.5 = (bf16[64,2176]{1,0:T(8,128)(2,1)S(1)}, bf16[64,2176]{1,0:T(8,128)(2,1)S(1)}, u32[]{:S(2)}, u32[]{:S(2)}) collective-permute-start(bf16[64,2176]{1,0:T(8,128)(2,1)S(1)} %bitcast.14), channel_id=1, source_target_pairs={{0,8},{4,12},{8,16},{12,20},{16,24},{20,28},{24,0},{28,4},{32,40},... | collective-permute-start | bytes 835592 | tf_op jit(solution)/shard_map/ppermute | solution.py:34
  41.8 6.5 %collective-permute-start.6 = (bf16[64,2176]{1,0:T(8,128)(2,1)S(1)}, bf16[64,2176]{1,0:T(8,128)(2,1)S(1)}, u32[]{:S(2)}, u32[]{:S(2)}) collective-permute-start(bf16[64,2176]{1,0:T(8,128)(2,1)S(1)} %bitcast.15), channel_id=1, source_target_pairs={{0,24},{4,28},{8,0},{12,4},{16,8},{20,12},{24,16},{28,20},{32,56},... | collective-permute-start | bytes 835592 | tf_op jit(solution)/shard_map/ppermute | solution.py:34
  46.8 3.4 %collective-permute-start.7 = (bf16[64,2176]{1,0:T(8,128)(2,1)S(1)}, bf16[64,2176]{1,0:T(8,128)(2,1)S(1)}, u32[]{:S(2)}, u32[]{:S(2)}) collective-permute-start(bf16[64,2176]{1,0:T(8,128)(2,1)S(1)} %collective-permute-done.5.refs_0_), channel_id=1, source_target_pairs={{0,4},{4,0},{8,12},{12,8},{16,20},{20,16},{24,28},{28,24},{32,36},... | collective-permute-start | bytes 835592 | tf_op jit(solution)/shard_map/ppermute | solution.py:39
  48.3 1.9 %collective-permute-start.8 = (bf16[64,2176]{1,0:T(8,128)(2,1)S(1)}, bf16[64,2176]{1,0:T(8,128)(2,1)S(1)}, u32[]{:S(2)}, u32[]{:S(2)}) collective-permute-start(bf16[64,2176]{1,0:T(8,128)(2,1)S(1)} %collective-permute-done.6.refs_1_), channel_id=1, source_target_pairs={{0,4},{4,0},{8,12},{12,8},{16,20},{20,16},{24,28},{28,24},{32,36},... | collective-permute-start | bytes 835592 | tf_op jit(solution)/shard_map/ppermute | solution.py:39
  51.3 10.8 %collective-permute-start.9 = (bf16[128,2048]{1,0:T(8,128)(2,1)S(1)}, bf16[128,2048]{1,0:T(8,128)(2,1)S(1)}, u32[]{:S(2)}, u32[]{:S(2)}) collective-permute-start(bf16[128,2048]{1,0:T(8,128)(2,1)S(1)} %get-tuple-element.46), channel_id=1, source_target_pairs={{0,4},{4,0},{8,12},{12,8},{16,20},{20,16},{24,28},{28,24},{32,36},... | collective-permute-start | bytes 1572872 | tf_op jit(solution)/shard_map/ppermute | solution.py:39
  51.9 5.7 %collective-permute-start.15 = (bf16[32,2176]{1,0:T(8,128)(2,1)S(1)}, bf16[32,2176]{1,0:T(8,128)(2,1)S(1)}, u32[]{:S(2)}, u32[]{:S(2)}) collective-permute-start(bf16[32,2176]{1,0:T(8,128)(2,1)S(1)} %slice.8), channel_id=1, source_target_pairs={{0,8},{4,12},{8,16},{12,20},{16,24},{20,28},{24,0},{28,4},{32,40},... | collective-permute-start | bytes 417800 | tf_op jit(solution)/shard_map/ppermute | solution.py:34
  53.2 5.4 %collective-permute-start.16 = (bf16[32,2176]{1,0:T(8,128)(2,1)S(1)}, bf16[32,2176]{1,0:T(8,128)(2,1)S(1)}, u32[]{:S(2)}, u32[]{:S(2)}) collective-permute-start(bf16[32,2176]{1,0:T(8,128)(2,1)S(1)} %slice.9), channel_id=1, source_target_pairs={{0,24},{4,28},{8,0},{12,4},{16,8},{20,12},{24,16},{28,20},{32,56},... | collective-permute-start | bytes 417800 | tf_op jit(solution)/shard_map/ppermute | solution.py:34
  54.1 6.8 %collective-permute-start.3 = (bf16[64,2176]{1,0:T(8,128)(2,1)S(1)}, bf16[64,2176]{1,0:T(8,128)(2,1)S(1)}, u32[]{:S(2)}, u32[]{:S(2)}) collective-permute-start(bf16[64,2176]{1,0:T(8,128)(2,1)S(1)} %bitcast.16), channel_id=1, source_target_pairs={{0,4},{4,0},{8,12},{12,8},{16,20},{20,16},{24,28},{28,24},{32,36},... | collective-permute-start | bytes 835592 | tf_op jit(solution)/shard_map/ppermute | solution.py:39
  57.6 1.4 %collective-permute-start.17 = (bf16[32,2176]{1,0:T(8,128)(2,1)S(1)}, bf16[32,2176]{1,0:T(8,128)(2,1)S(1)}, u32[]{:S(2)}, u32[]{:S(2)}) collective-permute-start(bf16[32,2176]{1,0:T(8,128)(2,1)S(1)} %collective-permute-done.15.refs_0_), channel_id=1, source_target_pairs={{0,4},{4,0},{8,12},{12,8},{16,20},{20,16},{24,28},{28,24},{32,36},... | collective-permute-start | bytes 417800 | tf_op jit(solution)/shard_map/ppermute | solution.py:39
  58.6 1.4 %collective-permute-start.18 = (bf16[32,2176]{1,0:T(8,128)(2,1)S(1)}, bf16[32,2176]{1,0:T(8,128)(2,1)S(1)}, u32[]{:S(2)}, u32[]{:S(2)}) collective-permute-start(bf16[32,2176]{1,0:T(8,128)(2,1)S(1)} %collective-permute-done.16.refs_1_), channel_id=1, source_target_pairs={{0,4},{4,0},{8,12},{12,8},{16,20},{20,16},{24,28},{28,24},{32,36},... | collective-permute-start | bytes 417800 | tf_op jit(solution)/shard_map/ppermute | solution.py:39
  60.7 3.6 %collective-permute-start.19 = (bf16[64,2048]{1,0:T(8,128)(2,1)S(1)}, bf16[64,2048]{1,0:T(8,128)(2,1)S(1)}, u32[]{:S(2)}, u32[]{:S(2)}) collective-permute-start(bf16[64,2048]{1,0:T(8,128)(2,1)S(1)} %get-tuple-element.54), channel_id=1, source_target_pairs={{0,4},{4,0},{8,12},{12,8},{16,20},{20,16},{24,28},{28,24},{32,36},... | collective-permute-start | bytes 786440 | tf_op jit(solution)/shard_map/ppermute | solution.py:39
  61.7 18.3 %collective-permute-start.4 = (bf16[64,2048]{1,0:T(8,128)(2,1)S(1)}, bf16[64,2048]{1,0:T(8,128)(2,1)S(1)}, u32[]{:S(2)}, u32[]{:S(2)}) collective-permute-start(bf16[64,2048]{1,0:T(8,128)(2,1)S(1)} %get-tuple-element.44), channel_id=1, source_target_pairs={{0,4},{4,0},{8,12},{12,8},{16,20},{20,16},{24,28},{28,24},{32,36},... | collective-permute-start | bytes 786440 | tf_op jit(solution)/shard_map/ppermute | solution.py:39
  62.3 17.7 %collective-permute-start.10 = (bf16[64,2048]{1,0:T(8,128)(2,1)S(1)}, bf16[64,2048]{1,0:T(8,128)(2,1)S(1)}, u32[]{:S(2)}, u32[]{:S(2)}) collective-permute-start(bf16[64,2048]{1,0:T(8,128)(2,1)S(1)} %get-tuple-element.47), channel_id=1, source_target_pairs={{0,24},{4,28},{8,0},{12,4},{16,8},{20,12},{24,16},{28,20},{32,56},... | collective-permute-start | bytes 786440 | tf_op jit(solution)/shard_map/ppermute | solution.py:34
  63.5 16.5 %collective-permute-start.11 = (bf16[64,2048]{1,0:T(8,128)(2,1)S(1)}, bf16[64,2048]{1,0:T(8,128)(2,1)S(1)}, u32[]{:S(2)}, u32[]{:S(2)}) collective-permute-start(bf16[64,2048]{1,0:T(8,128)(2,1)S(1)} %get-tuple-element.48), channel_id=1, source_target_pairs={{0,8},{4,12},{8,16},{12,20},{16,24},{20,28},{24,0},{28,4},{32,40},... | collective-permute-start | bytes 786440 | tf_op jit(solution)/shard_map/ppermute | solution.py:34
  64.4 5.6 %collective-permute-start.20 = (bf16[64,512]{1,0:T(8,128)(2,1)S(1)}, bf16[64,512]{1,0:T(8,128)(2,1)S(1)}, u32[]{:S(2)}, u32[]{:S(2)}) collective-permute-start(bf16[64,512]{1,0:T(8,128)(2,1)S(1)} %get-tuple-element.56), channel_id=1, source_target_pairs={{0,1},{1,2},{2,3},{3,0},{4,5},{5,6},{6,7},{7,4},{8,9},{9,10},{10,1... | collective-permute-start | bytes 196616 | tf_op jit(solution)/shard_map/ppermute | solution.py:44
  64.9 5.1 %collective-permute-start.21 = (bf16[64,512]{1,0:T(8,128)(2,1)S(1)}, bf16[64,512]{1,0:T(8,128)(2,1)S(1)}, u32[]{:S(2)}, u32[]{:S(2)}) collective-permute-start(bf16[64,512]{1,0:T(8,128)(2,1)S(1)} %get-tuple-element.57), channel_id=1, source_target_pairs={{0,3},{1,0},{2,1},{3,2},{4,7},{5,4},{6,5},{7,6},{8,11},{9,8},{10,9... | collective-permute-start | bytes 196616 | tf_op jit(solution)/shard_map/ppermute | solution.py:44
  70.0 5.8 %collective-permute-start.22 = (bf16[64,512]{1,0:T(8,128)(2,1)S(1)}, bf16[64,512]{1,0:T(8,128)(2,1)S(1)}, u32[]{:S(2)}, u32[]{:S(2)}) collective-permute-start(bf16[64,512]{1,0:T(8,128)(2,1)S(1)} %get-tuple-element.58), channel_id=1, source_target_pairs={{0,2},{1,3},{2,0},{3,1},{4,6},{5,7},{6,4},{7,5},{8,10},{9,11},{10,... | collective-permute-start | bytes 196616 | tf_op jit(solution)/shard_map/ppermute | solution.py:44
  75.8 7.6 %collective-permute-start.23 = (bf16[64,512]{1,0:T(8,128)(2,1)S(1)}, bf16[64,512]{1,0:T(8,128)(2,1)S(1)}, u32[]{:S(2)}, u32[]{:S(2)}) collective-permute-start(bf16[64,512]{1,0:T(8,128)(2,1)S(1)} %shard_map.152), channel_id=1, source_target_pairs={{0,16},{4,20},{8,24},{12,28},{16,0},{20,4},{24,8},{28,12},{32,48},... | collective-permute-start | bytes 196616 | tf_op jit(solution)/shard_map/ppermute | solution.py:34
  80.1 5.6 %collective-permute-start.12 = (bf16[64,512]{1,0:T(8,128)(2,1)S(1)}, bf16[64,512]{1,0:T(8,128)(2,1)S(1)}, u32[]{:S(2)}, u32[]{:S(2)}) collective-permute-start(bf16[64,512]{1,0:T(8,128)(2,1)S(1)} %get-tuple-element.50), channel_id=1, source_target_pairs={{0,1},{1,2},{2,3},{3,0},{4,5},{5,6},{6,7},{7,4},{8,9},{9,10},{10,1... | collective-permute-start | bytes 196616 | tf_op jit(solution)/shard_map/ppermute | solution.py:44
  80.2 5.7 %collective-permute-start.13 = (bf16[64,512]{1,0:T(8,128)(2,1)S(1)}, bf16[64,512]{1,0:T(8,128)(2,1)S(1)}, u32[]{:S(2)}, u32[]{:S(2)}) collective-permute-start(bf16[64,512]{1,0:T(8,128)(2,1)S(1)} %get-tuple-element.51), channel_id=1, source_target_pairs={{0,3},{1,0},{2,1},{3,2},{4,7},{5,4},{6,5},{7,6},{8,11},{9,8},{10,9... | collective-permute-start | bytes 196616 | tf_op jit(solution)/shard_map/ppermute | solution.py:44
  83.4 5.8 %collective-permute-start.14 = (bf16[64,512]{1,0:T(8,128)(2,1)S(1)}, bf16[64,512]{1,0:T(8,128)(2,1)S(1)}, u32[]{:S(2)}, u32[]{:S(2)}) collective-permute-start(bf16[64,512]{1,0:T(8,128)(2,1)S(1)} %get-tuple-element.52), channel_id=1, source_target_pairs={{0,2},{1,3},{2,0},{3,1},{4,6},{5,7},{6,4},{7,5},{8,10},{9,11},{10,... | collective-permute-start | bytes 196616 | tf_op jit(solution)/shard_map/ppermute | solution.py:44

commit v3 on v2

--- a/solution.py
+++ b/solution.py
@@ -60,12 +60,12 @@
     return out
 
 
-def attn_kernel(lengths, bias, gain_hbm, wq_hbm, k_hbm, v_hbm, wo_hbm, *refs):
+def attn_kernel(lengths_hbm, bias_hbm, gain_hbm, wq_hbm, k_hbm, v_hbm, wo_hbm, *refs):
     small = refs[:4]
     out, smalls = refs[4], refs[5:9]
     residual = smalls[0]
-    (gain, wq, k, v, wo, q_rows, s_rows, o_rows, wq_sem, wo_sem, k_sem, v_sem, small_sem,
-     gain_sem) = refs[9:]
+    (lengths, bias, gain, wq, k, v, wo, q_rows, s_rows, o_rows, wq_sem, wo_sem, k_sem, v_sem, small_sem,
+     gain_sem, lengths_sem, bias_sem) = refs[9:]
     seqs, _ = residual.shape
     cache = k.shape[1]
     heads = q_rows.shape[0] // seqs
@@ -87,6 +87,10 @@
         for n, (src, dst) in enumerate(zip(small, smalls))
     ]
     gain_copy = pltpu.make_async_copy(gain_hbm, gain, gain_sem)
+    lengths_copy = pltpu.make_async_copy(lengths_hbm, lengths, lengths_sem)
+    bias_copy = pltpu.make_async_copy(bias_hbm, bias, bias_sem)
+    lengths_copy.start()
+    bias_copy.start()
     first = [gain_copy, small_copies[0], wq_copy, *k_copies, *v_copies[:-1]]
     for piece in [*first, wo_copy, v_copies[-1], *small_copies[1:]]:
         piece.start()
@@ -99,6 +103,8 @@
     c = lax.broadcasted_iota(jnp.int32, (rows, rows), 1)
     perm = (c == (r % heads) * seqs + r // heads).astype(jnp.bfloat16)
     row = lax.broadcasted_iota(jnp.int32, (rows, 1), 0)
+    lengths_copy.wait()
+    bias_copy.wait()
     b = jnp.zeros((rows, 1), jnp.float32)
     for n in range(heads):
         b = jnp.where(row % heads == n, bias[n], b)
@@ -160,16 +166,19 @@
     cache, size = keys.shape[1:]
     hbm = pl.BlockSpec(memory_space=pltpu.HBM)
     vmem = pl.BlockSpec(memory_space=pltpu.VMEM)
-    smem = pl.BlockSpec(memory_space=pltpu.SMEM)
     outs = [((seqs, w_out.shape[1]), jnp.bfloat16)] + [(one.shape, one.dtype) for one in small]
     small = [pltpu.with_memory_space_constraint(one, pltpu.HBM) for one in small]
+    lengths = pltpu.with_memory_space_constraint(lengths, pltpu.HBM)
+    bias = pltpu.with_memory_space_constraint(bias, pltpu.HBM)
     gain = pltpu.with_memory_space_constraint(gain.reshape(1, width), pltpu.HBM)
     return pl.pallas_call(
         attn_kernel,
         out_shape=[pltpu.VMEM(shape, dtype) for shape, dtype in outs],
-        in_specs=[smem, smem] + [hbm] * (5 + len(small)),
+        in_specs=[hbm] * (7 + len(small)),
         out_specs=[vmem] * len(outs),
         scratch_shapes=[
+            pltpu.SMEM(lengths.shape, jnp.int32),
+            pltpu.SMEM(bias.shape, jnp.float32),
             pltpu.VMEM((1, width), jnp.float32),
             pltpu.VMEM(w_query.shape, jnp.bfloat16),
             pltpu.VMEM(keys.shape, jnp.bfloat16),
@@ -183,6 +192,8 @@
             pltpu.SemaphoreType.DMA((COPIES,)),
             pltpu.SemaphoreType.DMA((COPIES,)),
             pltpu.SemaphoreType.DMA((len(small),)),
+            pltpu.SemaphoreType.DMA(()),
+            pltpu.SemaphoreType.DMA(()),
             pltpu.SemaphoreType.DMA(()),
         ],
         name="attend",

time: 101 us -> 101 us (level)
  no operation moved by 1% of the time
where the time goes in v3:
time: 101 us; the launch traced here: 100 us
  blocking collectives  31 us (31%)
  waiting for transfers between devices  30.9 us (31%)
  starting transfers between devices  23.7 us (23%)
  Pallas kernels  14.6 us (14%)
    all_to_all x2, blocking collectives, z_exchange(): lax.all_to_all(value, 'ep', split_axis=0, concat_axis=0, axis_index_group...  31 us
    ppermute x9, waiting for transfers between devices, tp_shift(): return lax.ppermute(value, 'tp', [(i, (i + step) % n) for i in range(n)])  19 us
    ppermute x9, starting transfers between devices, tp_shift(): return lax.ppermute(value, 'tp', [(i, (i + step) % n) for i in range(n)])  11.9 us
    ppermute x7, waiting for transfers between devices, x_shift(): return lax.ppermute(value, 'ep', perm)  10.5 us
    ppermute x7, starting transfers between devices, x_shift(): return lax.ppermute(value, 'ep', perm)  10.4 us
    pallas_call x1, Pallas kernels, attention(): pl.pallas_call(attn_kernel, out_shape=[pltpu.VMEM(shape, dtype) for shape...  7.89 us
    pallas_call x9, Pallas kernels, call(): pl.pallas_call(kernel, out_shape=[pltpu.VMEM(shape, dtype) for shape, dty...  4.1 us
  transfers between devices with their start and end apart: 24, of which 14 were waited for; matrix products, arithmetic and copies ran while one was open for 0% of the time, Pallas kernels for 4%

profile of v3, /device:TPU:2, one launch (start us, length us, event | category | flops | bytes accessed | tf_op | source)
XLA Modules:
  0.0 100.4 jit_solution(4704247684565929696)
XLA Ops:
  0.0 7.9 %attend.1 = (bf16[32,2048]{1,0:T(8,128)(2,1)S(1)}, bf16[32,2048]{1,0:T(8,128)(2,1)S(1)}, f32[1,2048]{1,0:T(1,128)S(1)}, bf16[8,2048]{1,0:T(8,128)(2,1)S(1)}, bf16[64,2048]{1,0:T(8,128)(2,1)S(1)}) custom-call(s32[32]{0:T(128)} %lengths_hbm.1, f32[4]{0:T(128)} %bias_hbm.1, f32[1,2048]{1,0:T(1,128)} %bitcast.26, bf16[2048,512]{1,0:T(8,128)(2,1)} %wq_hbm.1, ...), custom_call_target="tpu_custom_call" | custom-call | tf_op jit(solution)/shard_map/attend/pallas_call | solution.py:174
  7.9 1.6 %collective-permute-start = (bf16[32,2048]{1,0:T(8,128)(2,1)S(1)}, bf16[32,2048]{1,0:T(8,128)(2,1)S(1)}, u32[]{:S(2)}, u32[]{:S(2)}) collective-permute-start(bf16[32,2048]{1,0:T(8,128)(2,1)S(1)} %get-tuple-element.32.refs_0_.after), channel_id=1, source_target_pairs={{0,1},{1,2},{2,3},{3,0},{4,5},{5,6},{6,7},{7,4},{8,9},{9,10},{10,1... | collective-permute-start | bytes 393224 | tf_op jit(solution)/shard_map/ppermute | solution.py:44
  9.6 1.7 %collective-permute-start.1 = (bf16[32,2048]{1,0:T(8,128)(2,1)S(1)}, bf16[32,2048]{1,0:T(8,128)(2,1)S(1)}, u32[]{:S(2)}, u32[]{:S(2)}) collective-permute-start(bf16[32,2048]{1,0:T(8,128)(2,1)S(1)} %get-tuple-element.32.refs_0_.after), channel_id=1, source_target_pairs={{0,3},{1,0},{2,1},{3,2},{4,7},{5,4},{6,5},{7,6},{8,11},{9,8},{10,9... | collective-permute-start | bytes 393224 | tf_op jit(solution)/shard_map/ppermute | solution.py:44
  11.2 2.0 %collective-permute-start.2 = (bf16[32,2048]{1,0:T(8,128)(2,1)S(1)}, bf16[32,2048]{1,0:T(8,128)(2,1)S(1)}, u32[]{:S(2)}, u32[]{:S(2)}) collective-permute-start(bf16[32,2048]{1,0:T(8,128)(2,1)S(1)} %get-tuple-element.32.refs_0_.after), channel_id=1, source_target_pairs={{0,2},{1,3},{2,0},{3,1},{4,6},{5,7},{6,4},{7,5},{8,10},{9,11},{10,... | collective-permute-start | bytes 393224 | tf_op jit(solution)/shard_map/ppermute | solution.py:44
  13.2 1.3 %collective-permute-done.refs_1_ = bf16[32,2048]{1,0:T(8,128)(2,1)S(1)} collective-permute-done((bf16[32,2048]{1,0:T(8,128)(2,1)S(1)}, bf16[32,2048]{1,0:T(8,128)(2,1)S(1)}, u32[]{:S(2)}, u32[]{:S(2)}) %collective-permute-start) | collective-permute-done | bytes 131104 | tf_op jit(solution)/shard_map/ppermute | solution.py:44
  14.5 2.2 %collective-permute-done.1.refs_2_ = bf16[32,2048]{1,0:T(8,128)(2,1)S(1)} collective-permute-done((bf16[32,2048]{1,0:T(8,128)(2,1)S(1)}, bf16[32,2048]{1,0:T(8,128)(2,1)S(1)}, u32[]{:S(2)}, u32[]{:S(2)}) %collective-permute-start.1) | collective-permute-done | bytes 131104 | tf_op jit(solution)/shard_map/ppermute | solution.py:44
  16.7 1.8 %collective-permute-done.2.refs_3_ = bf16[32,2048]{1,0:T(8,128)(2,1)S(1)} collective-permute-done((bf16[32,2048]{1,0:T(8,128)(2,1)S(1)}, bf16[32,2048]{1,0:T(8,128)(2,1)S(1)}, u32[]{:S(2)}, u32[]{:S(2)}) %collective-permute-start.2) | collective-permute-done | bytes 131104 | tf_op jit(solution)/shard_map/ppermute | solution.py:44
  18.5 1.2 %shard_map.145 = (bf16[64,2176]{1,0:T(8,128)(2,1)S(1)}, bf16[32,512]{1,0:T(8,128)(2,1)S(1)}, bf16[32,64]{1,0:T(8,128)(2,1)S(1)}) custom-call(bf16[32,2048]{1,0:T(8,128)(2,1)S(1)} %get-tuple-element.32.refs_0_.after, bf16[32,2048]{1,0:T(8,128)(2,1)S(1)} %collective-permute-done.refs_1_, bf16[32,2048]{1,0:T(8,128)(2,1)S(1)} %collective-permute-done.1.refs_2_, ...), custom_call_target="tpu_custom_call" | custom-call | tf_op jit(solution)/shard_map/pallas_call | solution.py:206
  19.6 19.8 %all_to_all.10 = bf16[8,8,2176]{2,1,0:T(8,128)(2,1)S(1)} all-to-all(bf16[8,8,2176]{2,1,0:T(8,128)(2,1)S(1)} %bitcast.18), channel_id=1, replica_groups={{0,32,64,96,128,160,192,224},{4,36,68,100,132,164,196,228},{8,40,72,104..., dimensions={0} | all-to-all | bytes 557056 | tf_op jit(solution)/shard_map/all_to_all | solution.py:49
  39.5 1.5 %collective-permute-start.5 = (bf16[64,2176]{1,0:T(8,128)(2,1)S(1)}, bf16[64,2176]{1,0:T(8,128)(2,1)S(1)}, u32[]{:S(2)}, u32[]{:S(2)}) collective-permute-start(bf16[64,2176]{1,0:T(8,128)(2,1)S(1)} %bitcast.14), channel_id=1, source_target_pairs={{0,8},{4,12},{8,16},{12,20},{16,24},{20,28},{24,0},{28,4},{32,40},... | collective-permute-start | bytes 835592 | tf_op jit(solution)/shard_map/ppermute | solution.py:34
  41.5 4.5 %collective-permute-done.5.refs_0_ = bf16[64,2176]{1,0:T(8,128)(2,1)S(1)} collective-permute-done((bf16[64,2176]{1,0:T(8,128)(2,1)S(1)}, bf16[64,2176]{1,0:T(8,128)(2,1)S(1)}, u32[]{:S(2)}, u32[]{:S(2)}) %collective-permute-start.5) | collective-permute-done | bytes 278560 | tf_op jit(solution)/shard_map/ppermute | solution.py:34
  46.0 1.5 %collective-permute-done.6.refs_1_ = bf16[64,2176]{1,0:T(8,128)(2,1)S(1)} collective-permute-done((bf16[64,2176]{1,0:T(8,128)(2,1)S(1)}, bf16[64,2176]{1,0:T(8,128)(2,1)S(1)}, u32[]{:S(2)}, u32[]{:S(2)}) %collective-permute-start.6) | collective-permute-done | bytes 278560 | tf_op jit(solution)/shard_map/ppermute | solution.py:34
  47.5 1.9 %fetch.1 = (bf16[2048,256]{1,0:T(8,128)(2,1)S(1)}, bf16[2048,256]{1,0:T(8,128)(2,1)S(1)}, bf16[256,2048]{1,0:T(8,128)(2,1)S(1)}) custom-call(bf16[32,2048]{1,0:T(8,128)(2,1)S(1)} %get-tuple-element.32.refs_0_.after, bf16[2048,256]{1,0:T(8,128)(2,1)} %bitcast.28, bf16[2048,256]{1,0:T(8,128)(2,1)} %bitcast.29, bf16[256,2048]{1,0:T(8,128)(2,1)} %bitcast.30), custom_call_target="tpu_custom_call" | custom-call | flops 1073741824 | tf_op jit(solution)/shard_map/fetch/pallas_call | solution.py:310
  49.4 1.1 %shard_map.147 = (bf16[128,2048]{1,0:T(8,128)(2,1)S(1)}, bf16[128,2048]{1,0:T(8,128)(2,1)S(1)}) custom-call(bf16[64,2176]{1,0:T(8,128)(2,1)S(1)} %collective-permute-done.5.refs_0_, bf16[64,2176]{1,0:T(8,128)(2,1)S(1)} %collective-permute-done.6.refs_1_, bf16[64,2176]{1,0:T(8,128)(2,1)S(1)} %collective-permute-done.7.refs_2_, ...), custom_call_target="tpu_custom_call" | custom-call | flops 805306368 | tf_op jit(solution)/shard_map/pallas_call | solution.py:206
  51.1 1.3 %collective-permute-start.15 = (bf16[32,2176]{1,0:T(8,128)(2,1)S(1)}, bf16[32,2176]{1,0:T(8,128)(2,1)S(1)}, u32[]{:S(2)}, u32[]{:S(2)}) collective-permute-start(bf16[32,2176]{1,0:T(8,128)(2,1)S(1)} %slice.8), channel_id=1, source_target_pairs={{0,8},{4,12},{8,16},{12,20},{16,24},{20,28},{24,0},{28,4},{32,40},... | collective-permute-start | bytes 417800 | tf_op jit(solution)/shard_map/ppermute | solution.py:34
  52.4 0.9 collective-permute-start.16
  53.3 3.5 %collective-permute-done.15.refs_0_ = bf16[32,2176]{1,0:T(8,128)(2,1)S(1)} collective-permute-done((bf16[32,2176]{1,0:T(8,128)(2,1)S(1)}, bf16[32,2176]{1,0:T(8,128)(2,1)S(1)}, u32[]{:S(2)}, u32[]{:S(2)}) %collective-permute-start.15) | collective-permute-done | bytes 139296 | tf_op jit(solution)/shard_map/ppermute | solution.py:34
  56.8 1.0 %collective-permute-done.16.refs_1_ = bf16[32,2176]{1,0:T(8,128)(2,1)S(1)} collective-permute-done((bf16[32,2176]{1,0:T(8,128)(2,1)S(1)}, bf16[32,2176]{1,0:T(8,128)(2,1)S(1)}, u32[]{:S(2)}, u32[]{:S(2)}) %collective-permute-start.16) | collective-permute-done | bytes 139296 | tf_op jit(solution)/shard_map/ppermute | solution.py:34
  58.2 1.0 %collective-permute-done.18.refs_3_ = bf16[32,2176]{1,0:T(8,128)(2,1)S(1)} collective-permute-done((bf16[32,2176]{1,0:T(8,128)(2,1)S(1)}, bf16[32,2176]{1,0:T(8,128)(2,1)S(1)}, u32[]{:S(2)}, u32[]{:S(2)}) %collective-permute-start.18) | collective-permute-done | bytes 139296 | tf_op jit(solution)/shard_map/ppermute | solution.py:39
  59.2 0.7 shard_map.150
  60.2 0.7 shard_map.146
  61.5 1.2 %collective-permute-start.10 = (bf16[64,2048]{1,0:T(8,128)(2,1)S(1)}, bf16[64,2048]{1,0:T(8,128)(2,1)S(1)}, u32[]{:S(2)}, u32[]{:S(2)}) collective-permute-start(bf16[64,2048]{1,0:T(8,128)(2,1)S(1)} %get-tuple-element.47), channel_id=1, source_target_pairs={{0,24},{4,28},{8,0},{12,4},{16,8},{20,12},{24,16},{28,20},{32,56},... | collective-permute-start | bytes 786440 | tf_op jit(solution)/shard_map/ppermute | solution.py:34
  62.7 0.9 collective-permute-start.11
  64.1 2.9 %collective-permute-start.21 = (bf16[64,512]{1,0:T(8,128)(2,1)S(1)}, bf16[64,512]{1,0:T(8,128)(2,1)S(1)}, u32[]{:S(2)}, u32[]{:S(2)}) collective-permute-start(bf16[64,512]{1,0:T(8,128)(2,1)S(1)} %get-tuple-element.57), channel_id=1, source_target_pairs={{0,3},{1,0},{2,1},{3,2},{4,7},{5,4},{6,5},{7,6},{8,11},{9,8},{10,9... | collective-permute-start | bytes 196616 | tf_op jit(solution)/shard_map/ppermute | solution.py:44
  66.9 2.2 %collective-permute-done.20.refs_1_ = bf16[64,512]{1,0:T(8,128)(2,1)S(1)} collective-permute-done((bf16[64,512]{1,0:T(8,128)(2,1)S(1)}, bf16[64,512]{1,0:T(8,128)(2,1)S(1)}, u32[]{:S(2)}, u32[]{:S(2)}) %collective-permute-start.20) | collective-permute-done | bytes 65568 | tf_op jit(solution)/shard_map/ppermute | solution.py:44
  69.2 5.8 %collective-permute-done.22.refs_3_ = bf16[64,512]{1,0:T(8,128)(2,1)S(1)} collective-permute-done((bf16[64,512]{1,0:T(8,128)(2,1)S(1)}, bf16[64,512]{1,0:T(8,128)(2,1)S(1)}, u32[]{:S(2)}, u32[]{:S(2)}) %collective-permute-start.22) | collective-permute-done | bytes 65568 | tf_op jit(solution)/shard_map/ppermute | solution.py:44
  75.0 4.1 %collective-permute-start.23 = (bf16[64,512]{1,0:T(8,128)(2,1)S(1)}, bf16[64,512]{1,0:T(8,128)(2,1)S(1)}, u32[]{:S(2)}, u32[]{:S(2)}) collective-permute-start(bf16[64,512]{1,0:T(8,128)(2,1)S(1)} %shard_map.152), channel_id=1, source_target_pairs={{0,16},{4,20},{8,24},{12,28},{16,0},{20,4},{24,8},{28,12},{32,48},... | collective-permute-start | bytes 196616 | tf_op jit(solution)/shard_map/ppermute | solution.py:34
  79.4 3.2 %collective-permute-start.13 = (bf16[64,512]{1,0:T(8,128)(2,1)S(1)}, bf16[64,512]{1,0:T(8,128)(2,1)S(1)}, u32[]{:S(2)}, u32[]{:S(2)}) collective-permute-start(bf16[64,512]{1,0:T(8,128)(2,1)S(1)} %get-tuple-element.51), channel_id=1, source_target_pairs={{0,3},{1,0},{2,1},{3,2},{4,7},{5,4},{6,5},{7,6},{8,11},{9,8},{10,9... | collective-permute-start | bytes 196616 | tf_op jit(solution)/shard_map/ppermute | solution.py:44
  82.6 2.3 %collective-permute-done.12.refs_1_ = bf16[64,512]{1,0:T(8,128)(2,1)S(1)} collective-permute-done((bf16[64,512]{1,0:T(8,128)(2,1)S(1)}, bf16[64,512]{1,0:T(8,128)(2,1)S(1)}, u32[]{:S(2)}, u32[]{:S(2)}) %collective-permute-start.12) | collective-permute-done | bytes 65568 | tf_op jit(solution)/shard_map/ppermute | solution.py:44
  85.1 3.3 %collective-permute-done.14.refs_3_ = bf16[64,512]{1,0:T(8,128)(2,1)S(1)} collective-permute-done((bf16[64,512]{1,0:T(8,128)(2,1)S(1)}, bf16[64,512]{1,0:T(8,128)(2,1)S(1)}, u32[]{:S(2)}, u32[]{:S(2)}) %collective-permute-start.14) | collective-permute-done | bytes 65568 | tf_op jit(solution)/shard_map/ppermute | solution.py:44
  88.4 11.2 %all_to_all.11 = bf16[8,8,512]{2,1,0:T(8,128)(2,1)S(1)} all-to-all(bf16[8,8,512]{2,1,0:T(8,128)(2,1)S(1)} %bitcast.20), channel_id=1, replica_groups={{0,32,64,96,128,160,192,224},{4,36,68,100,132,164,196,228},{8,40,72,104..., dimensions={0} | all-to-all | bytes 131072 | tf_op jit(solution)/shard_map/all_to_all | solution.py:49
  99.6 0.7 last.1
  (34 shorter events, 3.4 us)
Async XLA Ops:
  0.0 18.5 %copy-start = (s32[32,4]{0,1:T(4,128)S(1)}, s32[32,4]{0,1:T(4,128)}, u32[]{:S(2)}) copy-start(s32[32,4]{0,1:T(4,128)} %param.16) | copy-start | bytes 1540
  7.9 6.6 %collective-permute-start = (bf16[32,2048]{1,0:T(8,128)(2,1)S(1)}, bf16[32,2048]{1,0:T(8,128)(2,1)S(1)}, u32[]{:S(2)}, u32[]{:S(2)}) collective-permute-start(bf16[32,2048]{1,0:T(8,128)(2,1)S(1)} %get-tuple-element.32.refs_0_.after), channel_id=1, source_target_pairs={{0,1},{1,2},{2,3},{3,0},{4,5},{5,6},{6,7},{7,4},{8,9},{9,10},{10,1... | collective-permute-start | bytes 393224 | tf_op jit(solution)/shard_map/ppermute | solution.py:44
  9.6 7.1 %collective-permute-start.1 = (bf16[32,2048]{1,0:T(8,128)(2,1)S(1)}, bf16[32,2048]{1,0:T(8,128)(2,1)S(1)}, u32[]{:S(2)}, u32[]{:S(2)}) collective-permute-start(bf16[32,2048]{1,0:T(8,128)(2,1)S(1)} %get-tuple-element.32.refs_0_.after), channel_id=1, source_target_pairs={{0,3},{1,0},{2,1},{3,2},{4,7},{5,4},{6,5},{7,6},{8,11},{9,8},{10,9... | collective-permute-start | bytes 393224 | tf_op jit(solution)/shard_map/ppermute | solution.py:44
  11.2 7.3 %collective-permute-start.2 = (bf16[32,2048]{1,0:T(8,128)(2,1)S(1)}, bf16[32,2048]{1,0:T(8,128)(2,1)S(1)}, u32[]{:S(2)}, u32[]{:S(2)}) collective-permute-start(bf16[32,2048]{1,0:T(8,128)(2,1)S(1)} %get-tuple-element.32.refs_0_.after), channel_id=1, source_target_pairs={{0,2},{1,3},{2,0},{3,1},{4,6},{5,7},{6,4},{7,5},{8,10},{9,11},{10,... | collective-permute-start | bytes 393224 | tf_op jit(solution)/shard_map/ppermute | solution.py:44
  39.5 6.5 %collective-permute-start.5 = (bf16[64,2176]{1,0:T(8,128)(2,1)S(1)}, bf16[64,2176]{1,0:T(8,128)(2,1)S(1)}, u32[]{:S(2)}, u32[]{:S(2)}) collective-permute-start(bf16[64,2176]{1,0:T(8,128)(2,1)S(1)} %bitcast.14), channel_id=1, source_target_pairs={{0,8},{4,12},{8,16},{12,20},{16,24},{20,28},{24,0},{28,4},{32,40},... | collective-permute-start | bytes 835592 | tf_op jit(solution)/shard_map/ppermute | solution.py:34
  41.0 6.5 %collective-permute-start.6 = (bf16[64,2176]{1,0:T(8,128)(2,1)S(1)}, bf16[64,2176]{1,0:T(8,128)(2,1)S(1)}, u32[]{:S(2)}, u32[]{:S(2)}) collective-permute-start(bf16[64,2176]{1,0:T(8,128)(2,1)S(1)} %bitcast.15), channel_id=1, source_target_pairs={{0,24},{4,28},{8,0},{12,4},{16,8},{20,12},{24,16},{28,20},{32,56},... | collective-permute-start | bytes 835592 | tf_op jit(solution)/shard_map/ppermute | solution.py:34
  46.0 3.4 %collective-permute-start.7 = (bf16[64,2176]{1,0:T(8,128)(2,1)S(1)}, bf16[64,2176]{1,0:T(8,128)(2,1)S(1)}, u32[]{:S(2)}, u32[]{:S(2)}) collective-permute-start(bf16[64,2176]{1,0:T(8,128)(2,1)S(1)} %collective-permute-done.5.refs_0_), channel_id=1, source_target_pairs={{0,4},{4,0},{8,12},{12,8},{16,20},{20,16},{24,28},{28,24},{32,36},... | collective-permute-start | bytes 835592 | tf_op jit(solution)/shard_map/ppermute | solution.py:39
  47.5 1.9 %collective-permute-start.8 = (bf16[64,2176]{1,0:T(8,128)(2,1)S(1)}, bf16[64,2176]{1,0:T(8,128)(2,1)S(1)}, u32[]{:S(2)}, u32[]{:S(2)}) collective-permute-start(bf16[64,2176]{1,0:T(8,128)(2,1)S(1)} %collective-permute-done.6.refs_1_), channel_id=1, source_target_pairs={{0,4},{4,0},{8,12},{12,8},{16,20},{20,16},{24,28},{28,24},{32,36},... | collective-permute-start | bytes 835592 | tf_op jit(solution)/shard_map/ppermute | solution.py:39
  50.5 10.8 %collective-permute-start.9 = (bf16[128,2048]{1,0:T(8,128)(2,1)S(1)}, bf16[128,2048]{1,0:T(8,128)(2,1)S(1)}, u32[]{:S(2)}, u32[]{:S(2)}) collective-permute-start(bf16[128,2048]{1,0:T(8,128)(2,1)S(1)} %get-tuple-element.46), channel_id=1, source_target_pairs={{0,4},{4,0},{8,12},{12,8},{16,20},{20,16},{24,28},{28,24},{32,36},... | collective-permute-start | bytes 1572872 | tf_op jit(solution)/shard_map/ppermute | solution.py:39
  51.1 5.7 %collective-permute-start.15 = (bf16[32,2176]{1,0:T(8,128)(2,1)S(1)}, bf16[32,2176]{1,0:T(8,128)(2,1)S(1)}, u32[]{:S(2)}, u32[]{:S(2)}) collective-permute-start(bf16[32,2176]{1,0:T(8,128)(2,1)S(1)} %slice.8), channel_id=1, source_target_pairs={{0,8},{4,12},{8,16},{12,20},{16,24},{20,28},{24,0},{28,4},{32,40},... | collective-permute-start | bytes 417800 | tf_op jit(solution)/shard_map/ppermute | solution.py:34
  52.4 5.4 %collective-permute-start.16 = (bf16[32,2176]{1,0:T(8,128)(2,1)S(1)}, bf16[32,2176]{1,0:T(8,128)(2,1)S(1)}, u32[]{:S(2)}, u32[]{:S(2)}) collective-permute-start(bf16[32,2176]{1,0:T(8,128)(2,1)S(1)} %slice.9), channel_id=1, source_target_pairs={{0,24},{4,28},{8,0},{12,4},{16,8},{20,12},{24,16},{28,20},{32,56},... | collective-permute-start | bytes 417800 | tf_op jit(solution)/shard_map/ppermute | solution.py:34
  53.3 6.8 %collective-permute-start.3 = (bf16[64,2176]{1,0:T(8,128)(2,1)S(1)}, bf16[64,2176]{1,0:T(8,128)(2,1)S(1)}, u32[]{:S(2)}, u32[]{:S(2)}) collective-permute-start(bf16[64,2176]{1,0:T(8,128)(2,1)S(1)} %bitcast.16), channel_id=1, source_target_pairs={{0,4},{4,0},{8,12},{12,8},{16,20},{20,16},{24,28},{28,24},{32,36},... | collective-permute-start | bytes 835592 | tf_op jit(solution)/shard_map/ppermute | solution.py:39
  56.8 1.4 %collective-permute-start.17 = (bf16[32,2176]{1,0:T(8,128)(2,1)S(1)}, bf16[32,2176]{1,0:T(8,128)(2,1)S(1)}, u32[]{:S(2)}, u32[]{:S(2)}) collective-permute-start(bf16[32,2176]{1,0:T(8,128)(2,1)S(1)} %collective-permute-done.15.refs_0_), channel_id=1, source_target_pairs={{0,4},{4,0},{8,12},{12,8},{16,20},{20,16},{24,28},{28,24},{32,36},... | collective-permute-start | bytes 417800 | tf_op jit(solution)/shard_map/ppermute | solution.py:39
  57.8 1.4 %collective-permute-start.18 = (bf16[32,2176]{1,0:T(8,128)(2,1)S(1)}, bf16[32,2176]{1,0:T(8,128)(2,1)S(1)}, u32[]{:S(2)}, u32[]{:S(2)}) collective-permute-start(bf16[32,2176]{1,0:T(8,128)(2,1)S(1)} %collective-permute-done.16.refs_1_), channel_id=1, source_target_pairs={{0,4},{4,0},{8,12},{12,8},{16,20},{20,16},{24,28},{28,24},{32,36},... | collective-permute-start | bytes 417800 | tf_op jit(solution)/shard_map/ppermute | solution.py:39
  59.9 3.6 %collective-permute-start.19 = (bf16[64,2048]{1,0:T(8,128)(2,1)S(1)}, bf16[64,2048]{1,0:T(8,128)(2,1)S(1)}, u32[]{:S(2)}, u32[]{:S(2)}) collective-permute-start(bf16[64,2048]{1,0:T(8,128)(2,1)S(1)} %get-tuple-element.54), channel_id=1, source_target_pairs={{0,4},{4,0},{8,12},{12,8},{16,20},{20,16},{24,28},{28,24},{32,36},... | collective-permute-start | bytes 786440 | tf_op jit(solution)/shard_map/ppermute | solution.py:39
  60.9 18.2 %collective-permute-start.4 = (bf16[64,2048]{1,0:T(8,128)(2,1)S(1)}, bf16[64,2048]{1,0:T(8,128)(2,1)S(1)}, u32[]{:S(2)}, u32[]{:S(2)}) collective-permute-start(bf16[64,2048]{1,0:T(8,128)(2,1)S(1)} %get-tuple-element.44), channel_id=1, source_target_pairs={{0,4},{4,0},{8,12},{12,8},{16,20},{20,16},{24,28},{28,24},{32,36},... | collective-permute-start | bytes 786440 | tf_op jit(solution)/shard_map/ppermute | solution.py:39
  61.5 17.7 %collective-permute-start.10 = (bf16[64,2048]{1,0:T(8,128)(2,1)S(1)}, bf16[64,2048]{1,0:T(8,128)(2,1)S(1)}, u32[]{:S(2)}, u32[]{:S(2)}) collective-permute-start(bf16[64,2048]{1,0:T(8,128)(2,1)S(1)} %get-tuple-element.47), channel_id=1, source_target_pairs={{0,24},{4,28},{8,0},{12,4},{16,8},{20,12},{24,16},{28,20},{32,56},... | collective-permute-start | bytes 786440 | tf_op jit(solution)/shard_map/ppermute | solution.py:34
  62.7 16.5 %collective-permute-start.11 = (bf16[64,2048]{1,0:T(8,128)(2,1)S(1)}, bf16[64,2048]{1,0:T(8,128)(2,1)S(1)}, u32[]{:S(2)}, u32[]{:S(2)}) collective-permute-start(bf16[64,2048]{1,0:T(8,128)(2,1)S(1)} %get-tuple-element.48), channel_id=1, source_target_pairs={{0,8},{4,12},{8,16},{12,20},{16,24},{20,28},{24,0},{28,4},{32,40},... | collective-permute-start | bytes 786440 | tf_op jit(solution)/shard_map/ppermute | solution.py:34
  63.6 5.6 %collective-permute-start.20 = (bf16[64,512]{1,0:T(8,128)(2,1)S(1)}, bf16[64,512]{1,0:T(8,128)(2,1)S(1)}, u32[]{:S(2)}, u32[]{:S(2)}) collective-permute-start(bf16[64,512]{1,0:T(8,128)(2,1)S(1)} %get-tuple-element.56), channel_id=1, source_target_pairs={{0,1},{1,2},{2,3},{3,0},{4,5},{5,6},{6,7},{7,4},{8,9},{9,10},{10,1... | collective-permute-start | bytes 196616 | tf_op jit(solution)/shard_map/ppermute | solution.py:44
  64.1 5.1 %collective-permute-start.21 = (bf16[64,512]{1,0:T(8,128)(2,1)S(1)}, bf16[64,512]{1,0:T(8,128)(2,1)S(1)}, u32[]{:S(2)}, u32[]{:S(2)}) collective-permute-start(bf16[64,512]{1,0:T(8,128)(2,1)S(1)} %get-tuple-element.57), channel_id=1, source_target_pairs={{0,3},{1,0},{2,1},{3,2},{4,7},{5,4},{6,5},{7,6},{8,11},{9,8},{10,9... | collective-permute-start | bytes 196616 | tf_op jit(solution)/shard_map/ppermute | solution.py:44
  69.2 5.8 %collective-permute-start.22 = (bf16[64,512]{1,0:T(8,128)(2,1)S(1)}, bf16[64,512]{1,0:T(8,128)(2,1)S(1)}, u32[]{:S(2)}, u32[]{:S(2)}) collective-permute-start(bf16[64,512]{1,0:T(8,128)(2,1)S(1)} %get-tuple-element.58), channel_id=1, source_target_pairs={{0,2},{1,3},{2,0},{3,1},{4,6},{5,7},{6,4},{7,5},{8,10},{9,11},{10,... | collective-permute-start | bytes 196616 | tf_op jit(solution)/shard_map/ppermute | solution.py:44
  75.0 7.6 %collective-permute-start.23 = (bf16[64,512]{1,0:T(8,128)(2,1)S(1)}, bf16[64,512]{1,0:T(8,128)(2,1)S(1)}, u32[]{:S(2)}, u32[]{:S(2)}) collective-permute-start(bf16[64,512]{1,0:T(8,128)(2,1)S(1)} %shard_map.152), channel_id=1, source_target_pairs={{0,16},{4,20},{8,24},{12,28},{16,0},{20,4},{24,8},{28,12},{32,48},... | collective-permute-start | bytes 196616 | tf_op jit(solution)/shard_map/ppermute | solution.py:34
  79.3 5.6 %collective-permute-start.12 = (bf16[64,512]{1,0:T(8,128)(2,1)S(1)}, bf16[64,512]{1,0:T(8,128)(2,1)S(1)}, u32[]{:S(2)}, u32[]{:S(2)}) collective-permute-start(bf16[64,512]{1,0:T(8,128)(2,1)S(1)} %get-tuple-element.50), channel_id=1, source_target_pairs={{0,1},{1,2},{2,3},{3,0},{4,5},{5,6},{6,7},{7,4},{8,9},{9,10},{10,1... | collective-permute-start | bytes 196616 | tf_op jit(solution)/shard_map/ppermute | solution.py:44
  79.4 5.7 %collective-permute-start.13 = (bf16[64,512]{1,0:T(8,128)(2,1)S(1)}, bf16[64,512]{1,0:T(8,128)(2,1)S(1)}, u32[]{:S(2)}, u32[]{:S(2)}) collective-permute-start(bf16[64,512]{1,0:T(8,128)(2,1)S(1)} %get-tuple-element.51), channel_id=1, source_target_pairs={{0,3},{1,0},{2,1},{3,2},{4,7},{5,4},{6,5},{7,6},{8,11},{9,8},{10,9... | collective-permute-start | bytes 196616 | tf_op jit(solution)/shard_map/ppermute | solution.py:44
  82.6 5.8 %collective-permute-start.14 = (bf16[64,512]{1,0:T(8,128)(2,1)S(1)}, bf16[64,512]{1,0:T(8,128)(2,1)S(1)}, u32[]{:S(2)}, u32[]{:S(2)}) collective-permute-start(bf16[64,512]{1,0:T(8,128)(2,1)S(1)} %get-tuple-element.52), channel_id=1, source_target_pairs={{0,2},{1,3},{2,0},{3,1},{4,6},{5,7},{6,4},{7,5},{8,10},{9,11},{10,... | collective-permute-start | bytes 196616 | tf_op jit(solution)/shard_map/ppermute | solution.py:44

commit v4 on v3

--- a/solution.py
+++ b/solution.py
@@ -14,7 +14,7 @@
 NX = 4
 NC = 2
 EXTRA = 128
-COPIES = 4
+COPIES = 1
 
 
 EPSILON = 1e-06
@@ -61,11 +61,11 @@
 
 
 def attn_kernel(lengths_hbm, bias_hbm, gain_hbm, wq_hbm, k_hbm, v_hbm, wo_hbm, *refs):
-    small = refs[:4]
-    out, smalls = refs[4], refs[5:9]
+    small = refs[:1]
+    out, smalls = refs[1], refs[2:3]
     residual = smalls[0]
     (lengths, bias, gain, wq, k, v, wo, q_rows, s_rows, o_rows, wq_sem, wo_sem, k_sem, v_sem, small_sem,
-     gain_sem, lengths_sem, bias_sem) = refs[9:]
+     gain_sem, lengths_sem, bias_sem) = refs[3:]
     seqs, _ = residual.shape
     cache = k.shape[1]
     heads = q_rows.shape[0] // seqs
@@ -406,9 +406,12 @@
         lengths,
         key_cache.reshape(key_cache.shape[0], key_cache.shape[1], key_cache.shape[3]),
         value_cache.reshape(value_cache.shape[0], value_cache.shape[1], value_cache.shape[3]),
-        [residual, moe_gain.reshape(1, width), w_group.T, w_expert.T],
-    )
-    weights = fetched((expert_gate[0], expert_up[0], expert_down[0]), head_part)
+        [residual],
+    )
+    tables = (moe_gain.reshape(1, width), w_group.T, w_expert.T)
+    weights = (expert_gate[0], expert_up[0], expert_down[0])
+    fetch = fetched((*tables, *weights), head_part)
+    tables, weights = fetch[:3], fetch[3:]
     head_parts = [head_part]
     for step in (1, 3, 2):
         part = tp_shift(head_part, step)
@@ -423,6 +426,7 @@
         [
             *head_parts,
             *small,
+            *tables,
             routes.T,
         ],
     )

time: 101 us -> 98.1 us (0.971)
  waiting for transfers between devices: 30.9 us -> 28.4 us
  starting transfers between devices: 23.7 us -> 26.1 us
  Pallas kernels: 14.6 us -> 12.9 us
    ppermute x9, waiting for transfers between devices: 19 us -> 14.2 us  [tp_shift(): return lax.ppermute(value, 'tp', [(i, (i + step) % n) for i in range(n)])]
    ppermute x9, starting transfers between devices: 11.9 us -> 15.1 us  [tp_shift(): return lax.ppermute(value, 'tp', [(i, (i + step) % n) for i in range(n)])]
    pallas_call x1, Pallas kernels: 7.89 us -> 6.07 us  [attention(): pl.pallas_call(attn_kernel, out_shape=[pltpu.VMEM(shape, dtype) for shape...]
    ppermute x8, waiting for transfers between devices: 1.37 us -> 2.92 us  [core_swap(): return lax.ppermute(value, 'ep', perm)]
where the time goes in v4:
time: 98.1 us; the launch traced here: 97.9 us
  blocking collectives  30.4 us (31%)
  waiting for transfers between devices  28.4 us (29%)
  starting transfers between devices  26.1 us (27%)
  Pallas kernels  12.9 us (13%)
    all_to_all x2, blocking collectives, z_exchange(): lax.all_to_all(value, 'ep', split_axis=0, concat_axis=0, axis_index_group...  30.4 us
    ppermute x9, starting transfers between devices, tp_shift(): return lax.ppermute(value, 'tp', [(i, (i + step) % n) for i in range(n)])  15.1 us
    ppermute x9, waiting for transfers between devices, tp_shift(): return lax.ppermute(value, 'tp', [(i, (i + step) % n) for i in range(n)])  14.2 us
    ppermute x7, waiting for transfers between devices, x_shift(): return lax.ppermute(value, 'ep', perm)  11.3 us
    ppermute x7, starting transfers between devices, x_shift(): return lax.ppermute(value, 'ep', perm)  9.85 us
    pallas_call x1, Pallas kernels, attention(): pl.pallas_call(attn_kernel, out_shape=[pltpu.VMEM(shape, dtype) for shape...  6.07 us
    pallas_call x9, Pallas kernels, call(): pl.pallas_call(kernel, out_shape=[pltpu.VMEM(shape, dtype) for shape, dty...  4.09 us
    ppermute x8, waiting for transfers between devices, core_swap(): return lax.ppermute(value, 'ep', perm)  2.92 us
  transfers between devices with their start and end apart: 24, of which 14 were waited for; matrix products, arithmetic and copies ran while one was open for 0% of the time, Pallas kernels for 4%

profile of v4, /device:TPU:2, one launch (start us, length us, event | category | flops | bytes accessed | tf_op | source)
XLA Modules:
  0.0 97.9 jit_solution(4551012189680446387)
XLA Ops:
  0.0 6.1 %attend.1 = (bf16[32,2048]{1,0:T(8,128)(2,1)S(1)}, bf16[32,2048]{1,0:T(8,128)(2,1)S(1)}) custom-call(s32[32]{0:T(128)} %lengths_hbm.1, f32[4]{0:T(128)} %bias_hbm.1, f32[1,2048]{1,0:T(1,128)} %bitcast.24, bf16[2048,512]{1,0:T(8,128)(2,1)} %wq_hbm.1, bf16[32,512,128]{2,1,0:T(8,128)(2,1)} %bitcast.22, bf16[32,512,128]{2,1,0:T(8,128)(2,1)} %bitcast.23, ...), custom_call_target="tpu_custom_call" | custom-call | tf_op jit(solution)/shard_map/attend/pallas_call | solution.py:174
  6.1 3.3 %collective-permute-start.2 = (bf16[32,2048]{1,0:T(8,128)(2,1)S(1)}, bf16[32,2048]{1,0:T(8,128)(2,1)S(1)}, u32[]{:S(2)}, u32[]{:S(2)}) collective-permute-start(bf16[32,2048]{1,0:T(8,128)(2,1)S(1)} %get-tuple-element.32.after.refs_0_), channel_id=1, source_target_pairs={{0,2},{1,3},{2,0},{3,1},{4,6},{5,7},{6,4},{7,5},{8,10},{9,11},{10,... | collective-permute-start | bytes 393224 | tf_op jit(solution)/shard_map/ppermute | solution.py:44
  9.4 1.1 %collective-permute-start.1 = (bf16[32,2048]{1,0:T(8,128)(2,1)S(1)}, bf16[32,2048]{1,0:T(8,128)(2,1)S(1)}, u32[]{:S(2)}, u32[]{:S(2)}) collective-permute-start(bf16[32,2048]{1,0:T(8,128)(2,1)S(1)} %get-tuple-element.32.after.refs_0_), channel_id=1, source_target_pairs={{0,3},{1,0},{2,1},{3,2},{4,7},{5,4},{6,5},{7,6},{8,11},{9,8},{10,9... | collective-permute-start | bytes 393224 | tf_op jit(solution)/shard_map/ppermute | solution.py:44
  10.4 1.0 collective-permute-start
  11.4 2.0 %fetch.1 = (f32[1,2048]{1,0:T(1,128)S(1)}, bf16[8,2048]{1,0:T(8,128)(2,1)S(1)}, bf16[64,2048]{1,0:T(8,128)(2,1)S(1)}, bf16[2048,256]{1,0:T(8,128)(2,1)S(1)}, bf1...) custom-call(bf16[32,2048]{1,0:T(8,128)(2,1)S(1)} %get-tuple-element.32.after.refs_0_, f32[1,2048]{1,0:T(1,128)} %bitcast.30, ...), custom_call_target="tpu_custom_call" | custom-call | flops 1073741824 | tf_op jit(solution)/shard_map/fetch/pallas_call | solution.py:310
  13.6 2.5 %collective-permute-done.1.refs_2_ = bf16[32,2048]{1,0:T(8,128)(2,1)S(1)} collective-permute-done((bf16[32,2048]{1,0:T(8,128)(2,1)S(1)}, bf16[32,2048]{1,0:T(8,128)(2,1)S(1)}, u32[]{:S(2)}, u32[]{:S(2)}) %collective-permute-start.1) | collective-permute-done | bytes 131104 | tf_op jit(solution)/shard_map/ppermute | solution.py:44
  16.6 1.2 %shard_map.145 = (bf16[64,2176]{1,0:T(8,128)(2,1)S(1)}, bf16[32,512]{1,0:T(8,128)(2,1)S(1)}, bf16[32,64]{1,0:T(8,128)(2,1)S(1)}) custom-call(bf16[32,2048]{1,0:T(8,128)(2,1)S(1)} %get-tuple-element.32.after.refs_0_, bf16[32,2048]{1,0:T(8,128)(2,1)S(1)} %collective-permute-done.refs_1_, bf16[32,2048]{1,0:T(8,128)(2,1)S(1)} %collective-permute-done.1.refs_2_, ...), custom_call_target="tpu_custom_call" | custom-call | tf_op jit(solution)/shard_map/pallas_call | solution.py:206
  17.8 19.1 %all_to_all.10 = bf16[8,8,2176]{2,1,0:T(8,128)(2,1)S(1)} all-to-all(bf16[8,8,2176]{2,1,0:T(8,128)(2,1)S(1)} %bitcast.18), channel_id=1, replica_groups={{0,32,64,96,128,160,192,224},{4,36,68,100,132,164,196,228},{8,40,72,104..., dimensions={0} | all-to-all | bytes 557056 | tf_op jit(solution)/shard_map/all_to_all | solution.py:49
  37.4 1.5 %collective-permute-start.5 = (bf16[64,2176]{1,0:T(8,128)(2,1)S(1)}, bf16[64,2176]{1,0:T(8,128)(2,1)S(1)}, u32[]{:S(2)}, u32[]{:S(2)}) collective-permute-start(bf16[64,2176]{1,0:T(8,128)(2,1)S(1)} %bitcast.15), channel_id=1, source_target_pairs={{0,8},{4,12},{8,16},{12,20},{16,24},{20,28},{24,0},{28,4},{32,40},... | collective-permute-start | bytes 835592 | tf_op jit(solution)/shard_map/ppermute | solution.py:34
  38.9 4.5 %collective-permute-done.6.refs_1_ = bf16[64,2176]{1,0:T(8,128)(2,1)S(1)} collective-permute-done((bf16[64,2176]{1,0:T(8,128)(2,1)S(1)}, bf16[64,2176]{1,0:T(8,128)(2,1)S(1)}, u32[]{:S(2)}, u32[]{:S(2)}) %collective-permute-start.6) | collective-permute-done | bytes 278560 | tf_op jit(solution)/shard_map/ppermute | solution.py:34
  43.4 1.3 %collective-permute-done.5.refs_0_ = bf16[64,2176]{1,0:T(8,128)(2,1)S(1)} collective-permute-done((bf16[64,2176]{1,0:T(8,128)(2,1)S(1)}, bf16[64,2176]{1,0:T(8,128)(2,1)S(1)}, u32[]{:S(2)}, u32[]{:S(2)}) %collective-permute-start.5) | collective-permute-done | bytes 278560 | tf_op jit(solution)/shard_map/ppermute | solution.py:34
  45.0 1.3 %collective-permute-done.7.refs_2_ = bf16[64,2176]{1,0:T(8,128)(2,1)S(1)} collective-permute-done((bf16[64,2176]{1,0:T(8,128)(2,1)S(1)}, bf16[64,2176]{1,0:T(8,128)(2,1)S(1)}, u32[]{:S(2)}, u32[]{:S(2)}) %collective-permute-start.7) | collective-permute-done | bytes 278560 | tf_op jit(solution)/shard_map/ppermute | solution.py:39
  46.2 1.1 %shard_map.147 = (bf16[128,2048]{1,0:T(8,128)(2,1)S(1)}, bf16[128,2048]{1,0:T(8,128)(2,1)S(1)}) custom-call(bf16[64,2176]{1,0:T(8,128)(2,1)S(1)} %collective-permute-done.5.refs_0_, bf16[64,2176]{1,0:T(8,128)(2,1)S(1)} %collective-permute-done.6.refs_1_, bf16[64,2176]{1,0:T(8,128)(2,1)S(1)} %collective-permute-done.7.refs_2_, ...), custom_call_target="tpu_custom_call" | custom-call | flops 805306368 | tf_op jit(solution)/shard_map/pallas_call | solution.py:206
  47.6 3.3 %collective-permute-start.16 = (bf16[32,2176]{1,0:T(8,128)(2,1)S(1)}, bf16[32,2176]{1,0:T(8,128)(2,1)S(1)}, u32[]{:S(2)}, u32[]{:S(2)}) collective-permute-start(bf16[32,2176]{1,0:T(8,128)(2,1)S(1)} %slice.9), channel_id=1, source_target_pairs={{0,24},{4,28},{8,0},{12,4},{16,8},{20,12},{24,16},{28,20},{32,56},... | collective-permute-start | bytes 417800 | tf_op jit(solution)/shard_map/ppermute | solution.py:34
  51.2 3.2 %collective-permute-done.16.refs_1_ = bf16[32,2176]{1,0:T(8,128)(2,1)S(1)} collective-permute-done((bf16[32,2176]{1,0:T(8,128)(2,1)S(1)}, bf16[32,2176]{1,0:T(8,128)(2,1)S(1)}, u32[]{:S(2)}, u32[]{:S(2)}) %collective-permute-start.16) | collective-permute-done | bytes 139296 | tf_op jit(solution)/shard_map/ppermute | solution.py:34
  54.4 2.3 %collective-permute-done.15.refs_0_ = bf16[32,2176]{1,0:T(8,128)(2,1)S(1)} collective-permute-done((bf16[32,2176]{1,0:T(8,128)(2,1)S(1)}, bf16[32,2176]{1,0:T(8,128)(2,1)S(1)}, u32[]{:S(2)}, u32[]{:S(2)}) %collective-permute-start.15) | collective-permute-done | bytes 139296 | tf_op jit(solution)/shard_map/ppermute | solution.py:34
  56.7 1.4 %collective-permute-done.17.refs_2_ = bf16[32,2176]{1,0:T(8,128)(2,1)S(1)} collective-permute-done((bf16[32,2176]{1,0:T(8,128)(2,1)S(1)}, bf16[32,2176]{1,0:T(8,128)(2,1)S(1)}, u32[]{:S(2)}, u32[]{:S(2)}) %collective-permute-start.17) | collective-permute-done | bytes 139296 | tf_op jit(solution)/shard_map/ppermute | solution.py:39
  58.0 0.7 shard_map.150
  59.0 0.7 shard_map.146
  60.3 1.7 %collective-permute-start.10 = (bf16[64,2048]{1,0:T(8,128)(2,1)S(1)}, bf16[64,2048]{1,0:T(8,128)(2,1)S(1)}, u32[]{:S(2)}, u32[]{:S(2)}) collective-permute-start(bf16[64,2048]{1,0:T(8,128)(2,1)S(1)} %get-tuple-element.47), channel_id=1, source_target_pairs={{0,24},{4,28},{8,0},{12,4},{16,8},{20,12},{24,16},{28,20},{32,56},... | collective-permute-start | bytes 786440 | tf_op jit(solution)/shard_map/ppermute | solution.py:34
  62.5 2.3 %collective-permute-start.20 = (bf16[64,512]{1,0:T(8,128)(2,1)S(1)}, bf16[64,512]{1,0:T(8,128)(2,1)S(1)}, u32[]{:S(2)}, u32[]{:S(2)}) collective-permute-start(bf16[64,512]{1,0:T(8,128)(2,1)S(1)} %get-tuple-element.56), channel_id=1, source_target_pairs={{0,1},{1,2},{2,3},{3,0},{4,5},{5,6},{6,7},{7,4},{8,9},{9,10},{10,1... | collective-permute-start | bytes 196616 | tf_op jit(solution)/shard_map/ppermute | solution.py:44
  64.8 1.5 %collective-permute-start.21 = (bf16[64,512]{1,0:T(8,128)(2,1)S(1)}, bf16[64,512]{1,0:T(8,128)(2,1)S(1)}, u32[]{:S(2)}, u32[]{:S(2)}) collective-permute-start(bf16[64,512]{1,0:T(8,128)(2,1)S(1)} %get-tuple-element.57), channel_id=1, source_target_pairs={{0,3},{1,0},{2,1},{3,2},{4,7},{5,4},{6,5},{7,6},{8,11},{9,8},{10,9... | collective-permute-start | bytes 196616 | tf_op jit(solution)/shard_map/ppermute | solution.py:44
  66.2 2.2 %collective-permute-done.20.refs_1_ = bf16[64,512]{1,0:T(8,128)(2,1)S(1)} collective-permute-done((bf16[64,512]{1,0:T(8,128)(2,1)S(1)}, bf16[64,512]{1,0:T(8,128)(2,1)S(1)}, u32[]{:S(2)}, u32[]{:S(2)}) %collective-permute-start.20) | collective-permute-done | bytes 65568 | tf_op jit(solution)/shard_map/ppermute | solution.py:44
  68.4 2.0 %collective-permute-start.22 = (bf16[64,512]{1,0:T(8,128)(2,1)S(1)}, bf16[64,512]{1,0:T(8,128)(2,1)S(1)}, u32[]{:S(2)}, u32[]{:S(2)}) collective-permute-start(bf16[64,512]{1,0:T(8,128)(2,1)S(1)} %get-tuple-element.58), channel_id=1, source_target_pairs={{0,2},{1,3},{2,0},{3,1},{4,6},{5,7},{6,4},{7,5},{8,10},{9,11},{10,... | collective-permute-start | bytes 196616 | tf_op jit(solution)/shard_map/ppermute | solution.py:44
  70.4 3.7 %collective-permute-done.22.refs_3_ = bf16[64,512]{1,0:T(8,128)(2,1)S(1)} collective-permute-done((bf16[64,512]{1,0:T(8,128)(2,1)S(1)}, bf16[64,512]{1,0:T(8,128)(2,1)S(1)}, u32[]{:S(2)}, u32[]{:S(2)}) %collective-permute-start.22) | collective-permute-done | bytes 65568 | tf_op jit(solution)/shard_map/ppermute | solution.py:44
  74.2 2.3 %collective-permute-start.23 = (bf16[64,512]{1,0:T(8,128)(2,1)S(1)}, bf16[64,512]{1,0:T(8,128)(2,1)S(1)}, u32[]{:S(2)}, u32[]{:S(2)}) collective-permute-start(bf16[64,512]{1,0:T(8,128)(2,1)S(1)} %shard_map.152), channel_id=1, source_target_pairs={{0,16},{4,20},{8,24},{12,28},{16,0},{20,4},{24,8},{28,12},{32,48},... | collective-permute-start | bytes 196616 | tf_op jit(solution)/shard_map/ppermute | solution.py:34
  76.7 0.7 collective-permute-start.12
  77.4 2.6 %collective-permute-start.13 = (bf16[64,512]{1,0:T(8,128)(2,1)S(1)}, bf16[64,512]{1,0:T(8,128)(2,1)S(1)}, u32[]{:S(2)}, u32[]{:S(2)}) collective-permute-start(bf16[64,512]{1,0:T(8,128)(2,1)S(1)} %get-tuple-element.51), channel_id=1, source_target_pairs={{0,3},{1,0},{2,1},{3,2},{4,7},{5,4},{6,5},{7,6},{8,11},{9,8},{10,9... | collective-permute-start | bytes 196616 | tf_op jit(solution)/shard_map/ppermute | solution.py:44
  80.7 2.0 %collective-permute-done.12.refs_1_ = bf16[64,512]{1,0:T(8,128)(2,1)S(1)} collective-permute-done((bf16[64,512]{1,0:T(8,128)(2,1)S(1)}, bf16[64,512]{1,0:T(8,128)(2,1)S(1)}, u32[]{:S(2)}, u32[]{:S(2)}) %collective-permute-start.12) | collective-permute-done | bytes 65568 | tf_op jit(solution)/shard_map/ppermute | solution.py:44
  82.7 3.1 %collective-permute-done.14.refs_3_ = bf16[64,512]{1,0:T(8,128)(2,1)S(1)} collective-permute-done((bf16[64,512]{1,0:T(8,128)(2,1)S(1)}, bf16[64,512]{1,0:T(8,128)(2,1)S(1)}, u32[]{:S(2)}, u32[]{:S(2)}) %collective-permute-start.14) | collective-permute-done | bytes 65568 | tf_op jit(solution)/shard_map/ppermute | solution.py:44
  85.8 11.3 %all_to_all.11 = bf16[8,8,512]{2,1,0:T(8,128)(2,1)S(1)} all-to-all(bf16[8,8,512]{2,1,0:T(8,128)(2,1)S(1)} %bitcast.20), channel_id=1, replica_groups={{0,32,64,96,128,160,192,224},{4,36,68,100,132,164,196,228},{8,40,72,104..., dimensions={0} | all-to-all | bytes 131072 | tf_op jit(solution)/shard_map/all_to_all | solution.py:49
  97.1 0.7 last.1
  (34 shorter events, 4.2 us)
Async XLA Ops:
  0.0 16.6 %copy-start = (s32[32,4]{0,1:T(4,128)S(1)}, s32[32,4]{0,1:T(4,128)}, u32[]{:S(2)}) copy-start(s32[32,4]{0,1:T(4,128)} %param.16) | copy-start | bytes 1540
  6.1 7.5 %collective-permute-start.2 = (bf16[32,2048]{1,0:T(8,128)(2,1)S(1)}, bf16[32,2048]{1,0:T(8,128)(2,1)S(1)}, u32[]{:S(2)}, u32[]{:S(2)}) collective-permute-start(bf16[32,2048]{1,0:T(8,128)(2,1)S(1)} %get-tuple-element.32.after.refs_0_), channel_id=1, source_target_pairs={{0,2},{1,3},{2,0},{3,1},{4,6},{5,7},{6,4},{7,5},{8,10},{9,11},{10,... | collective-permute-start | bytes 393224 | tf_op jit(solution)/shard_map/ppermute | solution.py:44
  9.4 6.7 %collective-permute-start.1 = (bf16[32,2048]{1,0:T(8,128)(2,1)S(1)}, bf16[32,2048]{1,0:T(8,128)(2,1)S(1)}, u32[]{:S(2)}, u32[]{:S(2)}) collective-permute-start(bf16[32,2048]{1,0:T(8,128)(2,1)S(1)} %get-tuple-element.32.after.refs_0_), channel_id=1, source_target_pairs={{0,3},{1,0},{2,1},{3,2},{4,7},{5,4},{6,5},{7,6},{8,11},{9,8},{10,9... | collective-permute-start | bytes 393224 | tf_op jit(solution)/shard_map/ppermute | solution.py:44
  10.4 6.2 %collective-permute-start = (bf16[32,2048]{1,0:T(8,128)(2,1)S(1)}, bf16[32,2048]{1,0:T(8,128)(2,1)S(1)}, u32[]{:S(2)}, u32[]{:S(2)}) collective-permute-start(bf16[32,2048]{1,0:T(8,128)(2,1)S(1)} %get-tuple-element.32.after.refs_0_), channel_id=1, source_target_pairs={{0,1},{1,2},{2,3},{3,0},{4,5},{5,6},{6,7},{7,4},{8,9},{9,10},{10,1... | collective-permute-start | bytes 393224 | tf_op jit(solution)/shard_map/ppermute | solution.py:44
  36.9 6.5 %collective-permute-start.6 = (bf16[64,2176]{1,0:T(8,128)(2,1)S(1)}, bf16[64,2176]{1,0:T(8,128)(2,1)S(1)}, u32[]{:S(2)}, u32[]{:S(2)}) collective-permute-start(bf16[64,2176]{1,0:T(8,128)(2,1)S(1)} %bitcast.14), channel_id=1, source_target_pairs={{0,24},{4,28},{8,0},{12,4},{16,8},{20,12},{24,16},{28,20},{32,56},... | collective-permute-start | bytes 835592 | tf_op jit(solution)/shard_map/ppermute | solution.py:34
  37.4 7.3 %collective-permute-start.5 = (bf16[64,2176]{1,0:T(8,128)(2,1)S(1)}, bf16[64,2176]{1,0:T(8,128)(2,1)S(1)}, u32[]{:S(2)}, u32[]{:S(2)}) collective-permute-start(bf16[64,2176]{1,0:T(8,128)(2,1)S(1)} %bitcast.15), channel_id=1, source_target_pairs={{0,8},{4,12},{8,16},{12,20},{16,24},{20,28},{24,0},{28,4},{32,40},... | collective-permute-start | bytes 835592 | tf_op jit(solution)/shard_map/ppermute | solution.py:34
  43.4 1.6 %collective-permute-start.8 = (bf16[64,2176]{1,0:T(8,128)(2,1)S(1)}, bf16[64,2176]{1,0:T(8,128)(2,1)S(1)}, u32[]{:S(2)}, u32[]{:S(2)}) collective-permute-start(bf16[64,2176]{1,0:T(8,128)(2,1)S(1)} %collective-permute-done.6.refs_1_), channel_id=1, source_target_pairs={{0,4},{4,0},{8,12},{12,8},{16,20},{20,16},{24,28},{28,24},{32,36},... | collective-permute-start | bytes 835592 | tf_op jit(solution)/shard_map/ppermute | solution.py:39
  44.7 1.6 %collective-permute-start.7 = (bf16[64,2176]{1,0:T(8,128)(2,1)S(1)}, bf16[64,2176]{1,0:T(8,128)(2,1)S(1)}, u32[]{:S(2)}, u32[]{:S(2)}) collective-permute-start(bf16[64,2176]{1,0:T(8,128)(2,1)S(1)} %collective-permute-done.5.refs_0_), channel_id=1, source_target_pairs={{0,4},{4,0},{8,12},{12,8},{16,20},{20,16},{24,28},{28,24},{32,36},... | collective-permute-start | bytes 835592 | tf_op jit(solution)/shard_map/ppermute | solution.py:39
  47.3 12.8 %collective-permute-start.9 = (bf16[128,2048]{1,0:T(8,128)(2,1)S(1)}, bf16[128,2048]{1,0:T(8,128)(2,1)S(1)}, u32[]{:S(2)}, u32[]{:S(2)}) collective-permute-start(bf16[128,2048]{1,0:T(8,128)(2,1)S(1)} %get-tuple-element.46), channel_id=1, source_target_pairs={{0,4},{4,0},{8,12},{12,8},{16,20},{20,16},{24,28},{28,24},{32,36},... | collective-permute-start | bytes 1572872 | tf_op jit(solution)/shard_map/ppermute | solution.py:39
  47.6 6.8 %collective-permute-start.16 = (bf16[32,2176]{1,0:T(8,128)(2,1)S(1)}, bf16[32,2176]{1,0:T(8,128)(2,1)S(1)}, u32[]{:S(2)}, u32[]{:S(2)}) collective-permute-start(bf16[32,2176]{1,0:T(8,128)(2,1)S(1)} %slice.9), channel_id=1, source_target_pairs={{0,24},{4,28},{8,0},{12,4},{16,8},{20,12},{24,16},{28,20},{32,56},... | collective-permute-start | bytes 417800 | tf_op jit(solution)/shard_map/ppermute | solution.py:34
  50.9 5.7 %collective-permute-start.15 = (bf16[32,2176]{1,0:T(8,128)(2,1)S(1)}, bf16[32,2176]{1,0:T(8,128)(2,1)S(1)}, u32[]{:S(2)}, u32[]{:S(2)}) collective-permute-start(bf16[32,2176]{1,0:T(8,128)(2,1)S(1)} %slice.8), channel_id=1, source_target_pairs={{0,8},{4,12},{8,16},{12,20},{16,24},{20,28},{24,0},{28,4},{32,40},... | collective-permute-start | bytes 417800 | tf_op jit(solution)/shard_map/ppermute | solution.py:34
  51.0 8.0 %collective-permute-start.3 = (bf16[64,2176]{1,0:T(8,128)(2,1)S(1)}, bf16[64,2176]{1,0:T(8,128)(2,1)S(1)}, u32[]{:S(2)}, u32[]{:S(2)}) collective-permute-start(bf16[64,2176]{1,0:T(8,128)(2,1)S(1)} %bitcast.16), channel_id=1, source_target_pairs={{0,4},{4,0},{8,12},{12,8},{16,20},{20,16},{24,28},{28,24},{32,36},... | collective-permute-start | bytes 835592 | tf_op jit(solution)/shard_map/ppermute | solution.py:39
  54.4 2.3 %collective-permute-start.18 = (bf16[32,2176]{1,0:T(8,128)(2,1)S(1)}, bf16[32,2176]{1,0:T(8,128)(2,1)S(1)}, u32[]{:S(2)}, u32[]{:S(2)}) collective-permute-start(bf16[32,2176]{1,0:T(8,128)(2,1)S(1)} %collective-permute-done.16.refs_1_), channel_id=1, source_target_pairs={{0,4},{4,0},{8,12},{12,8},{16,20},{20,16},{24,28},{28,24},{32,36},... | collective-permute-start | bytes 417800 | tf_op jit(solution)/shard_map/ppermute | solution.py:39
  56.6 1.4 %collective-permute-start.17 = (bf16[32,2176]{1,0:T(8,128)(2,1)S(1)}, bf16[32,2176]{1,0:T(8,128)(2,1)S(1)}, u32[]{:S(2)}, u32[]{:S(2)}) collective-permute-start(bf16[32,2176]{1,0:T(8,128)(2,1)S(1)} %collective-permute-done.15.refs_0_), channel_id=1, source_target_pairs={{0,4},{4,0},{8,12},{12,8},{16,20},{20,16},{24,28},{28,24},{32,36},... | collective-permute-start | bytes 417800 | tf_op jit(solution)/shard_map/ppermute | solution.py:39
  58.7 3.6 %collective-permute-start.19 = (bf16[64,2048]{1,0:T(8,128)(2,1)S(1)}, bf16[64,2048]{1,0:T(8,128)(2,1)S(1)}, u32[]{:S(2)}, u32[]{:S(2)}) collective-permute-start(bf16[64,2048]{1,0:T(8,128)(2,1)S(1)} %get-tuple-element.54), channel_id=1, source_target_pairs={{0,4},{4,0},{8,12},{12,8},{16,20},{20,16},{24,28},{28,24},{32,36},... | collective-permute-start | bytes 786440 | tf_op jit(solution)/shard_map/ppermute | solution.py:39
  59.7 16.8 %collective-permute-start.4 = (bf16[64,2048]{1,0:T(8,128)(2,1)S(1)}, bf16[64,2048]{1,0:T(8,128)(2,1)S(1)}, u32[]{:S(2)}, u32[]{:S(2)}) collective-permute-start(bf16[64,2048]{1,0:T(8,128)(2,1)S(1)} %get-tuple-element.44), channel_id=1, source_target_pairs={{0,4},{4,0},{8,12},{12,8},{16,20},{20,16},{24,28},{28,24},{32,36},... | collective-permute-start | bytes 786440 | tf_op jit(solution)/shard_map/ppermute | solution.py:39
  60.3 16.2 %collective-permute-start.10 = (bf16[64,2048]{1,0:T(8,128)(2,1)S(1)}, bf16[64,2048]{1,0:T(8,128)(2,1)S(1)}, u32[]{:S(2)}, u32[]{:S(2)}) collective-permute-start(bf16[64,2048]{1,0:T(8,128)(2,1)S(1)} %get-tuple-element.47), channel_id=1, source_target_pairs={{0,24},{4,28},{8,0},{12,4},{16,8},{20,12},{24,16},{28,20},{32,56},... | collective-permute-start | bytes 786440 | tf_op jit(solution)/shard_map/ppermute | solution.py:34
  62.0 14.6 %collective-permute-start.11 = (bf16[64,2048]{1,0:T(8,128)(2,1)S(1)}, bf16[64,2048]{1,0:T(8,128)(2,1)S(1)}, u32[]{:S(2)}, u32[]{:S(2)}) collective-permute-start(bf16[64,2048]{1,0:T(8,128)(2,1)S(1)} %get-tuple-element.48), channel_id=1, source_target_pairs={{0,8},{4,12},{8,16},{12,20},{16,24},{20,28},{24,0},{28,4},{32,40},... | collective-permute-start | bytes 786440 | tf_op jit(solution)/shard_map/ppermute | solution.py:34
  62.5 5.9 %collective-permute-start.20 = (bf16[64,512]{1,0:T(8,128)(2,1)S(1)}, bf16[64,512]{1,0:T(8,128)(2,1)S(1)}, u32[]{:S(2)}, u32[]{:S(2)}) collective-permute-start(bf16[64,512]{1,0:T(8,128)(2,1)S(1)} %get-tuple-element.56), channel_id=1, source_target_pairs={{0,1},{1,2},{2,3},{3,0},{4,5},{5,6},{6,7},{7,4},{8,9},{9,10},{10,1... | collective-permute-start | bytes 196616 | tf_op jit(solution)/shard_map/ppermute | solution.py:44
  64.8 5.7 %collective-permute-start.21 = (bf16[64,512]{1,0:T(8,128)(2,1)S(1)}, bf16[64,512]{1,0:T(8,128)(2,1)S(1)}, u32[]{:S(2)}, u32[]{:S(2)}) collective-permute-start(bf16[64,512]{1,0:T(8,128)(2,1)S(1)} %get-tuple-element.57), channel_id=1, source_target_pairs={{0,3},{1,0},{2,1},{3,2},{4,7},{5,4},{6,5},{7,6},{8,11},{9,8},{10,9... | collective-permute-start | bytes 196616 | tf_op jit(solution)/shard_map/ppermute | solution.py:44
  68.4 5.8 %collective-permute-start.22 = (bf16[64,512]{1,0:T(8,128)(2,1)S(1)}, bf16[64,512]{1,0:T(8,128)(2,1)S(1)}, u32[]{:S(2)}, u32[]{:S(2)}) collective-permute-start(bf16[64,512]{1,0:T(8,128)(2,1)S(1)} %get-tuple-element.58), channel_id=1, source_target_pairs={{0,2},{1,3},{2,0},{3,1},{4,6},{5,7},{6,4},{7,5},{8,10},{9,11},{10,... | collective-permute-start | bytes 196616 | tf_op jit(solution)/shard_map/ppermute | solution.py:44
  74.2 6.5 %collective-permute-start.23 = (bf16[64,512]{1,0:T(8,128)(2,1)S(1)}, bf16[64,512]{1,0:T(8,128)(2,1)S(1)}, u32[]{:S(2)}, u32[]{:S(2)}) collective-permute-start(bf16[64,512]{1,0:T(8,128)(2,1)S(1)} %shard_map.152), channel_id=1, source_target_pairs={{0,16},{4,20},{8,24},{12,28},{16,0},{20,4},{24,8},{28,12},{32,48},... | collective-permute-start | bytes 196616 | tf_op jit(solution)/shard_map/ppermute | solution.py:34
  76.7 6.0 %collective-permute-start.12 = (bf16[64,512]{1,0:T(8,128)(2,1)S(1)}, bf16[64,512]{1,0:T(8,128)(2,1)S(1)}, u32[]{:S(2)}, u32[]{:S(2)}) collective-permute-start(bf16[64,512]{1,0:T(8,128)(2,1)S(1)} %get-tuple-element.50), channel_id=1, source_target_pairs={{0,1},{1,2},{2,3},{3,0},{4,5},{5,6},{6,7},{7,4},{8,9},{9,10},{10,1... | collective-permute-start | bytes 196616 | tf_op jit(solution)/shard_map/ppermute | solution.py:44
  77.4 5.3 %collective-permute-start.13 = (bf16[64,512]{1,0:T(8,128)(2,1)S(1)}, bf16[64,512]{1,0:T(8,128)(2,1)S(1)}, u32[]{:S(2)}, u32[]{:S(2)}) collective-permute-start(bf16[64,512]{1,0:T(8,128)(2,1)S(1)} %get-tuple-element.51), channel_id=1, source_target_pairs={{0,3},{1,0},{2,1},{3,2},{4,7},{5,4},{6,5},{7,6},{8,11},{9,8},{10,9... | collective-permute-start | bytes 196616 | tf_op jit(solution)/shard_map/ppermute | solution.py:44
  80.0 5.8 %collective-permute-start.14 = (bf16[64,512]{1,0:T(8,128)(2,1)S(1)}, bf16[64,512]{1,0:T(8,128)(2,1)S(1)}, u32[]{:S(2)}, u32[]{:S(2)}) collective-permute-start(bf16[64,512]{1,0:T(8,128)(2,1)S(1)} %get-tuple-element.52), channel_id=1, source_target_pairs={{0,2},{1,3},{2,0},{3,1},{4,6},{5,7},{6,4},{7,5},{8,10},{9,11},{10,... | collective-permute-start | bytes 196616 | tf_op jit(solution)/shard_map/ppermute | solution.py:44
